TPU v7x, 512 devices: a whole 4x4x16 slice. The times are simulated.
512 devices in a mesh: ep: 32 (over z, core), tp: 16 (over y, x).
Axes of the slice: x: 4, y: 4, z: 16, core: 2. Of those that a mesh axis runs over, the one named last changes fastest.
Arguments:
- tokens: bfloat16 [512, 2048], P('ep'), may hold values from -6 to 6
- attn_gain: float32 [2048], replicated, may hold values from 0.1 to 1.9
- query_weight: bfloat16 [2048, 2048], P('ep', 'tp'), may hold values from -0.125 to 0.125
- key_weight: bfloat16 [2048, 2048], P('ep', 'tp'), may hold values from -0.125 to 0.125
- value_weight: bfloat16 [2048, 2048], P('ep', 'tp'), may hold values from -0.125 to 0.125
- forget_weight: bfloat16 [2048, 16], P(None, 'tp'), may hold values from -0.125 to 0.125
- forget_bias: float32 [16], P('tp'), may hold values from -1 to 2
- cache_keys: bfloat16 [512, 16, 384, 128], P('ep', 'tp'), may hold values from -240 to 240
- cache_values: bfloat16 [512, 16, 384, 128], P('ep', 'tp'), may hold values from -6 to 6
- cache_gates: float32 [512, 16, 384], P('ep', 'tp'), may hold values from -768 to 0, as said below
- lengths: int32 [512], P('ep'), may hold values from 1 to 384
- output_weight: bfloat16 [2048, 2048], P('tp', 'ep'), may hold values from -0.125 to 0.125
- ffn_gain: float32 [2048], replicated, may hold values from 0.1 to 1.9
- dense_gate_proj: bfloat16 [2048, 2048], P('ep', 'tp'), may hold values from -0.125 to 0.125
- dense_up_proj: bfloat16 [2048, 2048], P('ep', 'tp'), may hold values from -0.125 to 0.125
- dense_down_proj: bfloat16 [2048, 2048], P('tp', 'ep'), may hold values from -0.125 to 0.125
- dense_mix: bfloat16 [2048], replicated, may hold values from -0.125 to 0.125
- expert_ids: int32 [512, 2], P('ep'), may hold values from 0 to 31, as said below
- group_prob: float32 [512], P('ep'), may hold values from 0.25 to 1
- pair_prob: float32 [512, 2], P('ep'), may hold values from 0.05 to 1
- expert_gate: bfloat16 [32, 2048, 2048], P('ep', None, 'tp'), may hold values from -0.125 to 0.125
- expert_up: bfloat16 [32, 2048, 2048], P('ep', None, 'tp'), may hold values from -0.125 to 0.125
- expert_down: bfloat16 [32, 2048, 2048], P('ep', 'tp'), may hold values from -0.125 to 0.125
Outputs:
- mixed_out: bfloat16 [512, 2048], P('ep')
Inputs may be any that keep to these rules, and one draw needn't show every extreme that they name: `expert_ids`: each row names two different experts of one group, the groups being 4 runs of consecutive ids. In each aligned block of 16 rows (the rows of one index of ep) no expert is named more than 2 times, and some expert exactly 2 times. `cache_gates`: along positions the values never rise.
All inputs are finite; a program needn't handle non-finite values.
Results may differ from a plain program's by a relative error of at most 0.014.
Values may be sent and summed in bfloat16 or wider, within the bound.
No kernel may reach another device: no remote copies, remote signals or barrier semaphores. Data moves between devices by JAX's collectives and lax.ppermute only.
A program may use at most 64 MiB of HBM per device.

v0:
```python
import math

import jax
import jax.numpy as jnp
from jax import lax
from jax.sharding import Mesh
from jax.sharding import PartitionSpec as P


EP = ("zh", "zl", "c")
Z = ("zh", "zl")
TP = ("y", "x")
EPSILON = 1e-06


def exchanged(pieces, axes):
    return lax.all_to_all(pieces, axes, split_axis=0, concat_axis=0, tiled=True)


def from_all(array, axis):
    return exchanged(jnp.broadcast_to(array, (lax.axis_size(axis), *array.shape)), axis)


def summed_over_heads(array):
    rows = jnp.sum(from_all(array, "x").astype(jnp.float32), axis=0).astype(jnp.bfloat16)
    return jnp.sum(from_all(rows, "y").astype(jnp.float32), axis=0)


def in_order(own, theirs, place, dim):
    return jnp.where(
        place == 0,
        jnp.concatenate((own, theirs), axis=dim),
        jnp.concatenate((theirs, own), axis=dim),
    )


def product(left, right):
    return jnp.dot(left, right, preferred_element_type=jnp.float32)


def product_transposed(left, right):
    return lax.dot_general(
        left, right, (((1,), (1,)), ((), ())), preferred_element_type=jnp.float32
    )


def rms_scale(values, norm_gain):
    widened = values.astype(jnp.float32)
    return (
        widened
        * lax.rsqrt(jnp.mean(widened * widened, axis=-1, keepdims=True) + EPSILON)
        * norm_gain
    )


def attend(queries, keys_new, values_new, key_cache, value_cache, gate_cache, lengths, log_forget):
    cache_span = key_cache.shape[2]
    score_scale = 1.0 / math.sqrt(key_cache.shape[3])
    positions = jnp.arange(cache_span, dtype=jnp.int32)
    live_mask = positions[None, :] < lengths[:, None]
    last_mask = positions[None, :] == lengths[:, None] - 1
    last_gate = jnp.sum(jnp.where(last_mask[:, None, :], gate_cache, 0.0), axis=-1)
    gate_now = last_gate + log_forget
    scores = (
        jnp.einsum("shd,shpd->shp", queries, key_cache, preferred_element_type=jnp.float32)
        * score_scale
    )
    scores = scores + gate_now[:, :, None] - gate_cache
    scores = jnp.where(live_mask[:, None, :], scores, -jnp.inf)
    own_score = (
        jnp.sum(queries.astype(jnp.float32) * keys_new.astype(jnp.float32), axis=-1) * score_scale
    )
    row_top = jnp.maximum(jnp.max(scores, axis=-1), own_score)
    raised = jnp.exp(scores - row_top[:, :, None])
    own_raised = jnp.exp(own_score - row_top)
    totals = jnp.sum(raised, axis=-1) + own_raised
    weights_low = (raised / totals[:, :, None]).astype(jnp.bfloat16)
    own_prob = (own_raised / totals).astype(jnp.bfloat16)
    attended = jnp.einsum(
        "shp,shpd->shd", weights_low, value_cache, preferred_element_type=jnp.float32
    )
    attended = attended + own_prob.astype(jnp.float32)[:, :, None] * values_new.astype(jnp.float32)
    return attended.astype(jnp.bfloat16)


def layer(
    tokens,
    attn_gain,
    query_weight,
    key_weight,
    value_weight,
    forget_weight,
    forget_bias,
    cache_keys,
    cache_values,
    cache_gates,
    lengths,
    output_weight,
    ffn_gain,
    dense_gate_proj,
    dense_up_proj,
    dense_down_proj,
    dense_mix,
    expert_ids,
    group_prob,
    pair_prob,
    expert_gate,
    expert_up,
    expert_down,
):
    seq_count, width = tokens.shape
    head_size = cache_keys.shape[3]
    chips = lax.axis_size(Z)
    quarters = lax.axis_size("zl")
    devices = lax.axis_size(EP)
    slab = width // chips
    core = lax.axis_index("c")
    side = lax.axis_index("zl") % 2
    pairs = chips // 2
    half = seq_count // 2

    own_rows = jnp.concatenate(
        (query_weight, key_weight, value_weight, dense_gate_proj, dense_up_proj), axis=1
    )
    chip_rows = in_order(own_rows, lax.ppermute(own_rows, "c", [(0, 1), (1, 0)]), core, 0)
    neighbours = [(k, k ^ 1) for k in range(quarters)]
    pair_rows = in_order(chip_rows, lax.ppermute(chip_rows, "zl", neighbours), side, 0)
    projection_width = 3 * head_size

    normed = rms_scale(tokens, attn_gain).astype(jnp.bfloat16)
    token_pieces = normed.reshape(2, half, pairs, 2, slab).transpose(2, 0, 3, 1, 4)
    token_pieces = token_pieces.reshape(chips, seq_count, slab)
    held = output_weight.shape[1]
    part = held // quarters
    out_parts = output_weight.T.reshape(quarters, part, head_size)
    down_parts = dense_down_proj.T.reshape(quarters, part, head_size)
    parts = jnp.tile(jnp.concatenate((out_parts, down_parts), axis=1), (chips // quarters, 1, 1))
    received = exchanged(jnp.concatenate((token_pieces, parts), axis=1), Z)
    token_columns = received[:, :seq_count].reshape(chips, 2, half, slab)
    token_columns = token_columns.transpose(0, 2, 1, 3).reshape(chips * half, 2 * slab)
    quarter = received[:, seq_count:]
    both = in_order(
        quarter[:, None], lax.ppermute(quarter, "c", [(0, 1), (1, 0)])[:, None], core, 1
    )

    def whole(pieces):
        gathered = lax.all_gather(pieces, "zl", axis=0, tiled=False)
        return gathered.transpose(1, 2, 0, 3, 4).reshape(width, head_size)

    shares = product(token_columns, pair_rows[:, :projection_width]).astype(jnp.bfloat16)
    shares = exchanged(shares.reshape(chips, half, projection_width), Z)
    output_columns = whole(both[:, :, :part])
    shares = shares.reshape(pairs, seq_count, projection_width)
    projected = jnp.sum(shares.astype(jnp.float32), axis=0).astype(jnp.bfloat16)
    projected = projected.reshape(seq_count, 3, 1, head_size)
    log_forget = jax.nn.log_sigmoid(product(normed, forget_weight) + forget_bias)
    attended = attend(
        projected[:, 0],
        projected[:, 1],
        projected[:, 2],
        cache_keys,
        cache_values,
        cache_gates,
        lengths,
        log_forget,
    ).reshape(seq_count, head_size)
    picks = expert_ids.reshape(-1)
    capacity = 4 * seq_count // devices
    slot_total = devices * capacity
    pick_onehot = (picks[:, None] == jnp.arange(devices, dtype=jnp.int32)[None, :]).astype(jnp.int32)
    earlier = jnp.cumsum(pick_onehot, axis=0) - pick_onehot
    slot_rank = jnp.sum(earlier * pick_onehot, axis=1)
    destination = (picks * capacity + slot_rank).reshape(seq_count, 2)
    slot_grid = jnp.arange(slot_total, dtype=jnp.int32)
    select_first = (destination[:, 0:1] == slot_grid[None, :]).astype(jnp.bfloat16)
    select_second = (destination[:, 1:2] == slot_grid[None, :]).astype(jnp.bfloat16)
    routes = group_prob[:, None] * pair_prob / jnp.sum(pair_prob, axis=1, keepdims=True)
    head_terms = product_transposed(attended, output_columns).astype(jnp.bfloat16)
    lane = lax.axis_index("x")
    share = width // lax.axis_size("x")
    head_terms, selectors, routes, lane, share_start = lax.optimization_barrier(
        (head_terms, (select_first, select_second), routes, lane, lane * share)
    )
    select_first, select_second = selectors
    residual = (tokens.astype(jnp.float32) + summed_over_heads(head_terms)).astype(jnp.bfloat16)
    ffn_in = rms_scale(residual, ffn_gain).astype(jnp.bfloat16)
    mix = jax.nn.sigmoid(product(ffn_in, dense_mix))

    lanes = lax.axis_size("x")
    ffn_share = lax.dynamic_slice_in_dim(
        ffn_in, share_start, share, axis=1, allow_negative_indices=False
    )
    outbound = jnp.einsum(
        "sk,sd->kd", select_first + select_second, ffn_share, preferred_element_type=jnp.float32
    )
    outbound = outbound.astype(jnp.bfloat16).reshape(devices, capacity, share)
    few = seq_count // 4
    dense_pieces = ffn_in.reshape(4, few, pairs, 2, slab)
    dense_pieces = lax.dynamic_index_in_dim(
        dense_pieces, lane, axis=1, keepdims=False, allow_negative_indices=False
    )
    dense_pieces = dense_pieces.transpose(1, 0, 2, 3).reshape(devices, 2, slab)
    arrived = exchanged(jnp.concatenate((outbound, dense_pieces), axis=2), EP)
    arrived = from_all(arrived, "x")
    row_data = jnp.concatenate(
        [arrived[k, :, :, :share].reshape(slot_total, share) for k in range(lanes)], axis=1
    )
    dense_rows = arrived[:, :, :, share:].transpose(1, 0, 2, 3).reshape(devices * few, 2 * slab)

    dense_shares = product(dense_rows, pair_rows[:, projection_width:]).astype(jnp.bfloat16)
    dense_width = dense_shares.shape[1]
    dense_shares = dense_shares.reshape(devices, capacity, few // capacity * dense_width)
    gate_part = product(row_data, expert_gate[0])
    up_part = product(row_data, expert_up[0])
    expert_hidden = (jax.nn.silu(gate_part) * up_part).astype(jnp.bfloat16)
    partial_out = product(expert_hidden, expert_down[0]).astype(jnp.bfloat16)
    back = exchanged(
        jnp.concatenate((partial_out.reshape(devices, capacity, width), dense_shares), axis=2),
        EP,
    )
    down_columns = whole(both[:, :, part:])
    returned = back[:, :, :width].reshape(slot_total, width)
    dense_parts = back[:, :, width:].reshape(pairs, seq_count, dense_width)
    dense_parts = jnp.sum(dense_parts.astype(jnp.float32), axis=0)
    dense_hidden = jax.nn.silu(dense_parts[:, :head_size]) * dense_parts[:, head_size:]
    dense_terms = product_transposed(dense_hidden.astype(jnp.bfloat16), down_columns)
    side_total = (
        routes[:, 0:1] * product(select_first, returned)
        + routes[:, 1:2] * product(select_second, returned)
        + mix[:, None] * dense_terms
    )
    result = residual.astype(jnp.float32) + summed_over_heads(side_total.astype(jnp.bfloat16))
    return result.astype(jnp.bfloat16)


def solution(mesh):
    chips = mesh.shape["ep"] // 2
    finer = Mesh(mesh.devices.reshape(chips // 4, 4, 2, 4, 4), ("zh", "zl", "c", "y", "x"))
    in_specs = (
        P(EP, None),
        P(),
        P(EP, TP),
        P(EP, TP),
        P(EP, TP),
        P(None, TP),
        P(TP),
        P(EP, TP, None, None),
        P(EP, TP, None, None),
        P(EP, TP, None),
        P(EP),
        P(TP, EP),
        P(),
        P(EP, TP),
        P(EP, TP),
        P(TP, EP),
        P(),
        P(EP, None),
        P(EP),
        P(EP, None),
        P(EP, None, TP),
        P(EP, None, TP),
        P(EP, TP, None),
    )
    out_specs = P(EP, None)
    return jax.shard_map(layer, mesh=finer, in_specs=in_specs, out_specs=out_specs, check_vma=False)
```

profile of v0, /device:TPU:128, one launch (start us, length us, event | category | flops | bytes accessed | tf_op | source)
XLA Modules:
  0.0 183.6 jit_solution(11927274937198588561)
XLA Ops:
  0.1 1.1 fusion.21
  1.2 0.9 fusion.23
  2.2 0.7 pad_maximum_fusion.3
  2.9 0.7 pad_maximum_fusion.1
  3.6 13.8 %all-to-all-start = ((bf16[16,48,128]{2,1,0:T(8,128)(2,1)}), bf16[16,48,128]{2,1,0:T(8,128)(2,1)S(1)}, u32[]{:S(2)}, u32[]{:S(2)}) async-start(bf16[16,48,128]{2,1,0:T(8,128)(2,1)} %pad_maximum_fusion.1), calls=%async_computation | async-start | bytes 393216 | tf_op jit(solution)/shard_map/all_to_all | solution.py:17
  17.5 0.7 constant_dynamic-update-slice_fusion.4
  18.2 0.7 constant_dynamic-update-slice_fusion.3
  18.9 0.7 constant_dynamic-update-slice_fusion.2
  19.7 1.9 %collective-permute-start = (bf16[64,640]{1,0:T(8,128)(2,1)S(1)}, bf16[64,640]{1,0:T(8,128)(2,1)S(1)}, u32[]{:S(2)}, u32[]{:S(2)}) collective-permute-start(bf16[64,640]{1,0:T(8,128)(2,1)S(1)} %constant_dynamic-update-slice_fusion), channel_id=1, source_target_pairs={{0,16},{16,0},{1,17},{17,1},{2,18},{18,2},{3,19},{19,3},{4,20},{20... | collective-permute-start | bytes 245768 | tf_op jit(solution)/shard_map/ppermute | solution.py:125
  23.6 3.4 %collective-permute-start.1 = (bf16[128,640]{1,0:T(8,128)(2,1)S(1)}, bf16[128,640]{1,0:T(8,128)(2,1)S(1)}, u32[]{:S(2)}, u32[]{:S(2)}) collective-permute-start(bf16[128,640]{1,0:T(8,128)(2,1)S(1)} %maximum_select_fusion.2), channel_id=1, source_target_pairs={{0,32},{32,0},{64,96},{96,64},{1,33},{33,1},{65,97},{97,65},{2,34}... | collective-permute-start | bytes 491528 | tf_op jit(solution)/shard_map/ppermute | solution.py:127
  27.0 4.1 %all-to-all-done = bf16[16,48,128]{2,1,0:T(8,128)(2,1)S(1)} async-done(((bf16[16,48,128]{2,1,0:T(8,128)(2,1)}), bf16[16,48,128]{2,1,0:T(8,128)(2,1)S(1)}, u32[]{:S(2)}, u32[]{:S(2)}) %all-to-all-start) | async-done | bytes 196640 | tf_op jit(solution)/shard_map/all_to_all | solution.py:17
  31.1 1.9 %collective-permute-start.2 = (bf16[16,32,128]{2,1,0:T(8,128)(2,1)S(1)}, bf16[16,32,128]{2,1,0:T(8,128)(2,1)S(1)}, u32[]{:S(2)}, u32[]{:S(2)}) collective-permute-start(bf16[16,32,128]{2,1,0:T(8,128)(2,1)S(1)} %get-tuple-element.28), channel_id=1, source_target_pairs={{0,16},{16,0},{1,17},{17,1},{2,18},{18,2},{3,19},{19,3},{4,20},{20... | collective-permute-start | bytes 393224 | tf_op jit(solution)/shard_map/ppermute | solution.py:143
  33.2 0.8 fusion.7
  34.0 11.0 %all-to-all-start.1 = ((bf16[16,8,384]{2,1,0:T(8,128)(2,1)}), bf16[16,8,384]{2,1,0:T(8,128)(2,1)S(1)}, u32[]{:S(2)}, u32[]{:S(2)}) async-start(bf16[16,8,384]{2,1,0:T(8,128)(2,1)} %fusion.7), calls=%async_computation.1 | async-start | bytes 196608 | tf_op jit(solution)/shard_map/all_to_all | solution.py:17
  45.1 19.1 %all-gather = bf16[64,2,16,128]{3,2,1,0:T(8,128)(2,1)S(1)} all-gather(bf16[16,2,16,128]{3,2,1,0:T(8,128)(2,1)S(1)} %get-tuple-element.26), channel_id=2, replica_groups=mesh['zh'=4,'zl'=4,'c'=2,'y'=4,'x'=4] {'zl'}, dimensions={0}, use_global_device_ids=true | all-gather | bytes 655360 | tf_op jit(solution)/shard_map/all_gather | solution.py:147
  66.7 10.8 %all_to_all.45 = bf16[4,16,2048]{2,1,0:T(8,128)(2,1)S(1)} all-to-all(bf16[4,16,2048]{2,1,0:T(8,128)(2,1)S(1)} %broadcast_in_dim.25), channel_id=1, replica_groups=mesh['zh'=4,'zl'=4,'c'=2,'y'=4,'x'=4] {'x'}, dimensions={0} | all-to-all | bytes 524288 | tf_op jit(solution)/shard_map/all_to_all | solution.py:17
  77.5 10.9 %all_to_all.46 = bf16[4,16,2048]{2,1,0:T(8,128)(2,1)S(1)} all-to-all(bf16[4,16,2048]{2,1,0:T(8,128)(2,1)S(1)} %broadcast_in_dim.26), channel_id=1, replica_groups=mesh['zh'=4,'zl'=4,'c'=2,'y'=4,'x'=4] {'y'}, dimensions={0} | all-to-all | bytes 524288 | tf_op jit(solution)/shard_map/all_to_all | solution.py:17
  89.2 18.2 %all_to_all.47 = bf16[32,2,640]{2,1,0:T(2,128)(2,1)S(1)} all-to-all(bf16[32,2,640]{2,1,0:T(2,128)(2,1)S(1)} %pad_maximum_fusion.2), channel_id=1, replica_groups=mesh['zh'=4,'zl'=4,'c'=2,'y'=4,'x'=4] {'zh','zl','c'}, dimensions={0} | all-to-all | bytes 163840 | tf_op jit(solution)/shard_map/all_to_all | solution.py:17
  107.6 10.4 %all_to_all.48 = bf16[4,32,2,640]{3,2,1,0:T(2,128)(2,1)S(1)} all-to-all(bf16[4,32,2,640]{3,2,1,0:T(2,128)(2,1)S(1)} %broadcast_in_dim.27), channel_id=1, replica_groups=mesh['zh'=4,'zl'=4,'c'=2,'y'=4,'x'=4] {'x'}, dimensions={0} | all-to-all | bytes 655360 | tf_op jit(solution)/shard_map/all_to_all | solution.py:17
  118.1 0.8 convolution_convert_fusion.4
  118.9 0.9 reshape.296
  119.7 0.8 fusion.66
  120.6 0.9 reshape_squeeze.13
  121.5 0.9 reshape_squeeze.14
  122.4 0.9 reshape_squeeze.15
  123.3 1.3 fusion.18
  125.2 1.0 pad_maximum_fusion
  126.2 8.3 %all-to-all-start.6 = ((bf16[32,2,2560]{2,1,0:T(2,128)(2,1)}), bf16[32,2,2560]{2,1,0:T(2,128)(2,1)S(1)}, u32[]{:S(2)}, u32[]{:S(2)}) async-start(bf16[32,2,2560]{2,1,0:T(2,128)(2,1)} %pad_maximum_fusion), calls=%async_computation.6 | async-start | bytes 655360 | tf_op jit(solution)/shard_map/all_to_all | solution.py:17
  134.6 28.8 %all-gather.1 = bf16[64,2,16,128]{3,2,1,0:T(8,128)(2,1)S(1)} all-gather(bf16[16,2,16,128]{3,2,1,0:T(8,128)(2,1)S(1)} %get-tuple-element.25), channel_id=3, replica_groups=mesh['zh'=4,'zl'=4,'c'=2,'y'=4,'x'=4] {'zl'}, dimensions={0}, use_global_device_ids=true | all-gather | bytes 655360 | tf_op jit(solution)/shard_map/all_gather | solution.py:147
  164.7 9.1 %all_to_all.49 = bf16[4,16,2048]{2,1,0:T(8,128)(2,1)S(1)} all-to-all(bf16[4,16,2048]{2,1,0:T(8,128)(2,1)S(1)} %broadcast_in_dim.28), channel_id=1, replica_groups=mesh['zh'=4,'zl'=4,'c'=2,'y'=4,'x'=4] {'x'}, dimensions={0} | all-to-all | bytes 524288 | tf_op jit(solution)/shard_map/all_to_all | solution.py:17
  173.9 9.1 %all_to_all.50 = bf16[4,16,2048]{2,1,0:T(8,128)(2,1)S(1)} all-to-all(bf16[4,16,2048]{2,1,0:T(8,128)(2,1)S(1)} %broadcast_in_dim.29), channel_id=1, replica_groups=mesh['zh'=4,'zl'=4,'c'=2,'y'=4,'x'=4] {'y'}, dimensions={0} | all-to-all | bytes 524288 | tf_op jit(solution)/shard_map/all_to_all | solution.py:17
  183.0 0.6 fusion.28
  (115 shorter events, 7.1 us)
Async XLA Ops:
  0.0 64.5 %copy-start = (bf16[16,1,384,128]{3,2,1,0:T(8,128)(2,1)S(1)}, bf16[16,1,384,128]{3,2,1,0:T(8,128)(2,1)}, u32[]{:S(2)}) copy-start(bf16[16,1,384,128]{3,2,1,0:T(8,128)(2,1)} %param.30) | copy-start | bytes 4718596
  0.0 19.6 %copy-start.5 = (bf16[64,128]{1,0:T(8,128)(2,1)S(1)}, bf16[64,128]{1,0:T(8,128)(2,1)}, u32[]{:S(2)}) copy-start(bf16[64,128]{1,0:T(8,128)(2,1)} %param.36) | copy-start | bytes 49156
  0.0 19.6 %copy-start.6 = (bf16[64,128]{1,0:T(8,128)(2,1)S(1)}, bf16[64,128]{1,0:T(8,128)(2,1)}, u32[]{:S(2)}) copy-start(bf16[64,128]{1,0:T(8,128)(2,1)} %param.37) | copy-start | bytes 49156
  0.0 21.6 %copy-start.9 = (s32[16,2]{0,1:T(2,128)S(1)}, s32[16,2]{0,1:T(2,128)}, u32[]{:S(2)}) copy-start(s32[16,2]{0,1:T(2,128)} %param.40) | copy-start | bytes 388
  0.0 22.3 %copy-start.11 = (s32[16]{0:T(128)S(1)}, s32[16]{0:T(128)}, u32[]{:S(2)}) copy-start(s32[16]{0:T(128)} %param.33) | copy-start | bytes 196
  0.0 23.0 %copy-start.10 = (f32[16,2]{0,1:T(2,128)S(1)}, f32[16,2]{0,1:T(2,128)}, u32[]{:S(2)}) copy-start(f32[16,2]{0,1:T(2,128)} %param.42) | copy-start | bytes 388
  0.0 23.0 %copy-start.4 = (f32[16,1,384]{2,1,0:T(1,128)S(1)}, f32[16,1,384]{2,1,0:T(1,128)}, u32[]{:S(2)}) copy-start(f32[16,1,384]{2,1,0:T(1,128)} %param.32) | copy-start | bytes 73732
  0.1 23.3 %copy-start.14 = (bf16[2048,1]{0,1:T(2,128)(2,1)S(1)}, bf16[2048,1]{0,1:T(2,128)(2,1)}, u32[]{:S(2)}) copy-start(bf16[2048,1]{0,1:T(2,128)(2,1)} %param.28) | copy-start | bytes 12292
  0.1 23.5 %copy-start.12 = (f32[16]{0:T(128)S(1)}, f32[16]{0:T(128)}, u32[]{:S(2)}) copy-start(f32[16]{0:T(128)} %param.41) | copy-start | bytes 196
  3.6 27.5 %all-to-all-start = ((bf16[16,48,128]{2,1,0:T(8,128)(2,1)}), bf16[16,48,128]{2,1,0:T(8,128)(2,1)S(1)}, u32[]{:S(2)}, u32[]{:S(2)}) async-start(bf16[16,48,128]{2,1,0:T(8,128)(2,1)} %pad_maximum_fusion.1), calls=%async_computation | async-start | bytes 393216 | tf_op jit(solution)/shard_map/all_to_all | solution.py:17
  19.7 3.9 %collective-permute-start = (bf16[64,640]{1,0:T(8,128)(2,1)S(1)}, bf16[64,640]{1,0:T(8,128)(2,1)S(1)}, u32[]{:S(2)}, u32[]{:S(2)}) collective-permute-start(bf16[64,640]{1,0:T(8,128)(2,1)S(1)} %constant_dynamic-update-slice_fusion), channel_id=1, source_target_pairs={{0,16},{16,0},{1,17},{17,1},{2,18},{18,2},{3,19},{19,3},{4,20},{20... | collective-permute-start | bytes 245768 | tf_op jit(solution)/shard_map/ppermute | solution.py:125
  23.6 9.5 %collective-permute-start.1 = (bf16[128,640]{1,0:T(8,128)(2,1)S(1)}, bf16[128,640]{1,0:T(8,128)(2,1)S(1)}, u32[]{:S(2)}, u32[]{:S(2)}) collective-permute-start(bf16[128,640]{1,0:T(8,128)(2,1)S(1)} %maximum_select_fusion.2), channel_id=1, source_target_pairs={{0,32},{32,0},{64,96},{96,64},{1,33},{33,1},{65,97},{97,65},{2,34}... | collective-permute-start | bytes 491528 | tf_op jit(solution)/shard_map/ppermute | solution.py:127
  31.1 13.9 %collective-permute-start.2 = (bf16[16,32,128]{2,1,0:T(8,128)(2,1)S(1)}, bf16[16,32,128]{2,1,0:T(8,128)(2,1)S(1)}, u32[]{:S(2)}, u32[]{:S(2)}) collective-permute-start(bf16[16,32,128]{2,1,0:T(8,128)(2,1)S(1)} %get-tuple-element.28), channel_id=1, source_target_pairs={{0,16},{16,0},{1,17},{17,1},{2,18},{18,2},{3,19},{19,3},{4,20},{20... | collective-permute-start | bytes 393224 | tf_op jit(solution)/shard_map/ppermute | solution.py:143
  34.0 30.2 %all-to-all-start.1 = ((bf16[16,8,384]{2,1,0:T(8,128)(2,1)}), bf16[16,8,384]{2,1,0:T(8,128)(2,1)S(1)}, u32[]{:S(2)}, u32[]{:S(2)}) async-start(bf16[16,8,384]{2,1,0:T(8,128)(2,1)} %fusion.7), calls=%async_computation.1 | async-start | bytes 196608 | tf_op jit(solution)/shard_map/all_to_all | solution.py:17
  64.3 1.6 copy-start.13
  66.3 22.2 %copy-start.1 = (bf16[16,2048]{1,0:T(8,128)(2,1)S(1)}, bf16[16,2048]{1,0:T(8,128)(2,1)}, u32[]{:S(2)}) copy-start(bf16[16,2048]{1,0:T(8,128)(2,1)} %param.23) | copy-start | bytes 196612
  66.3 22.3 %copy-start.7 = (f32[2048]{0:T(1024)S(1)}, f32[2048]{0:T(1024)}, u32[]{:S(2)}) copy-start(f32[2048]{0:T(1024)} %param.35) | copy-start | bytes 24580
  117.9 6.6 %copy-start.2 = (bf16[1,128,2048]{2,1,0:T(8,128)(2,1)S(1)}, bf16[1,128,2048]{2,1,0:T(8,128)(2,1)}, u32[]{:S(2)}) copy-start(bf16[1,128,2048]{2,1,0:T(8,128)(2,1)} %param.45) | copy-start | bytes 1572868
  117.9 6.6 %copy-start.3 = (bf16[1,2048,128]{2,1,0:T(8,128)(2,1)S(1)}, bf16[1,2048,128]{2,1,0:T(8,128)(2,1)}, u32[]{:S(2)}) copy-start(bf16[1,2048,128]{2,1,0:T(8,128)(2,1)} %param.44) | copy-start | bytes 1572868
  124.6 10.0 %copy-start.8 = (bf16[2048]{0:T(1024)(128)(2,1)S(1)}, bf16[2048]{0:T(1024)(128)(2,1)}, u32[]{:S(2)}) copy-start(bf16[2048]{0:T(1024)(128)(2,1)} %param.39) | copy-start | bytes 12292
  126.2 37.4 %all-to-all-start.6 = ((bf16[32,2,2560]{2,1,0:T(2,128)(2,1)}), bf16[32,2,2560]{2,1,0:T(2,128)(2,1)S(1)}, u32[]{:S(2)}, u32[]{:S(2)}) async-start(bf16[32,2,2560]{2,1,0:T(2,128)(2,1)} %pad_maximum_fusion), calls=%async_computation.6 | async-start | bytes 655360 | tf_op jit(solution)/shard_map/all_to_all | solution.py:17
where the time goes:
time: 185 us; the launch traced here: 184 us
  blocking collectives  116 us (63%)
  starting transfers between devices  40.4 us (22%)
  local copies, waits for them, and re-layouts  8.33 us (5%)
  other arithmetic  7.42 us (4%)
  matrix products  5.68 us (3%)
  waiting for transfers between devices  4.19 us (2%)
    all_to_all x6, blocking collectives, exchanged(): return lax.all_to_all(pieces, axes, split_axis=0, concat_axis=0, tiled=True)  68.4 us
    all_gather x2, blocking collectives, whole(): gathered = lax.all_gather(pieces, 'zl', axis=0, tiled=False)  47.9 us
    all_to_all x3, starting transfers between devices, exchanged(): return lax.all_to_all(pieces, axes, split_axis=0, concat_axis=0, tiled=True)  33.2 us
    all_to_all x3, waiting for transfers between devices, exchanged(): return lax.all_to_all(pieces, axes, split_axis=0, concat_axis=0, tiled=True)  4.09 us
    dot_general x8, matrix products, product(): return jnp.dot(left, right, preferred_element_type=jnp.float32)  3.87 us
  transfers between devices with their start and end apart: 6, of which 2 were waited for; matrix products, arithmetic and copies ran while one was open for 3% of the time, Pallas kernels for 0%

commit v1 on v0

--- a/solution.py
+++ b/solution.py
@@ -3,6 +3,8 @@
 import jax
 import jax.numpy as jnp
 from jax import lax
+from jax.experimental import pallas as pl
+from jax.experimental.pallas import tpu as pltpu
 from jax.sharding import Mesh
 from jax.sharding import PartitionSpec as P
 
@@ -51,6 +53,83 @@
         * lax.rsqrt(jnp.mean(widened * widened, axis=-1, keepdims=True) + EPSILON)
         * norm_gain
     )
+
+
+def first_payload(tokens_ref, gain_ref, out_ref, down_ref, payload_ref, normed_ref):
+    seq_count, _ = tokens_ref.shape
+    chips, _, slab = payload_ref.shape
+    half = seq_count // 2
+    held = out_ref.shape[0]
+    widened = tokens_ref[...].astype(jnp.float32)
+    mean = jnp.mean(widened * widened, axis=-1, keepdims=True)
+    normed = (widened * lax.rsqrt(mean + EPSILON) * gain_ref[...]).astype(jnp.bfloat16)
+    normed_ref[...] = normed
+    for chip in range(chips):
+        pair, side = divmod(chip, 2)
+        for k in range(2):
+            first = (2 * pair + k) * slab
+            payload_ref[chip, k * half : (k + 1) * half, :] = normed[
+                side * half : (side + 1) * half, first : first + slab
+            ]
+        row = seq_count
+        payload_ref[chip, row : row + held // 2, :] = out_ref[
+            side * (held // 2) : (side + 1) * (held // 2), :
+        ]
+        row += held // 2
+        quarter = chip % 4
+        payload_ref[chip, row : row + held // 4, :] = down_ref[
+            quarter * (held // 4) : (quarter + 1) * (held // 4), :
+        ]
+
+
+def experts(
+    rows_ref, dense_ref, gate_hbm, up_hbm, down_hbm, payload_ref,
+    gate_ref, up_ref, down_ref, low_ref, high_ref, mixed_ref, sems,
+):
+    lanes, slots, _ = rows_ref.shape
+    width, hidden_width = gate_ref.shape
+    share = width // lanes
+    slab = dense_ref.shape[0] // 2
+    dense_width = hidden_width * 2
+    first = dense_ref.shape[1] - dense_width
+    copies = [
+        pltpu.make_async_copy(source, target, sems.at[k])
+        for k, (source, target) in enumerate(
+            ((gate_hbm, gate_ref), (up_hbm, up_ref), (down_hbm, down_ref))
+        )
+    ]
+    for copy in copies:
+        copy.start()
+    for lane in range(lanes):
+        pieces = rows_ref[lane, :, share : share + slab]
+        low = jnp.dot(pieces, dense_ref[:slab, first:], preferred_element_type=jnp.float32)
+        high = jnp.dot(pieces, dense_ref[slab:, first:], preferred_element_type=jnp.float32)
+        row, place = divmod(lane, 2)
+        for part in range(2):
+            span = slice(part * hidden_width, (part + 1) * hidden_width)
+            low_ref[part] = low[:, span]
+            high_ref[part] = high[:, span]
+            mixed_ref[2 * place + part, pl.ds(row, slots // 2, stride=2), :] = (
+                low_ref[part, pl.ds(0, slots // 2, stride=2), :]
+                + high_ref[part, pl.ds(1, slots // 2, stride=2), :]
+            )
+    for part in range(mixed_ref.shape[0]):
+        span = slice(width + part * hidden_width, width + (part + 1) * hidden_width)
+        payload_ref[:, span] = mixed_ref[part].astype(jnp.bfloat16)
+    copies[0].wait()
+    copies[1].wait()
+    gate_part = jnp.zeros((slots, hidden_width), jnp.float32)
+    up_part = jnp.zeros((slots, hidden_width), jnp.float32)
+    for lane in range(lanes):
+        rows = rows_ref[lane, :, :share]
+        span = slice(lane * share, (lane + 1) * share)
+        gate_part += jnp.dot(rows, gate_ref[span, :], preferred_element_type=jnp.float32)
+        up_part += jnp.dot(rows, up_ref[span, :], preferred_element_type=jnp.float32)
+    hidden = (gate_part / (1.0 + jnp.exp(-gate_part)) * up_part).astype(jnp.bfloat16)
+    copies[2].wait()
+    payload_ref[:, :width] = jnp.dot(
+        hidden, down_ref[...], preferred_element_type=jnp.float32
+    ).astype(jnp.bfloat16)
 
 
 def attend(queries, keys_new, values_new, key_cache, value_cache, gate_cache, lengths, log_forget):
@@ -127,29 +206,34 @@
     pair_rows = in_order(chip_rows, lax.ppermute(chip_rows, "zl", neighbours), side, 0)
     projection_width = 3 * head_size
 
-    normed = rms_scale(tokens, attn_gain).astype(jnp.bfloat16)
-    token_pieces = normed.reshape(2, half, pairs, 2, slab).transpose(2, 0, 3, 1, 4)
-    token_pieces = token_pieces.reshape(chips, seq_count, slab)
     held = output_weight.shape[1]
     part = held // quarters
-    out_parts = output_weight.T.reshape(quarters, part, head_size)
-    down_parts = dense_down_proj.T.reshape(quarters, part, head_size)
-    parts = jnp.tile(jnp.concatenate((out_parts, down_parts), axis=1), (chips // quarters, 1, 1))
-    received = exchanged(jnp.concatenate((token_pieces, parts), axis=1), Z)
+    vmem = pl.BlockSpec(memory_space=pltpu.VMEM)
+    payload, normed = pl.pallas_call(
+        first_payload,
+        out_shape=(
+            jax.ShapeDtypeStruct((chips, seq_count + held // 2 + part, slab), jnp.bfloat16),
+            jax.ShapeDtypeStruct((seq_count, width), jnp.bfloat16),
+        ),
+        in_specs=(vmem,) * 4,
+        out_specs=(vmem,) * 2,
+        name="first_payload",
+    )(tokens, attn_gain[None], output_weight.T, dense_down_proj.T)
+    received = exchanged(payload, Z)
     token_columns = received[:, :seq_count].reshape(chips, 2, half, slab)
     token_columns = token_columns.transpose(0, 2, 1, 3).reshape(chips * half, 2 * slab)
-    quarter = received[:, seq_count:]
-    both = in_order(
-        quarter[:, None], lax.ppermute(quarter, "c", [(0, 1), (1, 0)])[:, None], core, 1
-    )
-
-    def whole(pieces):
-        gathered = lax.all_gather(pieces, "zl", axis=0, tiled=False)
-        return gathered.transpose(1, 2, 0, 3, 4).reshape(width, head_size)
+    out_half = received[:, seq_count : seq_count + held // 2]
+    down_quarter = received[:, seq_count + held // 2 :]
+    swap = [(0, 1), (1, 0)]
+
+    out_held = in_order(
+        out_half[:, None], lax.ppermute(out_half, "zl", neighbours)[:, None], side, 1
+    )
+    out_all = in_order(out_held[:, None], lax.ppermute(out_held, "c", swap)[:, None], core, 1)
+    output_columns = out_all.reshape(width, head_size)
 
     shares = product(token_columns, pair_rows[:, :projection_width]).astype(jnp.bfloat16)
     shares = exchanged(shares.reshape(chips, half, projection_width), Z)
-    output_columns = whole(both[:, :, :part])
     shares = shares.reshape(pairs, seq_count, projection_width)
     projected = jnp.sum(shares.astype(jnp.float32), axis=0).astype(jnp.bfloat16)
     projected = projected.reshape(seq_count, 3, 1, head_size)
@@ -202,23 +286,35 @@
     dense_pieces = dense_pieces.transpose(1, 0, 2, 3).reshape(devices, 2, slab)
     arrived = exchanged(jnp.concatenate((outbound, dense_pieces), axis=2), EP)
     arrived = from_all(arrived, "x")
-    row_data = jnp.concatenate(
-        [arrived[k, :, :, :share].reshape(slot_total, share) for k in range(lanes)], axis=1
-    )
-    dense_rows = arrived[:, :, :, share:].transpose(1, 0, 2, 3).reshape(devices * few, 2 * slab)
-
-    dense_shares = product(dense_rows, pair_rows[:, projection_width:]).astype(jnp.bfloat16)
-    dense_width = dense_shares.shape[1]
-    dense_shares = dense_shares.reshape(devices, capacity, few // capacity * dense_width)
-    gate_part = product(row_data, expert_gate[0])
-    up_part = product(row_data, expert_up[0])
-    expert_hidden = (jax.nn.silu(gate_part) * up_part).astype(jnp.bfloat16)
-    partial_out = product(expert_hidden, expert_down[0]).astype(jnp.bfloat16)
-    back = exchanged(
-        jnp.concatenate((partial_out.reshape(devices, capacity, width), dense_shares), axis=2),
-        EP,
-    )
-    down_columns = whole(both[:, :, part:])
+    dense_width = 2 * head_size
+    payload_width = width + few // capacity * dense_width
+    hbm = pl.BlockSpec(memory_space=pl.ANY)
+    payload = pl.pallas_call(
+        experts,
+        out_shape=jax.ShapeDtypeStruct((slot_total, payload_width), jnp.bfloat16),
+        in_specs=(vmem, vmem, hbm, hbm, hbm),
+        out_specs=vmem,
+        scratch_shapes=(
+            pltpu.VMEM(expert_gate.shape[1:], jnp.bfloat16),
+            pltpu.VMEM(expert_up.shape[1:], jnp.bfloat16),
+            pltpu.VMEM(expert_down.shape[1:], jnp.bfloat16),
+            pltpu.VMEM((2, slot_total, head_size), jnp.float32),
+            pltpu.VMEM((2, slot_total, head_size), jnp.float32),
+            pltpu.VMEM(((payload_width - width) // head_size, slot_total, head_size), jnp.float32),
+            pltpu.SemaphoreType.DMA((3,)),
+        ),
+        name="experts",
+    )(
+        arrived.reshape(lanes, slot_total, share + slab),
+        pair_rows,
+        expert_gate[0],
+        expert_up[0],
+        expert_down[0],
+    )
+    back = exchanged(payload.reshape(devices, capacity, payload_width), EP)
+    down_held = lax.all_gather(down_quarter, "zl", axis=1, tiled=False)
+    down_all = in_order(down_held[:, None], lax.ppermute(down_held, "c", swap)[:, None], core, 1)
+    down_columns = down_all.reshape(width, head_size)
     returned = back[:, :, :width].reshape(slot_total, width)
     dense_parts = back[:, :, width:].reshape(pairs, seq_count, dense_width)
     dense_parts = jnp.sum(dense_parts.astype(jnp.float32), axis=0)

time: 185 us -> 179 us (0.968)
  the two profiles are of different devices: /device:TPU:128 before, /device:TPU:1 now
where the time goes in v1:
time: 179 us; the launch traced here: 178 us
  blocking collectives  89.3 us (50%)
  starting transfers between devices  50.2 us (28%)
  waiting for transfers between devices  13.9 us (8%)
  local copies, waits for them, and re-layouts  8.3 us (5%)
  other arithmetic  5.88 us (3%)
  Pallas kernels  5.39 us (3%)
  matrix products  4.06 us (2%)
    all_to_all x6, blocking collectives, exchanged(): return lax.all_to_all(pieces, axes, split_axis=0, concat_axis=0, tiled=True)  66.5 us
    all_to_all x3, starting transfers between devices, exchanged(): return lax.all_to_all(pieces, axes, split_axis=0, concat_axis=0, tiled=True)  32.4 us
    all_gather x1, blocking collectives, layer(): down_held = lax.all_gather(down_quarter, 'zl', axis=1, tiled=False)  22.9 us
    all_to_all x3, waiting for transfers between devices, exchanged(): return lax.all_to_all(pieces, axes, split_axis=0, concat_axis=0, tiled=True)  8.38 us
    ppermute x1, starting transfers between devices, layer(): lax.ppermute(down_held, 'c', swap)[:, None]  4.72 us
    ppermute x1, waiting for transfers between devices, layer(): lax.ppermute(chip_rows, 'zl', neighbours)  4.38 us
    unnamed x26, local copies, waits for them, and re-layouts  3.71 us
  transfers between devices with their start and end apart: 8, of which 3 were waited for; matrix products, arithmetic and copies ran while one was open for 7% of the time, Pallas kernels for 0%

profile of v1, /device:TPU:1, one launch (start us, length us, event | category | flops | bytes accessed | tf_op | source)
XLA Modules:
  0.0 178.2 jit_solution(9902292523806004820)
XLA Ops:
  0.0 1.8 %first_payload.1 = (bf16[16,64,128]{2,1,0:T(8,128)(2,1)}, bf16[16,2048]{1,0:T(8,128)(2,1)}) custom-call(bf16[16,2048]{1,0:T(8,128)(2,1)} %tokens_ref.1, f32[1,2048]{1,0:T(1,128)} %bitcast.114, bf16[64,128]{1,0:T(8,128)(2,1)} %bitcast.111, bf16[64,128]{1,0:T(8,128)(2,1)} %bitcast.112), custom_call_target="tpu_custom_call" | custom-call | tf_op jit(solution)/shard_map/first_payload/pallas_call | solution.py:212
  1.8 15.7 %all-to-all-start = ((bf16[16,64,128]{2,1,0:T(8,128)(2,1)}), bf16[16,64,128]{2,1,0:T(8,128)(2,1)S(1)}, u32[]{:S(2)}, u32[]{:S(2)}) async-start(bf16[16,64,128]{2,1,0:T(8,128)(2,1)} %get-tuple-element.13), calls=%async_computation | async-start | bytes 524288 | tf_op jit(solution)/shard_map/all_to_all | solution.py:19
  17.6 0.7 constant_dynamic-update-slice_fusion.4
  18.3 0.7 constant_dynamic-update-slice_fusion.3
  19.0 0.7 constant_dynamic-update-slice_fusion.2
  19.7 0.7 constant_dynamic-update-slice_fusion.1
  20.5 0.7 constant_dynamic-update-slice_fusion
  21.2 2.9 %collective-permute-start = (bf16[64,640]{1,0:T(8,128)(2,1)S(1)}, bf16[64,640]{1,0:T(8,128)(2,1)S(1)}, u32[]{:S(2)}, u32[]{:S(2)}) collective-permute-start(bf16[64,640]{1,0:T(8,128)(2,1)S(1)} %constant_dynamic-update-slice_fusion), channel_id=1, source_target_pairs={{0,16},{16,0},{1,17},{17,1},{2,18},{18,2},{3,19},{19,3},{4,20},{20... | collective-permute-start | bytes 245768 | tf_op jit(solution)/shard_map/ppermute | solution.py:204
  25.4 0.8 copy.52
  27.4 1.0 fusion.23
  28.4 1.0 fusion.39
  29.4 0.7 reduce_sum.125
  30.2 3.6 %collective-permute-start.1 = (bf16[128,640]{1,0:T(8,128)(2,1)S(1)}, bf16[128,640]{1,0:T(8,128)(2,1)S(1)}, u32[]{:S(2)}, u32[]{:S(2)}) collective-permute-start(bf16[128,640]{1,0:T(8,128)(2,1)S(1)} %maximum_select_fusion.5), channel_id=1, source_target_pairs={{0,32},{32,0},{64,96},{96,64},{1,33},{33,1},{65,97},{97,65},{2,34}... | collective-permute-start | bytes 491528 | tf_op jit(solution)/shard_map/ppermute | solution.py:206
  33.8 4.4 %collective-permute-done.1 = bf16[128,640]{1,0:T(8,128)(2,1)S(1)} collective-permute-done((bf16[128,640]{1,0:T(8,128)(2,1)S(1)}, bf16[128,640]{1,0:T(8,128)(2,1)S(1)}, u32[]{:S(2)}, u32[]{:S(2)}) %collective-permute-start.1) | collective-permute-done | bytes 163872 | tf_op jit(solution)/shard_map/ppermute | solution.py:206
  38.4 3.3 %collective-permute-start.2 = (bf16[16,32,128]{2,1,0:T(8,128)(2,1)S(1)}, bf16[16,32,128]{2,1,0:T(8,128)(2,1)S(1)}, u32[]{:S(2)}, u32[]{:S(2)}) collective-permute-start(bf16[16,32,128]{2,1,0:T(8,128)(2,1)S(1)} %get-tuple-element.27), channel_id=1, source_target_pairs={{0,32},{32,0},{64,96},{96,64},{1,33},{33,1},{65,97},{97,65},{2,34}... | collective-permute-start | bytes 393224 | tf_op jit(solution)/shard_map/ppermute | solution.py:230
  41.6 0.8 fusion.7
  42.5 10.4 %all-to-all-start.1 = ((bf16[16,8,384]{2,1,0:T(8,128)(2,1)}), bf16[16,8,384]{2,1,0:T(8,128)(2,1)S(1)}, u32[]{:S(2)}, u32[]{:S(2)}) async-start(bf16[16,8,384]{2,1,0:T(8,128)(2,1)} %fusion.7), calls=%async_computation.1 | async-start | bytes 196608 | tf_op jit(solution)/shard_map/all_to_all | solution.py:19
  53.0 3.3 %collective-permute-start.3 = (bf16[16,2,32,128]{3,2,0,1:T(8,128)(2,1)S(1)}, bf16[16,2,32,128]{3,2,0,1:T(8,128)(2,1)S(1)}, u32[]{:S(2)}, u32[]{:S(2)}) collective-permute-start(bf16[16,2,32,128]{3,2,0,1:T(8,128)(2,1)S(1)} %maximum_select_fusion.4), channel_id=1, source_target_pairs={{0,16},{16,0},{1,17},{17,1},{2,18},{18,2},{3,19},{19,3},{4,20},{20... | collective-permute-start | bytes 786440 | tf_op jit(solution)/shard_map/ppermute | solution.py:232
  56.3 8.4 %all-to-all-done.1 = bf16[16,8,384]{2,1,0:T(8,128)(2,1)S(1)} async-done(((bf16[16,8,384]{2,1,0:T(8,128)(2,1)}), bf16[16,8,384]{2,1,0:T(8,128)(2,1)S(1)}, u32[]{:S(2)}, u32[]{:S(2)}) %all-to-all-start.1) | async-done | bytes 98336 | tf_op jit(solution)/shard_map/all_to_all | solution.py:19
  67.3 9.3 %all_to_all.45 = bf16[4,16,2048]{2,1,0:T(8,128)(2,1)S(1)} all-to-all(bf16[4,16,2048]{2,1,0:T(8,128)(2,1)S(1)} %broadcast_in_dim.66), channel_id=1, replica_groups=mesh['zh'=4,'zl'=4,'c'=2,'y'=4,'x'=4] {'x'}, dimensions={0} | all-to-all | bytes 524288 | tf_op jit(solution)/shard_map/all_to_all | solution.py:19
  76.7 9.5 %all_to_all.46 = bf16[4,16,2048]{2,1,0:T(8,128)(2,1)S(1)} all-to-all(bf16[4,16,2048]{2,1,0:T(8,128)(2,1)S(1)} %broadcast_in_dim.67), channel_id=1, replica_groups=mesh['zh'=4,'zl'=4,'c'=2,'y'=4,'x'=4] {'y'}, dimensions={0} | all-to-all | bytes 524288 | tf_op jit(solution)/shard_map/all_to_all | solution.py:19
  87.0 22.7 %all_to_all.47 = bf16[32,2,640]{2,1,0:T(2,128)(2,1)S(1)} all-to-all(bf16[32,2,640]{2,1,0:T(2,128)(2,1)S(1)} %pad_maximum_fusion), channel_id=1, replica_groups=mesh['zh'=4,'zl'=4,'c'=2,'y'=4,'x'=4] {'zh','zl','c'}, dimensions={0} | all-to-all | bytes 163840 | tf_op jit(solution)/shard_map/all_to_all | solution.py:19
  109.9 8.3 %all_to_all.48 = bf16[4,32,2,640]{3,2,1,0:T(2,128)(2,1)S(1)} all-to-all(bf16[4,32,2,640]{3,2,1,0:T(2,128)(2,1)S(1)} %broadcast_in_dim.68), channel_id=1, replica_groups=mesh['zh'=4,'zl'=4,'c'=2,'y'=4,'x'=4] {'x'}, dimensions={0} | all-to-all | bytes 655360 | tf_op jit(solution)/shard_map/all_to_all | solution.py:19
  118.1 0.9 reshape.327.rows_ref
  119.0 3.6 %experts.1 = bf16[64,2560]{1,0:T(8,128)(2,1)} custom-call(bf16[4,64,640]{2,1,0:T(8,128)(2,1)} %reshape.327.rows_ref, bf16[256,640]{1,0:T(8,128)(2,1)} %copy-done.1, bf16[2048,128]{1,0:T(8,128)(2,1)} %bitcast.100, bf16[2048,128]{1,0:T(8,128)(2,1)} %bitcast.101, bf16[128,2048]{1,0:T(8,128)(2,1)} %bitcast.102), custom_call_target="tpu_custom_call" | custom-call | tf_op jit(solution)/shard_map/experts/pallas_call | solution.py:292
  122.6 1.8 %reshape.328 = bf16[32,2,2560]{2,1,0:T(2,128)(2,1)} reshape(bf16[64,2560]{1,0:T(8,128)(2,1)} %experts.1) | data formatting | bytes 655360 | tf_op jit(solution)/shard_map/reshape | solution.py:314
  124.4 6.3 %all-to-all-start.6 = ((bf16[32,2,2560]{2,1,0:T(2,128)(2,1)}), bf16[32,2,2560]{2,1,0:T(2,128)(2,1)S(1)}, u32[]{:S(2)}, u32[]{:S(2)}) async-start(bf16[32,2,2560]{2,1,0:T(2,128)(2,1)} %reshape.328), calls=%async_computation.6 | async-start | bytes 655360 | tf_op jit(solution)/shard_map/all_to_all | solution.py:19
  130.7 22.9 %all-gather = bf16[16,64,128]{2,1,0:T(8,128)(2,1)S(1)} all-gather(bf16[16,16,128]{2,1,0:T(8,128)(2,1)S(1)} %slice.70), channel_id=2, replica_groups=mesh['zh'=4,'zl'=4,'c'=2,'y'=4,'x'=4] {'zl'}, dimensions={1}, use_global_device_ids=true | all-gather | bytes 327680 | tf_op jit(solution)/shard_map/all_gather | solution.py:315
  153.5 4.7 %collective-permute-start.4 = (bf16[16,4,16,128]{3,2,1,0:T(8,128)(2,1)S(1)}, bf16[16,4,16,128]{3,2,1,0:T(8,128)(2,1)S(1)}, u32[]{:S(2)}, u32[]{:S(2)}) collective-permute-start(bf16[16,4,16,128]{3,2,1,0:T(8,128)(2,1)S(1)} %bitcast.98), channel_id=1, source_target_pairs={{0,16},{16,0},{1,17},{17,1},{2,18},{18,2},{3,19},{19,3},{4,20},{20... | collective-permute-start | bytes 786440 | tf_op jit(solution)/shard_map/ppermute | solution.py:316
  158.3 1.1 collective-permute-done.4
  160.7 8.8 %all_to_all.49 = bf16[4,16,2048]{2,1,0:T(8,128)(2,1)S(1)} all-to-all(bf16[4,16,2048]{2,1,0:T(8,128)(2,1)S(1)} %broadcast_in_dim.71), channel_id=1, replica_groups=mesh['zh'=4,'zl'=4,'c'=2,'y'=4,'x'=4] {'x'}, dimensions={0} | all-to-all | bytes 524288 | tf_op jit(solution)/shard_map/all_to_all | solution.py:19
  169.6 7.9 %all_to_all.50 = bf16[4,16,2048]{2,1,0:T(8,128)(2,1)S(1)} all-to-all(bf16[4,16,2048]{2,1,0:T(8,128)(2,1)S(1)} %broadcast_in_dim.72), channel_id=1, replica_groups=mesh['zh'=4,'zl'=4,'c'=2,'y'=4,'x'=4] {'y'}, dimensions={0} | all-to-all | bytes 524288 | tf_op jit(solution)/shard_map/all_to_all | solution.py:19
  (89 shorter events, 7.7 us)
Async XLA Ops:
  0.0 65.0 %copy-start = (bf16[16,1,384,128]{3,2,1,0:T(8,128)(2,1)S(1)}, bf16[16,1,384,128]{3,2,1,0:T(8,128)(2,1)}, u32[]{:S(2)}) copy-start(bf16[16,1,384,128]{3,2,1,0:T(8,128)(2,1)} %param.30) | copy-start | bytes 4718596
  0.0 52.9 %copy-start.6 = (f32[16,2]{0,1:T(2,128)S(1)}, f32[16,2]{0,1:T(2,128)}, u32[]{:S(2)}) copy-start(f32[16,2]{0,1:T(2,128)} %param.42) | copy-start | bytes 388
  0.0 52.9 %copy-start.8 = (f32[16]{0:T(128)S(1)}, f32[16]{0:T(128)}, u32[]{:S(2)}) copy-start(f32[16]{0:T(128)} %param.41) | copy-start | bytes 196
  1.8 36.5 %all-to-all-start = ((bf16[16,64,128]{2,1,0:T(8,128)(2,1)}), bf16[16,64,128]{2,1,0:T(8,128)(2,1)S(1)}, u32[]{:S(2)}, u32[]{:S(2)}) async-start(bf16[16,64,128]{2,1,0:T(8,128)(2,1)} %get-tuple-element.13), calls=%async_computation | async-start | bytes 524288 | tf_op jit(solution)/shard_map/all_to_all | solution.py:19
  21.2 9.0 %collective-permute-start = (bf16[64,640]{1,0:T(8,128)(2,1)S(1)}, bf16[64,640]{1,0:T(8,128)(2,1)S(1)}, u32[]{:S(2)}, u32[]{:S(2)}) collective-permute-start(bf16[64,640]{1,0:T(8,128)(2,1)S(1)} %constant_dynamic-update-slice_fusion), channel_id=1, source_target_pairs={{0,16},{16,0},{1,17},{17,1},{2,18},{18,2},{3,19},{19,3},{4,20},{20... | collective-permute-start | bytes 245768 | tf_op jit(solution)/shard_map/ppermute | solution.py:204
  30.2 8.0 %collective-permute-start.1 = (bf16[128,640]{1,0:T(8,128)(2,1)S(1)}, bf16[128,640]{1,0:T(8,128)(2,1)S(1)}, u32[]{:S(2)}, u32[]{:S(2)}) collective-permute-start(bf16[128,640]{1,0:T(8,128)(2,1)S(1)} %maximum_select_fusion.5), channel_id=1, source_target_pairs={{0,32},{32,0},{64,96},{96,64},{1,33},{33,1},{65,97},{97,65},{2,34}... | collective-permute-start | bytes 491528 | tf_op jit(solution)/shard_map/ppermute | solution.py:206
  38.3 27.4 %copy-start.1 = (bf16[256,640]{1,0:T(8,128)(2,1)}, bf16[256,640]{1,0:T(8,128)(2,1)S(1)}, u32[]{:S(2)}) copy-start(bf16[256,640]{1,0:T(8,128)(2,1)S(1)} %maximum_select_fusion.2.dense_ref) | copy-start | bytes 983044
  38.4 14.6 %collective-permute-start.2 = (bf16[16,32,128]{2,1,0:T(8,128)(2,1)S(1)}, bf16[16,32,128]{2,1,0:T(8,128)(2,1)S(1)}, u32[]{:S(2)}, u32[]{:S(2)}) collective-permute-start(bf16[16,32,128]{2,1,0:T(8,128)(2,1)S(1)} %get-tuple-element.27), channel_id=1, source_target_pairs={{0,32},{32,0},{64,96},{96,64},{1,33},{33,1},{65,97},{97,65},{2,34}... | collective-permute-start | bytes 393224 | tf_op jit(solution)/shard_map/ppermute | solution.py:230
  42.5 23.3 %copy-start.3 = (f32[16,1,384]{2,1,0:T(1,128)S(1)}, f32[16,1,384]{2,1,0:T(1,128)}, u32[]{:S(2)}) copy-start(f32[16,1,384]{2,1,0:T(1,128)} %param.32) | copy-start | bytes 73732
  42.5 23.3 %copy-start.7 = (s32[16]{0:T(128)S(1)}, s32[16]{0:T(128)}, u32[]{:S(2)}) copy-start(s32[16]{0:T(128)} %param.33) | copy-start | bytes 196
  42.5 22.3 %all-to-all-start.1 = ((bf16[16,8,384]{2,1,0:T(8,128)(2,1)}), bf16[16,8,384]{2,1,0:T(8,128)(2,1)S(1)}, u32[]{:S(2)}, u32[]{:S(2)}) async-start(bf16[16,8,384]{2,1,0:T(8,128)(2,1)} %fusion.7), calls=%async_computation.1 | async-start | bytes 196608 | tf_op jit(solution)/shard_map/all_to_all | solution.py:19
  53.0 13.9 %collective-permute-start.3 = (bf16[16,2,32,128]{3,2,0,1:T(8,128)(2,1)S(1)}, bf16[16,2,32,128]{3,2,0,1:T(8,128)(2,1)S(1)}, u32[]{:S(2)}, u32[]{:S(2)}) collective-permute-start(bf16[16,2,32,128]{3,2,0,1:T(8,128)(2,1)S(1)} %maximum_select_fusion.4), channel_id=1, source_target_pairs={{0,16},{16,0},{1,17},{17,1},{2,18},{18,2},{3,19},{19,3},{4,20},{20... | collective-permute-start | bytes 786440 | tf_op jit(solution)/shard_map/ppermute | solution.py:232
  64.8 1.6 copy-start.9
  67.0 19.3 %copy-start.2 = (bf16[16,2048]{1,0:T(8,128)(2,1)S(1)}, bf16[16,2048]{1,0:T(8,128)(2,1)}, u32[]{:S(2)}) copy-start(bf16[16,2048]{1,0:T(8,128)(2,1)} %tokens_ref.1) | copy-start | bytes 196612
  67.0 19.5 %copy-start.4 = (f32[2048]{0:T(1024)S(1)}, f32[2048]{0:T(1024)}, u32[]{:S(2)}) copy-start(f32[2048]{0:T(1024)} %param.35) | copy-start | bytes 24580
  119.0 39.3 %copy-start.5 = (bf16[2048]{0:T(1024)(128)(2,1)S(1)}, bf16[2048]{0:T(1024)(128)(2,1)}, u32[]{:S(2)}) copy-start(bf16[2048]{0:T(1024)(128)(2,1)} %param.39) | copy-start | bytes 12292
  124.4 35.2 %all-to-all-start.6 = ((bf16[32,2,2560]{2,1,0:T(2,128)(2,1)}), bf16[32,2,2560]{2,1,0:T(2,128)(2,1)S(1)}, u32[]{:S(2)}, u32[]{:S(2)}) async-start(bf16[32,2,2560]{2,1,0:T(2,128)(2,1)} %reshape.328), calls=%async_computation.6 | async-start | bytes 655360 | tf_op jit(solution)/shard_map/all_to_all | solution.py:19
  153.5 5.9 %collective-permute-start.4 = (bf16[16,4,16,128]{3,2,1,0:T(8,128)(2,1)S(1)}, bf16[16,4,16,128]{3,2,1,0:T(8,128)(2,1)S(1)}, u32[]{:S(2)}, u32[]{:S(2)}) collective-permute-start(bf16[16,4,16,128]{3,2,1,0:T(8,128)(2,1)S(1)} %bitcast.98), channel_id=1, source_target_pairs={{0,16},{16,0},{1,17},{17,1},{2,18},{18,2},{3,19},{19,3},{4,20},{20... | collective-permute-start | bytes 786440 | tf_op jit(solution)/shard_map/ppermute | solution.py:316

commit v2 on v1

--- a/solution.py
+++ b/solution.py
@@ -55,11 +55,16 @@
     )
 
 
-def first_payload(tokens_ref, gain_ref, out_ref, down_ref, payload_ref, normed_ref):
+def first_payload(
+    tokens_ref, gain_ref, out_ref, down_ref, query_ref, key_ref, value_ref, gate_ref, up_ref,
+    payload_ref, normed_ref, rows_ref,
+):
     seq_count, _ = tokens_ref.shape
     chips, _, slab = payload_ref.shape
     half = seq_count // 2
-    held = out_ref.shape[0]
+    held = out_ref.shape[0] // 2
+    for k, weight_ref in enumerate((query_ref, key_ref, value_ref, gate_ref, up_ref)):
+        rows_ref[:, k * slab : (k + 1) * slab] = weight_ref[...]
     widened = tokens_ref[...].astype(jnp.float32)
     mean = jnp.mean(widened * widened, axis=-1, keepdims=True)
     normed = (widened * lax.rsqrt(mean + EPSILON) * gain_ref[...]).astype(jnp.bfloat16)
@@ -71,15 +76,9 @@
             payload_ref[chip, k * half : (k + 1) * half, :] = normed[
                 side * half : (side + 1) * half, first : first + slab
             ]
-        row = seq_count
-        payload_ref[chip, row : row + held // 2, :] = out_ref[
-            side * (held // 2) : (side + 1) * (held // 2), :
-        ]
-        row += held // 2
-        quarter = chip % 4
-        payload_ref[chip, row : row + held // 4, :] = down_ref[
-            quarter * (held // 4) : (quarter + 1) * (held // 4), :
-        ]
+        columns = slice(side * held, (side + 1) * held)
+        payload_ref[chip, seq_count : seq_count + held, :] = out_ref[columns, :]
+        payload_ref[chip, seq_count + held :, :] = down_ref[columns, :]
 
 
 def experts(
@@ -198,39 +197,46 @@
     pairs = chips // 2
     half = seq_count // 2
 
-    own_rows = jnp.concatenate(
-        (query_weight, key_weight, value_weight, dense_gate_proj, dense_up_proj), axis=1
-    )
-    chip_rows = in_order(own_rows, lax.ppermute(own_rows, "c", [(0, 1), (1, 0)]), core, 0)
+    held = output_weight.shape[1] // 2
+    vmem = pl.BlockSpec(memory_space=pltpu.VMEM)
+    payload, normed, own_rows = pl.pallas_call(
+        first_payload,
+        out_shape=(
+            jax.ShapeDtypeStruct((chips, seq_count + 2 * held, slab), jnp.bfloat16),
+            jax.ShapeDtypeStruct((seq_count, width), jnp.bfloat16),
+            jax.ShapeDtypeStruct((query_weight.shape[0], 5 * slab), jnp.bfloat16),
+        ),
+        in_specs=(vmem,) * 9,
+        out_specs=(vmem,) * 3,
+        name="first_payload",
+    )(
+        tokens,
+        attn_gain[None],
+        output_weight.T,
+        dense_down_proj.T,
+        query_weight,
+        key_weight,
+        value_weight,
+        dense_gate_proj,
+        dense_up_proj,
+    )
+    received = exchanged(payload, Z)
+
+    swap = [(0, 1), (1, 0)]
     neighbours = [(k, k ^ 1) for k in range(quarters)]
+    their_rows = lax.ppermute(own_rows, "c", swap)
+    chip_rows = in_order(own_rows, their_rows, core, 0)
     pair_rows = in_order(chip_rows, lax.ppermute(chip_rows, "zl", neighbours), side, 0)
     projection_width = 3 * head_size
-
-    held = output_weight.shape[1]
-    part = held // quarters
-    vmem = pl.BlockSpec(memory_space=pltpu.VMEM)
-    payload, normed = pl.pallas_call(
-        first_payload,
-        out_shape=(
-            jax.ShapeDtypeStruct((chips, seq_count + held // 2 + part, slab), jnp.bfloat16),
-            jax.ShapeDtypeStruct((seq_count, width), jnp.bfloat16),
-        ),
-        in_specs=(vmem,) * 4,
-        out_specs=(vmem,) * 2,
-        name="first_payload",
-    )(tokens, attn_gain[None], output_weight.T, dense_down_proj.T)
-    received = exchanged(payload, Z)
     token_columns = received[:, :seq_count].reshape(chips, 2, half, slab)
     token_columns = token_columns.transpose(0, 2, 1, 3).reshape(chips * half, 2 * slab)
-    out_half = received[:, seq_count : seq_count + held // 2]
-    down_quarter = received[:, seq_count + held // 2 :]
-    swap = [(0, 1), (1, 0)]
-
-    out_held = in_order(
-        out_half[:, None], lax.ppermute(out_half, "zl", neighbours)[:, None], side, 1
-    )
-    out_all = in_order(out_held[:, None], lax.ppermute(out_held, "c", swap)[:, None], core, 1)
-    output_columns = out_all.reshape(width, head_size)
+
+    halves = received[:, seq_count:].reshape(chips, 2, 1, held, slab)
+    other_halves = lax.ppermute(halves, "zl", neighbours)
+    both = in_order(halves, other_halves, side, 2)
+    columns = in_order(both[:, None], lax.ppermute(both, "c", swap)[:, None], core, 1)
+    output_columns = columns[:, :, 0].reshape(width, head_size)
+    down_columns = columns[:, :, 1].reshape(width, head_size)
 
     shares = product(token_columns, pair_rows[:, :projection_width]).astype(jnp.bfloat16)
     shares = exchanged(shares.reshape(chips, half, projection_width), Z)
@@ -262,13 +268,20 @@
     head_terms = product_transposed(attended, output_columns).astype(jnp.bfloat16)
     lane = lax.axis_index("x")
     share = width // lax.axis_size("x")
-    head_terms, selectors, routes, lane, share_start = lax.optimization_barrier(
-        (head_terms, (select_first, select_second), routes, lane, lane * share)
+    head_terms, selectors, routes, lane, share_start, mix_row = lax.optimization_barrier(
+        (
+            head_terms,
+            (select_first, select_second),
+            (routes[:, 0], routes[:, 1]),
+            lane,
+            lane * share,
+            dense_mix.astype(jnp.float32),
+        )
     )
     select_first, select_second = selectors
     residual = (tokens.astype(jnp.float32) + summed_over_heads(head_terms)).astype(jnp.bfloat16)
     ffn_in = rms_scale(residual, ffn_gain).astype(jnp.bfloat16)
-    mix = jax.nn.sigmoid(product(ffn_in, dense_mix))
+    mix = jax.nn.sigmoid(jnp.sum(ffn_in.astype(jnp.float32) * mix_row, axis=-1))
 
     lanes = lax.axis_size("x")
     ffn_share = lax.dynamic_slice_in_dim(
@@ -284,7 +297,10 @@
         dense_pieces, lane, axis=1, keepdims=False, allow_negative_indices=False
     )
     dense_pieces = dense_pieces.transpose(1, 0, 2, 3).reshape(devices, 2, slab)
-    arrived = exchanged(jnp.concatenate((outbound, dense_pieces), axis=2), EP)
+    outbound, mix = lax.optimization_barrier(
+        (jnp.concatenate((outbound, dense_pieces), axis=2), mix)
+    )
+    arrived = exchanged(outbound, EP)
     arrived = from_all(arrived, "x")
     dense_width = 2 * head_size
     payload_width = width + few // capacity * dense_width
@@ -312,17 +328,14 @@
         expert_down[0],
     )
     back = exchanged(payload.reshape(devices, capacity, payload_width), EP)
-    down_held = lax.all_gather(down_quarter, "zl", axis=1, tiled=False)
-    down_all = in_order(down_held[:, None], lax.ppermute(down_held, "c", swap)[:, None], core, 1)
-    down_columns = down_all.reshape(width, head_size)
     returned = back[:, :, :width].reshape(slot_total, width)
     dense_parts = back[:, :, width:].reshape(pairs, seq_count, dense_width)
     dense_parts = jnp.sum(dense_parts.astype(jnp.float32), axis=0)
     dense_hidden = jax.nn.silu(dense_parts[:, :head_size]) * dense_parts[:, head_size:]
     dense_terms = product_transposed(dense_hidden.astype(jnp.bfloat16), down_columns)
     side_total = (
-        routes[:, 0:1] * product(select_first, returned)
-        + routes[:, 1:2] * product(select_second, returned)
+        routes[0][:, None] * product(select_first, returned)
+        + routes[1][:, None] * product(select_second, returned)
         + mix[:, None] * dense_terms
     )
     result = residual.astype(jnp.float32) + summed_over_heads(side_total.astype(jnp.bfloat16))

time: 179 us -> 173 us (0.966)
  starting transfers between devices: 50.2 us -> 39 us
  blocking collectives: 89.3 us -> 96 us
  local copies, waits for them, and re-layouts: 8.3 us -> 3.93 us
  other arithmetic: 5.88 us -> 8.81 us
    all_to_all x6 -> x7, blocking collectives: 66.5 us -> 96 us  [exchanged(): return lax.all_to_all(pieces, axes, split_axis=0, concat_axis=0, tiled=True)]
    all_gather x1 -> x0, blocking collectives: 22.9 us -> none  [layer(): down_held = lax.all_gather(down_quarter, 'zl', axis=1, tiled=False)]
    all_to_all x3 -> x2, starting transfers between devices: 32.4 us -> 16.8 us  [exchanged(): return lax.all_to_all(pieces, axes, split_axis=0, concat_axis=0, tiled=True)]
    ppermute x4 -> x3, starting transfers between devices: 14.2 us -> 18.9 us  [the longest x1 8.73 us: layer(): their_rows = lax.ppermute(own_rows, 'c', swap)]
    ppermute x1, waiting for transfers between devices: 4.38 us -> 0.01 us  [layer(): lax.ppermute(chip_rows, 'zl', neighbours)]
    all_to_all x3 -> x2, waiting for transfers between devices: 8.38 us -> 12.6 us  [exchanged(): return lax.all_to_all(pieces, axes, split_axis=0, concat_axis=0, tiled=True)]
    unnamed x26 -> x17, local copies, waits for them, and re-layouts: 3.71 us -> 0.8 us
    select_n x6 -> x5, other arithmetic: 0.3 us -> 2.2 us  [in_order(): jnp.where(place == 0, jnp.concatenate((own, theirs), axis=dim), jnp.conca...]
  transfers between devices with their start and end apart: 8 -> 6, of which waited for: 3 -> 2; matrix products, arithmetic and copies ran while one was open for 7% -> 7% of each run, Pallas kernels for 0% -> 0%
where the time goes in v2:
time: 173 us; the launch traced here: 171 us
  blocking collectives  96 us (55%)
  starting transfers between devices  39 us (23%)
  waiting for transfers between devices  12.6 us (7%)
  other arithmetic  8.81 us (5%)
  Pallas kernels  5.49 us (3%)
  local copies, waits for them, and re-layouts  3.93 us (2%)
  matrix products  3.9 us (2%)
    all_to_all x7, blocking collectives, exchanged(): return lax.all_to_all(pieces, axes, split_axis=0, concat_axis=0, tiled=True)  96 us
    all_to_all x2, starting transfers between devices, exchanged(): return lax.all_to_all(pieces, axes, split_axis=0, concat_axis=0, tiled=True)  16.8 us
    all_to_all x2, waiting for transfers between devices, exchanged(): return lax.all_to_all(pieces, axes, split_axis=0, concat_axis=0, tiled=True)  12.6 us
    ppermute x1, starting transfers between devices, layer(): their_rows = lax.ppermute(own_rows, 'c', swap)  8.73 us
    ppermute x1, starting transfers between devices, layer(): other_halves = lax.ppermute(halves, 'zl', neighbours)  7.52 us
    pallas_call x1, Pallas kernels, layer(): pl.pallas_call(experts, out_shape=jax.ShapeDtypeStruct((slot_total, paylo...  3.57 us
  transfers between devices with their start and end apart: 6, of which 2 were waited for; matrix products, arithmetic and copies ran while one was open for 7% of the time, Pallas kernels for 0%

profile of v2, /device:TPU:1, one launch (start us, length us, event | category | flops | bytes accessed | tf_op | source)
XLA Modules:
  0.0 170.8 jit_solution(18088003451810678697)
XLA Ops:
  0.0 1.9 %first_payload.1 = (bf16[16,80,128]{2,1,0:T(8,128)(2,1)}, bf16[16,2048]{1,0:T(8,128)(2,1)}, bf16[64,640]{1,0:T(8,128)(2,1)}) custom-call(bf16[16,2048]{1,0:T(8,128)(2,1)} %tokens_ref.1, f32[1,2048]{1,0:T(1,128)} %bitcast.92, bf16[64,128]{1,0:T(8,128)(2,1)} %bitcast.89, bf16[64,128]{1,0:T(8,128)(2,1)} %bitcast.90, bf16[64,128]{1,0:T(8,128)(2,1)} %query_ref.1, ...), custom_call_target="tpu_custom_call" | custom-call | tf_op jit(solution)/shard_map/first_payload/pallas_call | solution.py:202
  1.9 8.7 %collective-permute-start = (bf16[64,640]{1,0:T(8,128)(2,1)}, bf16[64,640]{1,0:T(8,128)(2,1)S(1)}, u32[]{:S(2)}, u32[]{:S(2)}) collective-permute-start(bf16[64,640]{1,0:T(8,128)(2,1)} %get-tuple-element.19), channel_id=1, source_target_pairs={{0,16},{16,0},{1,17},{17,1},{2,18},{18,2},{3,19},{19,3},{4,20},{20... | collective-permute-start | bytes 245768 | tf_op jit(solution)/shard_map/ppermute | solution.py:227
  10.7 9.6 %all-to-all-start = ((bf16[16,80,128]{2,1,0:T(8,128)(2,1)}), bf16[16,80,128]{2,1,0:T(8,128)(2,1)S(1)}, u32[]{:S(2)}, u32[]{:S(2)}) async-start(bf16[16,80,128]{2,1,0:T(8,128)(2,1)} %get-tuple-element.18), calls=%async_computation | async-start | bytes 655360 | tf_op jit(solution)/shard_map/all_to_all | solution.py:19
  20.3 0.7 broadcast_add_fusion
  21.6 0.8 copy.70
  22.9 1.0 fusion.19
  23.9 0.7 reduce_sum.134
  24.6 0.7 multiply_add_fusion
  25.4 1.0 fusion.35
  26.4 0.7 multiply_divide_fusion
  27.1 1.0 maximum_select_fusion.3
  28.1 3.3 %collective-permute-start.1 = (bf16[128,640]{1,0:T(8,128)(2,1)S(1)}, bf16[128,640]{1,0:T(8,128)(2,1)S(1)}, u32[]{:S(2)}, u32[]{:S(2)}) collective-permute-start(bf16[128,640]{1,0:T(8,128)(2,1)S(1)} %maximum_select_fusion.3), channel_id=1, source_target_pairs={{0,32},{32,0},{64,96},{96,64},{1,33},{33,1},{65,97},{97,65},{2,34}... | collective-permute-start | bytes 491528 | tf_op jit(solution)/shard_map/ppermute | solution.py:229
  31.4 4.7 %all-to-all-done = bf16[16,80,128]{2,1,0:T(8,128)(2,1)S(1)} async-done(((bf16[16,80,128]{2,1,0:T(8,128)(2,1)}), bf16[16,80,128]{2,1,0:T(8,128)(2,1)S(1)}, u32[]{:S(2)}, u32[]{:S(2)}) %all-to-all-start) | async-done | bytes 327712 | tf_op jit(solution)/shard_map/all_to_all | solution.py:19
  36.1 7.5 %collective-permute-start.2 = (bf16[16,2,1,32,128]{4,3,2,0,1:T(8,128)(2,1)S(1)}, bf16[16,2,1,32,128]{4,3,2,0,1:T(8,128)(2,1)S(1)}, u32[]{:S(2)}, u32[]{:S(2)}) collective-permute-start(bf16[16,2,1,32,128]{4,3,2,0,1:T(8,128)(2,1)S(1)} %copy.63), channel_id=1, source_target_pairs={{0,32},{32,0},{64,96},{96,64},{1,33},{33,1},{65,97},{97,65},{2,34}... | collective-permute-start | bytes 786440 | tf_op jit(solution)/shard_map/ppermute | solution.py:235
  43.8 0.8 fusion.7
  44.6 7.2 %all-to-all-start.1 = ((bf16[16,8,384]{2,1,0:T(8,128)(2,1)}), bf16[16,8,384]{2,1,0:T(8,128)(2,1)S(1)}, u32[]{:S(2)}, u32[]{:S(2)}) async-start(bf16[16,8,384]{2,1,0:T(8,128)(2,1)} %fusion.7), calls=%async_computation.1 | async-start | bytes 196608 | tf_op jit(solution)/shard_map/all_to_all | solution.py:19
  51.8 1.0 maximum_select_fusion.1
  52.8 2.7 %collective-permute-start.3 = (bf16[16,2,2,32,128]{4,3,2,0,1:T(8,128)(2,1)}, bf16[16,2,2,32,128]{4,3,2,0,1:T(8,128)(2,1)S(1)}, u32[]{:S(2)}, u32[]{:S(2)}) collective-permute-start(bf16[16,2,2,32,128]{4,3,2,0,1:T(8,128)(2,1)} %maximum_select_fusion.1), channel_id=1, source_target_pairs={{0,16},{16,0},{1,17},{17,1},{2,18},{18,2},{3,19},{19,3},{4,20},{20... | collective-permute-start | bytes 1572872 | tf_op jit(solution)/shard_map/ppermute | solution.py:237
  55.7 7.9 %all-to-all-done.1 = bf16[16,8,384]{2,1,0:T(8,128)(2,1)S(1)} async-done(((bf16[16,8,384]{2,1,0:T(8,128)(2,1)}), bf16[16,8,384]{2,1,0:T(8,128)(2,1)S(1)}, u32[]{:S(2)}, u32[]{:S(2)}) %all-to-all-start.1) | async-done | bytes 98336 | tf_op jit(solution)/shard_map/all_to_all | solution.py:19
  63.9 0.6 fusion.5
  65.3 0.4 fusion.3
  66.3 9.3 %all_to_all.45 = bf16[4,16,2048]{2,1,0:T(8,128)(2,1)S(1)} all-to-all(bf16[4,16,2048]{2,1,0:T(8,128)(2,1)S(1)} %broadcast_in_dim.25), channel_id=1, replica_groups=mesh['zh'=4,'zl'=4,'c'=2,'y'=4,'x'=4] {'x'}, dimensions={0} | all-to-all | bytes 524288 | tf_op jit(solution)/shard_map/all_to_all | solution.py:19
  75.7 9.5 %all_to_all.46 = bf16[4,16,2048]{2,1,0:T(8,128)(2,1)S(1)} all-to-all(bf16[4,16,2048]{2,1,0:T(8,128)(2,1)S(1)} %broadcast_in_dim.26), channel_id=1, replica_groups=mesh['zh'=4,'zl'=4,'c'=2,'y'=4,'x'=4] {'y'}, dimensions={0} | all-to-all | bytes 524288 | tf_op jit(solution)/shard_map/all_to_all | solution.py:19
  86.2 22.6 %all_to_all.47 = bf16[32,2,640]{2,1,0:T(2,128)(2,1)S(1)} all-to-all(bf16[32,2,640]{2,1,0:T(2,128)(2,1)S(1)} %pad_maximum_fusion.2), channel_id=1, replica_groups=mesh['zh'=4,'zl'=4,'c'=2,'y'=4,'x'=4] {'zh','zl','c'}, dimensions={0} | all-to-all | bytes 163840 | tf_op jit(solution)/shard_map/all_to_all | solution.py:19
  109.0 8.3 %all_to_all.48 = bf16[4,32,2,640]{3,2,1,0:T(2,128)(2,1)S(1)} all-to-all(bf16[4,32,2,640]{3,2,1,0:T(2,128)(2,1)S(1)} %broadcast_in_dim.27), channel_id=1, replica_groups=mesh['zh'=4,'zl'=4,'c'=2,'y'=4,'x'=4] {'x'}, dimensions={0} | all-to-all | bytes 655360 | tf_op jit(solution)/shard_map/all_to_all | solution.py:19
  117.2 0.8 reshape.319.rows_ref
  118.1 3.6 %experts.1 = bf16[64,2560]{1,0:T(8,128)(2,1)} custom-call(bf16[4,64,640]{2,1,0:T(8,128)(2,1)} %reshape.319.rows_ref, bf16[256,640]{1,0:T(8,128)(2,1)} %copy-done.1, bf16[2048,128]{1,0:T(8,128)(2,1)} %bitcast.81, bf16[2048,128]{1,0:T(8,128)(2,1)} %bitcast.82, bf16[128,2048]{1,0:T(8,128)(2,1)} %bitcast.83), custom_call_target="tpu_custom_call" | custom-call | tf_op jit(solution)/shard_map/experts/pallas_call | solution.py:308
  121.6 1.1 reshape.320
  122.7 30.4 %all_to_all.49 = bf16[32,2,2560]{2,1,0:T(2,128)(2,1)S(1)} all-to-all(bf16[32,2,2560]{2,1,0:T(2,128)(2,1)S(1)} %reshape.320), channel_id=1, replica_groups=mesh['zh'=4,'zl'=4,'c'=2,'y'=4,'x'=4] {'zh','zl','c'}, dimensions={0} | all-to-all | bytes 655360 | tf_op jit(solution)/shard_map/all_to_all | solution.py:19
  154.2 7.9 %all_to_all.50 = bf16[4,16,2048]{2,1,0:T(8,128)(2,1)S(1)} all-to-all(bf16[4,16,2048]{2,1,0:T(8,128)(2,1)S(1)} %broadcast_in_dim.28), channel_id=1, replica_groups=mesh['zh'=4,'zl'=4,'c'=2,'y'=4,'x'=4] {'x'}, dimensions={0} | all-to-all | bytes 524288 | tf_op jit(solution)/shard_map/all_to_all | solution.py:19
  162.2 7.9 %all_to_all.51 = bf16[4,16,2048]{2,1,0:T(8,128)(2,1)S(1)} all-to-all(bf16[4,16,2048]{2,1,0:T(8,128)(2,1)S(1)} %broadcast_in_dim.29), channel_id=1, replica_groups=mesh['zh'=4,'zl'=4,'c'=2,'y'=4,'x'=4] {'y'}, dimensions={0} | all-to-all | bytes 524288 | tf_op jit(solution)/shard_map/all_to_all | solution.py:19
  170.2 0.6 fusion.14
  (76 shorter events, 4.7 us)
Async XLA Ops:
  0.0 63.9 %copy-start = (bf16[16,1,384,128]{3,2,1,0:T(8,128)(2,1)S(1)}, bf16[16,1,384,128]{3,2,1,0:T(8,128)(2,1)}, u32[]{:S(2)}) copy-start(bf16[16,1,384,128]{3,2,1,0:T(8,128)(2,1)} %param.30) | copy-start | bytes 4718596
  0.0 43.7 %copy-start.5 = (bf16[2048]{0:T(1024)(128)(2,1)S(1)}, bf16[2048]{0:T(1024)(128)(2,1)}, u32[]{:S(2)}) copy-start(bf16[2048]{0:T(1024)(128)(2,1)} %param.39) | copy-start | bytes 12292
  1.9 25.2 %collective-permute-start = (bf16[64,640]{1,0:T(8,128)(2,1)}, bf16[64,640]{1,0:T(8,128)(2,1)S(1)}, u32[]{:S(2)}, u32[]{:S(2)}) collective-permute-start(bf16[64,640]{1,0:T(8,128)(2,1)} %get-tuple-element.19), channel_id=1, source_target_pairs={{0,16},{16,0},{1,17},{17,1},{2,18},{18,2},{3,19},{19,3},{4,20},{20... | collective-permute-start | bytes 245768 | tf_op jit(solution)/shard_map/ppermute | solution.py:227
  10.7 25.4 %all-to-all-start = ((bf16[16,80,128]{2,1,0:T(8,128)(2,1)}), bf16[16,80,128]{2,1,0:T(8,128)(2,1)S(1)}, u32[]{:S(2)}, u32[]{:S(2)}) async-start(bf16[16,80,128]{2,1,0:T(8,128)(2,1)} %get-tuple-element.18), calls=%async_computation | async-start | bytes 655360 | tf_op jit(solution)/shard_map/all_to_all | solution.py:19
  28.1 15.6 %collective-permute-start.1 = (bf16[128,640]{1,0:T(8,128)(2,1)S(1)}, bf16[128,640]{1,0:T(8,128)(2,1)S(1)}, u32[]{:S(2)}, u32[]{:S(2)}) collective-permute-start(bf16[128,640]{1,0:T(8,128)(2,1)S(1)} %maximum_select_fusion.3), channel_id=1, source_target_pairs={{0,32},{32,0},{64,96},{96,64},{1,33},{33,1},{65,97},{97,65},{2,34}... | collective-permute-start | bytes 491528 | tf_op jit(solution)/shard_map/ppermute | solution.py:229
  36.1 15.7 %collective-permute-start.2 = (bf16[16,2,1,32,128]{4,3,2,0,1:T(8,128)(2,1)S(1)}, bf16[16,2,1,32,128]{4,3,2,0,1:T(8,128)(2,1)S(1)}, u32[]{:S(2)}, u32[]{:S(2)}) collective-permute-start(bf16[16,2,1,32,128]{4,3,2,0,1:T(8,128)(2,1)S(1)} %copy.63), channel_id=1, source_target_pairs={{0,32},{32,0},{64,96},{96,64},{1,33},{33,1},{65,97},{97,65},{2,34}... | collective-permute-start | bytes 786440 | tf_op jit(solution)/shard_map/ppermute | solution.py:235
  43.8 11.9 %copy-start.1 = (bf16[256,640]{1,0:T(8,128)(2,1)}, bf16[256,640]{1,0:T(8,128)(2,1)S(1)}, u32[]{:S(2)}) copy-start(bf16[256,640]{1,0:T(8,128)(2,1)S(1)} %maximum_select_fusion.2.dense_ref) | copy-start | bytes 983044
  44.6 19.1 %all-to-all-start.1 = ((bf16[16,8,384]{2,1,0:T(8,128)(2,1)}), bf16[16,8,384]{2,1,0:T(8,128)(2,1)S(1)}, u32[]{:S(2)}, u32[]{:S(2)}) async-start(bf16[16,8,384]{2,1,0:T(8,128)(2,1)} %fusion.7), calls=%async_computation.1 | async-start | bytes 196608 | tf_op jit(solution)/shard_map/all_to_all | solution.py:19
  52.8 13.0 %collective-permute-start.3 = (bf16[16,2,2,32,128]{4,3,2,0,1:T(8,128)(2,1)}, bf16[16,2,2,32,128]{4,3,2,0,1:T(8,128)(2,1)S(1)}, u32[]{:S(2)}, u32[]{:S(2)}) collective-permute-start(bf16[16,2,2,32,128]{4,3,2,0,1:T(8,128)(2,1)} %maximum_select_fusion.1), channel_id=1, source_target_pairs={{0,16},{16,0},{1,17},{17,1},{2,18},{18,2},{3,19},{19,3},{4,20},{20... | collective-permute-start | bytes 1572872 | tf_op jit(solution)/shard_map/ppermute | solution.py:237
  55.7 9.0 %copy-start.3 = (f32[16,1,384]{2,1,0:T(1,128)S(1)}, f32[16,1,384]{2,1,0:T(1,128)}, u32[]{:S(2)}) copy-start(f32[16,1,384]{2,1,0:T(1,128)} %param.32) | copy-start | bytes 73732
  55.7 9.0 %copy-start.6 = (s32[16]{0:T(128)S(1)}, s32[16]{0:T(128)}, u32[]{:S(2)}) copy-start(s32[16]{0:T(128)} %param.33) | copy-start | bytes 196
  63.7 1.6 copy-start.7
  66.0 19.3 %copy-start.2 = (bf16[16,2048]{1,0:T(8,128)(2,1)S(1)}, bf16[16,2048]{1,0:T(8,128)(2,1)}, u32[]{:S(2)}) copy-start(bf16[16,2048]{1,0:T(8,128)(2,1)} %tokens_ref.1) | copy-start | bytes 196612
  66.0 19.5 %copy-start.4 = (f32[2048]{0:T(1024)S(1)}, f32[2048]{0:T(1024)}, u32[]{:S(2)}) copy-start(f32[2048]{0:T(1024)} %param.35) | copy-start | bytes 24580

commit v3 on v2

--- a/solution.py
+++ b/solution.py
@@ -57,38 +57,59 @@
 
 def first_payload(
     tokens_ref, gain_ref, out_ref, down_ref, query_ref, key_ref, value_ref, gate_ref, up_ref,
-    payload_ref, normed_ref, rows_ref,
+    forget_ref, bias_ref, ids_ref, pair_ref, group_ref,
+    payload_ref, logits_ref, rows_ref, first_ref, second_ref, routes_ref,
 ):
     seq_count, _ = tokens_ref.shape
     chips, _, slab = payload_ref.shape
-    half = seq_count // 2
     held = out_ref.shape[0] // 2
     for k, weight_ref in enumerate((query_ref, key_ref, value_ref, gate_ref, up_ref)):
         rows_ref[:, k * slab : (k + 1) * slab] = weight_ref[...]
     widened = tokens_ref[...].astype(jnp.float32)
     mean = jnp.mean(widened * widened, axis=-1, keepdims=True)
     normed = (widened * lax.rsqrt(mean + EPSILON) * gain_ref[...]).astype(jnp.bfloat16)
-    normed_ref[...] = normed
+    forget = normed.astype(jnp.float32) * forget_ref[...].astype(jnp.float32)
+    logits_ref[...] = jnp.sum(forget, axis=-1, keepdims=True) + bias_ref[...]
     for chip in range(chips):
-        pair, side = divmod(chip, 2)
-        for k in range(2):
-            first = (2 * pair + k) * slab
-            payload_ref[chip, k * half : (k + 1) * half, :] = normed[
-                side * half : (side + 1) * half, first : first + slab
-            ]
+        side = chip % 2
+        payload_ref[chip, :seq_count, :] = normed[:, chip * slab : (chip + 1) * slab]
         columns = slice(side * held, (side + 1) * held)
         payload_ref[chip, seq_count : seq_count + held, :] = out_ref[columns, :]
         payload_ref[chip, seq_count + held :, :] = down_ref[columns, :]
 
+    row = lax.broadcasted_iota(jnp.int32, (seq_count, seq_count), 0)
+    place = lax.broadcasted_iota(jnp.int32, (seq_count, seq_count), 1)
+
+    def column(values):
+        return jnp.sum(jnp.where(row == place, values, 0.0), axis=1, keepdims=True)
+
+    slot_total = first_ref.shape[1]
+    devices = 2 * chips
+    grid = lax.broadcasted_iota(jnp.int32, (seq_count, devices), 1).astype(jnp.float32)
+    slots = lax.broadcasted_iota(jnp.int32, (seq_count, slot_total), 1).astype(jnp.float32)
+    named = [column(ids_ref[k : k + 1, :].astype(jnp.float32)) for k in range(2)]
+    hot = [(expert == grid).astype(jnp.float32) for expert in named]
+    before = jnp.dot(
+        (place < row).astype(jnp.float32), hot[0] + hot[1], preferred_element_type=jnp.float32
+    )
+    for k, select_ref in enumerate((first_ref, second_ref)):
+        rank = jnp.sum(before * hot[k], axis=1, keepdims=True)
+        target = named[k] * (slot_total // devices) + rank
+        select_ref[...] = (target == slots).astype(jnp.float32).astype(jnp.bfloat16)
+    pair = [column(pair_ref[k : k + 1, :]) for k in range(2)]
+    group = column(group_ref[...])
+    for k in range(2):
+        routes_ref[k] = group * pair[k] / (pair[0] + pair[1])
+
 
 def experts(
     rows_ref, dense_ref, gate_hbm, up_hbm, down_hbm, payload_ref,
-    gate_ref, up_ref, down_ref, low_ref, high_ref, mixed_ref, sems,
+    gate_ref, up_ref, down_ref, sems,
 ):
     lanes, slots, _ = rows_ref.shape
     width, hidden_width = gate_ref.shape
     share = width // lanes
-    slab = dense_ref.shape[0] // 2
+    slab = dense_ref.shape[0]
     dense_width = hidden_width * 2
     first = dense_ref.shape[1] - dense_width
     copies = [
@@ -100,21 +121,12 @@
     for copy in copies:
         copy.start()
     for lane in range(lanes):
-        pieces = rows_ref[lane, :, share : share + slab]
-        low = jnp.dot(pieces, dense_ref[:slab, first:], preferred_element_type=jnp.float32)
-        high = jnp.dot(pieces, dense_ref[slab:, first:], preferred_element_type=jnp.float32)
-        row, place = divmod(lane, 2)
-        for part in range(2):
-            span = slice(part * hidden_width, (part + 1) * hidden_width)
-            low_ref[part] = low[:, span]
-            high_ref[part] = high[:, span]
-            mixed_ref[2 * place + part, pl.ds(row, slots // 2, stride=2), :] = (
-                low_ref[part, pl.ds(0, slots // 2, stride=2), :]
-                + high_ref[part, pl.ds(1, slots // 2, stride=2), :]
-            )
-    for part in range(mixed_ref.shape[0]):
-        span = slice(width + part * hidden_width, width + (part + 1) * hidden_width)
-        payload_ref[:, span] = mixed_ref[part].astype(jnp.bfloat16)
+        start = width + lane * dense_width
+        payload_ref[:, start : start + dense_width] = jnp.dot(
+            rows_ref[lane, :, share : share + slab],
+            dense_ref[:, first:],
+            preferred_element_type=jnp.float32,
+        ).astype(jnp.bfloat16)
     copies[0].wait()
     copies[1].wait()
     gate_part = jnp.zeros((slots, hidden_width), jnp.float32)
@@ -194,20 +206,23 @@
     slab = width // chips
     core = lax.axis_index("c")
     side = lax.axis_index("zl") % 2
-    pairs = chips // 2
-    half = seq_count // 2
 
     held = output_weight.shape[1] // 2
     vmem = pl.BlockSpec(memory_space=pltpu.VMEM)
-    payload, normed, own_rows = pl.pallas_call(
+    capacity = 4 * seq_count // devices
+    slot_total = devices * capacity
+    payload, forget_logits, own_rows, *routing = pl.pallas_call(
         first_payload,
         out_shape=(
-            jax.ShapeDtypeStruct((chips, seq_count + 2 * held, slab), jnp.bfloat16),
-            jax.ShapeDtypeStruct((seq_count, width), jnp.bfloat16),
+            pltpu.VMEM((chips, seq_count + 2 * held, slab), jnp.bfloat16),
+            jax.ShapeDtypeStruct((seq_count, 1), jnp.float32),
             jax.ShapeDtypeStruct((query_weight.shape[0], 5 * slab), jnp.bfloat16),
+            jax.ShapeDtypeStruct((seq_count, slot_total), jnp.bfloat16),
+            jax.ShapeDtypeStruct((seq_count, slot_total), jnp.bfloat16),
+            jax.ShapeDtypeStruct((2, seq_count, 1), jnp.float32),
         ),
-        in_specs=(vmem,) * 9,
-        out_specs=(vmem,) * 3,
+        in_specs=(vmem,) * 14,
+        out_specs=(vmem,) * 6,
         name="first_payload",
     )(
         tokens,
@@ -219,17 +234,32 @@
         value_weight,
         dense_gate_proj,
         dense_up_proj,
-    )
-    received = exchanged(payload, Z)
-
+        forget_weight.T,
+        forget_bias[None],
+        expert_ids.T,
+        pair_prob.T,
+        group_prob[None],
+    )
+    select_first, select_second, routes = routing
     swap = [(0, 1), (1, 0)]
     neighbours = [(k, k ^ 1) for k in range(quarters)]
     their_rows = lax.ppermute(own_rows, "c", swap)
+    payload, their_rows, core, side, lane = lax.optimization_barrier(
+        (payload, their_rows, core, side, lax.axis_index("x"))
+    )
+    received = exchanged(payload, Z)
+    (
+        received, their_rows, own_rows, forget_logits, cache_gates, lengths, select_first,
+        select_second, routes, dense_mix, core, side, lane,
+    ) = lax.optimization_barrier(
+        (
+            received, their_rows, own_rows, forget_logits, cache_gates, lengths, select_first,
+            select_second, routes, dense_mix, core, side, lane,
+        )
+    )
     chip_rows = in_order(own_rows, their_rows, core, 0)
-    pair_rows = in_order(chip_rows, lax.ppermute(chip_rows, "zl", neighbours), side, 0)
     projection_width = 3 * head_size
-    token_columns = received[:, :seq_count].reshape(chips, 2, half, slab)
-    token_columns = token_columns.transpose(0, 2, 1, 3).reshape(chips * half, 2 * slab)
+    token_columns = received[:, :seq_count].reshape(chips * seq_count, slab)
 
     halves = received[:, seq_count:].reshape(chips, 2, 1, held, slab)
     other_halves = lax.ppermute(halves, "zl", neighbours)
@@ -238,12 +268,11 @@
     output_columns = columns[:, :, 0].reshape(width, head_size)
     down_columns = columns[:, :, 1].reshape(width, head_size)
 
-    shares = product(token_columns, pair_rows[:, :projection_width]).astype(jnp.bfloat16)
-    shares = exchanged(shares.reshape(chips, half, projection_width), Z)
-    shares = shares.reshape(pairs, seq_count, projection_width)
+    shares = product(token_columns, chip_rows[:, :projection_width]).astype(jnp.bfloat16)
+    shares = exchanged(shares.reshape(chips, seq_count, projection_width), Z)
     projected = jnp.sum(shares.astype(jnp.float32), axis=0).astype(jnp.bfloat16)
     projected = projected.reshape(seq_count, 3, 1, head_size)
-    log_forget = jax.nn.log_sigmoid(product(normed, forget_weight) + forget_bias)
+    log_forget = jax.nn.log_sigmoid(forget_logits)
     attended = attend(
         projected[:, 0],
         projected[:, 1],
@@ -254,25 +283,13 @@
         lengths,
         log_forget,
     ).reshape(seq_count, head_size)
-    picks = expert_ids.reshape(-1)
-    capacity = 4 * seq_count // devices
-    slot_total = devices * capacity
-    pick_onehot = (picks[:, None] == jnp.arange(devices, dtype=jnp.int32)[None, :]).astype(jnp.int32)
-    earlier = jnp.cumsum(pick_onehot, axis=0) - pick_onehot
-    slot_rank = jnp.sum(earlier * pick_onehot, axis=1)
-    destination = (picks * capacity + slot_rank).reshape(seq_count, 2)
-    slot_grid = jnp.arange(slot_total, dtype=jnp.int32)
-    select_first = (destination[:, 0:1] == slot_grid[None, :]).astype(jnp.bfloat16)
-    select_second = (destination[:, 1:2] == slot_grid[None, :]).astype(jnp.bfloat16)
-    routes = group_prob[:, None] * pair_prob / jnp.sum(pair_prob, axis=1, keepdims=True)
     head_terms = product_transposed(attended, output_columns).astype(jnp.bfloat16)
-    lane = lax.axis_index("x")
     share = width // lax.axis_size("x")
     head_terms, selectors, routes, lane, share_start, mix_row = lax.optimization_barrier(
         (
             head_terms,
             (select_first, select_second),
-            (routes[:, 0], routes[:, 1]),
+            (routes[0], routes[1]),
             lane,
             lane * share,
             dense_mix.astype(jnp.float32),
@@ -291,51 +308,47 @@
         "sk,sd->kd", select_first + select_second, ffn_share, preferred_element_type=jnp.float32
     )
     outbound = outbound.astype(jnp.bfloat16).reshape(devices, capacity, share)
-    few = seq_count // 4
-    dense_pieces = ffn_in.reshape(4, few, pairs, 2, slab)
+    dense_pieces = ffn_in.reshape(2, capacity, lanes, chips, slab)
     dense_pieces = lax.dynamic_index_in_dim(
-        dense_pieces, lane, axis=1, keepdims=False, allow_negative_indices=False
-    )
-    dense_pieces = dense_pieces.transpose(1, 0, 2, 3).reshape(devices, 2, slab)
+        dense_pieces, lane, axis=2, keepdims=False, allow_negative_indices=False
+    )
+    dense_pieces = dense_pieces.transpose(2, 0, 1, 3).reshape(devices, capacity, slab)
     outbound, mix = lax.optimization_barrier(
         (jnp.concatenate((outbound, dense_pieces), axis=2), mix)
     )
     arrived = exchanged(outbound, EP)
     arrived = from_all(arrived, "x")
     dense_width = 2 * head_size
-    payload_width = width + few // capacity * dense_width
+    payload_width = width + lanes * dense_width
     hbm = pl.BlockSpec(memory_space=pl.ANY)
     payload = pl.pallas_call(
         experts,
-        out_shape=jax.ShapeDtypeStruct((slot_total, payload_width), jnp.bfloat16),
+        out_shape=pltpu.VMEM((slot_total, payload_width), jnp.bfloat16),
         in_specs=(vmem, vmem, hbm, hbm, hbm),
         out_specs=vmem,
         scratch_shapes=(
             pltpu.VMEM(expert_gate.shape[1:], jnp.bfloat16),
             pltpu.VMEM(expert_up.shape[1:], jnp.bfloat16),
             pltpu.VMEM(expert_down.shape[1:], jnp.bfloat16),
-            pltpu.VMEM((2, slot_total, head_size), jnp.float32),
-            pltpu.VMEM((2, slot_total, head_size), jnp.float32),
-            pltpu.VMEM(((payload_width - width) // head_size, slot_total, head_size), jnp.float32),
             pltpu.SemaphoreType.DMA((3,)),
         ),
         name="experts",
     )(
         arrived.reshape(lanes, slot_total, share + slab),
-        pair_rows,
+        chip_rows,
         expert_gate[0],
         expert_up[0],
         expert_down[0],
     )
     back = exchanged(payload.reshape(devices, capacity, payload_width), EP)
     returned = back[:, :, :width].reshape(slot_total, width)
-    dense_parts = back[:, :, width:].reshape(pairs, seq_count, dense_width)
+    dense_parts = back[:, :, width:].reshape(chips, seq_count, dense_width)
     dense_parts = jnp.sum(dense_parts.astype(jnp.float32), axis=0)
     dense_hidden = jax.nn.silu(dense_parts[:, :head_size]) * dense_parts[:, head_size:]
     dense_terms = product_transposed(dense_hidden.astype(jnp.bfloat16), down_columns)
     side_total = (
-        routes[0][:, None] * product(select_first, returned)
-        + routes[1][:, None] * product(select_second, returned)
+        routes[0] * product(select_first, returned)
+        + routes[1] * product(select_second, returned)
         + mix[:, None] * dense_terms
     )
     result = residual.astype(jnp.float32) + summed_over_heads(side_total.astype(jnp.bfloat16))

time: 173 us -> 179 us (1.035)
  blocking collectives: 96 us -> 128 us
  starting transfers between devices: 39 us -> 26.5 us
  other arithmetic: 8.81 us -> 4.08 us
  waiting for transfers between devices: 12.6 us -> 8.76 us
    all_to_all x7 -> x8, blocking collectives: 96 us -> 128 us  [exchanged(): return lax.all_to_all(pieces, axes, split_axis=0, concat_axis=0, tiled=True)]
    all_to_all x2 -> x1, starting transfers between devices: 16.8 us -> 7.26 us  [exchanged(): return lax.all_to_all(pieces, axes, split_axis=0, concat_axis=0, tiled=True)]
    all_to_all x2 -> x1, waiting for transfers between devices: 12.6 us -> 7.66 us  [exchanged(): return lax.all_to_all(pieces, axes, split_axis=0, concat_axis=0, tiled=True)]
    ppermute x1 -> x0, starting transfers between devices: 3.27 us -> none  [layer(): lax.ppermute(chip_rows, 'zl', neighbours)]
  transfers between devices with their start and end apart: 6 -> 4, of which waited for: 2 -> 2; matrix products, arithmetic and copies ran while one was open for 7% -> 3% of each run, Pallas kernels for 0% -> 0%
where the time goes in v3:
time: 179 us; the launch traced here: 178 us
  blocking collectives  128 us (72%)
  starting transfers between devices  26.5 us (15%)
  waiting for transfers between devices  8.76 us (5%)
  Pallas kernels  4.67 us (3%)
  other arithmetic  4.08 us (2%)
  matrix products  2.98 us (2%)
  local copies, waits for them, and re-layouts  2.23 us (1%)
    all_to_all x8, blocking collectives, exchanged(): return lax.all_to_all(pieces, axes, split_axis=0, concat_axis=0, tiled=True)  128 us
    ppermute x1, starting transfers between devices, layer(): their_rows = lax.ppermute(own_rows, 'c', swap)  8.88 us
    all_to_all x1, waiting for transfers between devices, exchanged(): return lax.all_to_all(pieces, axes, split_axis=0, concat_axis=0, tiled=True)  7.66 us
    all_to_all x1, starting transfers between devices, exchanged(): return lax.all_to_all(pieces, axes, split_axis=0, concat_axis=0, tiled=True)  7.26 us
    ppermute x1, starting transfers between devices, layer(): other_halves = lax.ppermute(halves, 'zl', neighbours)  7.22 us
  transfers between devices with their start and end apart: 4, of which 2 were waited for; matrix products, arithmetic and copies ran while one was open for 3% of the time, Pallas kernels for 0%

profile of v3, /device:TPU:1, one launch (start us, length us, event | category | flops | bytes accessed | tf_op | source)
XLA Modules:
  0.0 178.0 jit_solution(2302840397704874680)
XLA Ops:
  0.8 1.9 %first_payload.1 = (bf16[16,80,128]{2,1,0:T(8,128)(2,1)S(1)}, f32[16,1]{1,0:T(8,128)}, bf16[64,640]{1,0:T(8,128)(2,1)}, bf16[16,64]{1,0:T(8,128)(2,1)}, bf16[16,64]{1,0:T(8,128)(2,1)}, /*index=5*/f32[2,16,1]{2,1,0:T(8,128)}) custom-call(bf16[16,2048]{1,0:T(8,128)(2,1)} %tokens_ref.1, f32[1,2048]{1,0:T(1,128)} %bitcast.77, bf16[64,128]{1,0:T(8,128)(2,1)} %bitcast.74, ...), custom_call_target="tpu_custom_call" | custom-call | tf_op jit(solution)/shard_map/first_payload/pallas_call | solution.py:214
  2.7 8.9 %collective-permute-start = (bf16[64,640]{1,0:T(8,128)(2,1)}, bf16[64,640]{1,0:T(8,128)(2,1)S(1)}, u32[]{:S(2)}, u32[]{:S(2)}) collective-permute-start(bf16[64,640]{1,0:T(8,128)(2,1)} %get-tuple-element.53), channel_id=1, source_target_pairs={{0,16},{16,0},{1,17},{17,1},{2,18},{18,2},{3,19},{19,3},{4,20},{20... | collective-permute-start | bytes 245768 | tf_op jit(solution)/shard_map/ppermute | solution.py:246
  11.6 1.1 collective-permute-done
  12.7 24.8 %all_to_all.45 = bf16[16,80,128]{2,1,0:T(8,128)(2,1)S(1)} all-to-all(bf16[16,80,128]{2,1,0:T(8,128)(2,1)S(1)} %get-tuple-element.41), channel_id=1, replica_groups=mesh['zh'=4,'zl'=4,'c'=2,'y'=4,'x'=4] {'zh','zl'}, dimensions={0} | all-to-all | bytes 655360 | tf_op jit(solution)/shard_map/all_to_all | solution.py:19
  37.6 7.2 %collective-permute-start.1 = (bf16[16,2,1,32,128]{4,3,2,0,1:T(8,128)(2,1)S(1)}, bf16[16,2,1,32,128]{4,3,2,0,1:T(8,128)(2,1)S(1)}, u32[]{:S(2)}, u32[]{:S(2)}) collective-permute-start(bf16[16,2,1,32,128]{4,3,2,0,1:T(8,128)(2,1)S(1)} %copy.44), channel_id=1, source_target_pairs={{0,32},{32,0},{64,96},{96,64},{1,33},{33,1},{65,97},{97,65},{2,34}... | collective-permute-start | bytes 786440 | tf_op jit(solution)/shard_map/ppermute | solution.py:265
  44.9 0.9 convolution_convert_fusion.1
  45.8 0.3 fusion.16
  46.2 7.3 %all-to-all-start.1 = ((bf16[16,16,384]{2,1,0:T(8,128)(2,1)}), bf16[16,16,384]{2,1,0:T(8,128)(2,1)S(1)}, u32[]{:S(2)}, u32[]{:S(2)}) async-start(bf16[16,16,384]{2,1,0:T(8,128)(2,1)} %bitcast.9), calls=%async_computation.1 | async-start | bytes 393216 | tf_op jit(solution)/shard_map/all_to_all | solution.py:19
  53.7 0.9 maximum_select_fusion.1
  54.6 3.2 %collective-permute-start.2 = (bf16[16,2,2,32,128]{4,3,2,0,1:T(8,128)(2,1)}, bf16[16,2,2,32,128]{4,3,2,0,1:T(8,128)(2,1)S(1)}, u32[]{:S(2)}, u32[]{:S(2)}) collective-permute-start(bf16[16,2,2,32,128]{4,3,2,0,1:T(8,128)(2,1)} %maximum_select_fusion.1), channel_id=1, source_target_pairs={{0,16},{16,0},{1,17},{17,1},{2,18},{18,2},{3,19},{19,3},{4,20},{20... | collective-permute-start | bytes 1572872 | tf_op jit(solution)/shard_map/ppermute | solution.py:267
  58.1 7.7 %all-to-all-done.1 = bf16[16,16,384]{2,1,0:T(8,128)(2,1)S(1)} async-done(((bf16[16,16,384]{2,1,0:T(8,128)(2,1)}), bf16[16,16,384]{2,1,0:T(8,128)(2,1)S(1)}, u32[]{:S(2)}, u32[]{:S(2)}) %all-to-all-start.1) | async-done | bytes 196640 | tf_op jit(solution)/shard_map/all_to_all | solution.py:19
  65.8 0.2 fusion.25
  66.0 0.6 fusion.5
  66.7 0.3 fusion.36
  67.0 0.3 fusion.34
  67.4 0.4 fusion.3
  68.1 0.3 convolution_convert_fusion
  68.4 9.3 %all_to_all.46 = bf16[4,16,2048]{2,1,0:T(8,128)(2,1)S(1)} all-to-all(bf16[4,16,2048]{2,1,0:T(8,128)(2,1)S(1)} %broadcast_in_dim.55), channel_id=1, replica_groups=mesh['zh'=4,'zl'=4,'c'=2,'y'=4,'x'=4] {'x'}, dimensions={0} | all-to-all | bytes 524288 | tf_op jit(solution)/shard_map/all_to_all | solution.py:19
  77.8 9.5 %all_to_all.47 = bf16[4,16,2048]{2,1,0:T(8,128)(2,1)S(1)} all-to-all(bf16[4,16,2048]{2,1,0:T(8,128)(2,1)S(1)} %broadcast_in_dim.56), channel_id=1, replica_groups=mesh['zh'=4,'zl'=4,'c'=2,'y'=4,'x'=4] {'y'}, dimensions={0} | all-to-all | bytes 524288 | tf_op jit(solution)/shard_map/all_to_all | solution.py:19
  87.5 0.2 multiply_reduce_fusion
  87.8 0.2 convolution_convert_fusion.2
  88.2 26.4 %all_to_all.48 = bf16[32,2,640]{2,1,0:T(2,128)(2,1)S(1)} all-to-all(bf16[32,2,640]{2,1,0:T(2,128)(2,1)S(1)} %pad_maximum_fusion.2), channel_id=1, replica_groups=mesh['zh'=4,'zl'=4,'c'=2,'y'=4,'x'=4] {'zh','zl','c'}, dimensions={0} | all-to-all | bytes 163840 | tf_op jit(solution)/shard_map/all_to_all | solution.py:19
  114.8 8.3 %all_to_all.49 = bf16[4,32,2,640]{3,2,1,0:T(2,128)(2,1)S(1)} all-to-all(bf16[4,32,2,640]{3,2,1,0:T(2,128)(2,1)S(1)} %broadcast_in_dim.57), channel_id=1, replica_groups=mesh['zh'=4,'zl'=4,'c'=2,'y'=4,'x'=4] {'x'}, dimensions={0} | all-to-all | bytes 655360 | tf_op jit(solution)/shard_map/all_to_all | solution.py:19
  123.1 0.8 reshape.280.rows_ref
  123.9 2.8 %experts.1 = bf16[64,3072]{1,0:T(8,128)(2,1)S(1)} custom-call(bf16[4,64,640]{2,1,0:T(8,128)(2,1)} %reshape.280.rows_ref, bf16[128,640]{1,0:T(8,128)(2,1)} %copy-done.1, bf16[2048,128]{1,0:T(8,128)(2,1)} %bitcast.65, bf16[2048,128]{1,0:T(8,128)(2,1)} %bitcast.66, bf16[128,2048]{1,0:T(8,128)(2,1)} %bitcast.67), custom_call_target="tpu_custom_call" | custom-call | tf_op jit(solution)/shard_map/experts/pallas_call | solution.py:324
  126.8 33.2 %all_to_all.50 = bf16[32,2,3072]{2,1,0:T(2,128)(2,1)S(1)} all-to-all(bf16[32,2,3072]{2,1,0:T(2,128)(2,1)S(1)} %reshape.281), channel_id=1, replica_groups=mesh['zh'=4,'zl'=4,'c'=2,'y'=4,'x'=4] {'zh','zl','c'}, dimensions={0} | all-to-all | bytes 786432 | tf_op jit(solution)/shard_map/all_to_all | solution.py:19
  160.1 0.2 slice.61
  160.5 0.2 reshape.284
  161.0 0.2 fusion.2
  161.3 8.0 %all_to_all.51 = bf16[4,16,2048]{2,1,0:T(8,128)(2,1)S(1)} all-to-all(bf16[4,16,2048]{2,1,0:T(8,128)(2,1)S(1)} %broadcast_in_dim.58), channel_id=1, replica_groups=mesh['zh'=4,'zl'=4,'c'=2,'y'=4,'x'=4] {'x'}, dimensions={0} | all-to-all | bytes 524288 | tf_op jit(solution)/shard_map/all_to_all | solution.py:19
  169.4 7.9 %all_to_all.52 = bf16[4,16,2048]{2,1,0:T(8,128)(2,1)S(1)} all-to-all(bf16[4,16,2048]{2,1,0:T(8,128)(2,1)S(1)} %broadcast_in_dim.59), channel_id=1, replica_groups=mesh['zh'=4,'zl'=4,'c'=2,'y'=4,'x'=4] {'y'}, dimensions={0} | all-to-all | bytes 524288 | tf_op jit(solution)/shard_map/all_to_all | solution.py:19
  177.3 0.6 fusion.10
  (71 shorter events, 2.5 us)
Async XLA Ops:
  0.0 66.0 %copy-start = (bf16[16,1,384,128]{3,2,1,0:T(8,128)(2,1)S(1)}, bf16[16,1,384,128]{3,2,1,0:T(8,128)(2,1)}, u32[]{:S(2)}) copy-start(bf16[16,1,384,128]{3,2,1,0:T(8,128)(2,1)} %param.30) | copy-start | bytes 4718596
  0.0 46.2 %copy-start.10 = (bf16[2048]{0:T(1024)(128)(2,1)S(1)}, bf16[2048]{0:T(1024)(128)(2,1)}, u32[]{:S(2)}) copy-start(bf16[2048]{0:T(1024)(128)(2,1)} %param.39) | copy-start | bytes 12292
  0.0 37.6 %copy-start.11 = (s32[16]{0:T(128)S(1)}, s32[16]{0:T(128)}, u32[]{:S(2)}) copy-start(s32[16]{0:T(128)} %param.33) | copy-start | bytes 196
  0.0 45.8 %copy-start.3 = (f32[16,1,384]{2,1,0:T(1,128)S(1)}, f32[16,1,384]{2,1,0:T(1,128)}, u32[]{:S(2)}) copy-start(f32[16,1,384]{2,1,0:T(1,128)} %param.32) | copy-start | bytes 73732
  2.7 42.2 %copy-start.4 = (bf16[64,640]{1,0:T(8,128)(2,1)S(1)}, bf16[64,640]{1,0:T(8,128)(2,1)}, u32[]{:S(2)}) copy-start(bf16[64,640]{1,0:T(8,128)(2,1)} %get-tuple-element.53) | copy-start | bytes 245764
  2.7 50.8 %copy-start.7 = (f32[2,16,1]{2,1,0:T(8,128)S(1)}, f32[2,16,1]{2,1,0:T(8,128)}, u32[]{:S(2)}) copy-start(f32[2,16,1]{2,1,0:T(8,128)} %get-tuple-element.60) | copy-start | bytes 388
  2.7 50.9 %copy-start.9 = (f32[16,1]{1,0:T(8,128)S(1)}, f32[16,1]{1,0:T(8,128)}, u32[]{:S(2)}) copy-start(f32[16,1]{1,0:T(8,128)} %get-tuple-element.56) | copy-start | bytes 196
  2.7 10.0 %collective-permute-start = (bf16[64,640]{1,0:T(8,128)(2,1)}, bf16[64,640]{1,0:T(8,128)(2,1)S(1)}, u32[]{:S(2)}, u32[]{:S(2)}) collective-permute-start(bf16[64,640]{1,0:T(8,128)(2,1)} %get-tuple-element.53), channel_id=1, source_target_pairs={{0,16},{16,0},{1,17},{17,1},{2,18},{18,2},{3,19},{19,3},{4,20},{20... | collective-permute-start | bytes 245768 | tf_op jit(solution)/shard_map/ppermute | solution.py:246
  37.6 16.1 %collective-permute-start.1 = (bf16[16,2,1,32,128]{4,3,2,0,1:T(8,128)(2,1)S(1)}, bf16[16,2,1,32,128]{4,3,2,0,1:T(8,128)(2,1)S(1)}, u32[]{:S(2)}, u32[]{:S(2)}) collective-permute-start(bf16[16,2,1,32,128]{4,3,2,0,1:T(8,128)(2,1)S(1)} %copy.44), channel_id=1, source_target_pairs={{0,32},{32,0},{64,96},{96,64},{1,33},{33,1},{65,97},{97,65},{2,34}... | collective-permute-start | bytes 786440 | tf_op jit(solution)/shard_map/ppermute | solution.py:265
  44.9 13.1 %copy-start.1 = (bf16[128,640]{1,0:T(8,128)(2,1)}, bf16[128,640]{1,0:T(8,128)(2,1)S(1)}, u32[]{:S(2)}) copy-start(bf16[128,640]{1,0:T(8,128)(2,1)S(1)} %maximum_select_fusion.2.dense_ref) | copy-start | bytes 491524
  46.2 19.6 %all-to-all-start.1 = ((bf16[16,16,384]{2,1,0:T(8,128)(2,1)}), bf16[16,16,384]{2,1,0:T(8,128)(2,1)S(1)}, u32[]{:S(2)}, u32[]{:S(2)}) async-start(bf16[16,16,384]{2,1,0:T(8,128)(2,1)} %bitcast.9), calls=%async_computation.1 | async-start | bytes 393216 | tf_op jit(solution)/shard_map/all_to_all | solution.py:19
  54.6 13.2 %collective-permute-start.2 = (bf16[16,2,2,32,128]{4,3,2,0,1:T(8,128)(2,1)}, bf16[16,2,2,32,128]{4,3,2,0,1:T(8,128)(2,1)S(1)}, u32[]{:S(2)}, u32[]{:S(2)}) collective-permute-start(bf16[16,2,2,32,128]{4,3,2,0,1:T(8,128)(2,1)} %maximum_select_fusion.1), channel_id=1, source_target_pairs={{0,16},{16,0},{1,17},{17,1},{2,18},{18,2},{3,19},{19,3},{4,20},{20... | collective-permute-start | bytes 1572872 | tf_op jit(solution)/shard_map/ppermute | solution.py:267
  65.8 1.6 copy-start.12
  68.1 19.3 %copy-start.2 = (bf16[16,2048]{1,0:T(8,128)(2,1)S(1)}, bf16[16,2048]{1,0:T(8,128)(2,1)}, u32[]{:S(2)}) copy-start(bf16[16,2048]{1,0:T(8,128)(2,1)} %tokens_ref.1) | copy-start | bytes 196612
  68.1 19.5 %copy-start.8 = (f32[2048]{0:T(1024)S(1)}, f32[2048]{0:T(1024)}, u32[]{:S(2)}) copy-start(f32[2048]{0:T(1024)} %param.35) | copy-start | bytes 24580
  68.3 19.4 %copy-start.5 = (bf16[16,64]{1,0:T(8,128)(2,1)S(1)}, bf16[16,64]{1,0:T(8,128)(2,1)}, u32[]{:S(2)}) copy-start(bf16[16,64]{1,0:T(8,128)(2,1)} %get-tuple-element.66) | copy-start | bytes 6148
  68.4 19.4 %copy-start.6 = (bf16[16,64]{1,0:T(8,128)(2,1)S(1)}, bf16[16,64]{1,0:T(8,128)(2,1)}, u32[]{:S(2)}) copy-start(bf16[16,64]{1,0:T(8,128)(2,1)} %get-tuple-element.65) | copy-start | bytes 6148

commit v4 on v2

--- a/solution.py
+++ b/solution.py
@@ -57,7 +57,8 @@
 
 def first_payload(
     tokens_ref, gain_ref, out_ref, down_ref, query_ref, key_ref, value_ref, gate_ref, up_ref,
-    payload_ref, normed_ref, rows_ref,
+    forget_ref, bias_ref, ids_ref, pair_ref, group_ref,
+    payload_ref, logits_ref, rows_ref, first_ref, second_ref, routes_ref,
 ):
     seq_count, _ = tokens_ref.shape
     chips, _, slab = payload_ref.shape
@@ -68,7 +69,8 @@
     widened = tokens_ref[...].astype(jnp.float32)
     mean = jnp.mean(widened * widened, axis=-1, keepdims=True)
     normed = (widened * lax.rsqrt(mean + EPSILON) * gain_ref[...]).astype(jnp.bfloat16)
-    normed_ref[...] = normed
+    forget = normed.astype(jnp.float32) * forget_ref[...].astype(jnp.float32)
+    logits_ref[...] = jnp.sum(forget, axis=-1, keepdims=True) + bias_ref[...]
     for chip in range(chips):
         pair, side = divmod(chip, 2)
         for k in range(2):
@@ -79,6 +81,30 @@
         columns = slice(side * held, (side + 1) * held)
         payload_ref[chip, seq_count : seq_count + held, :] = out_ref[columns, :]
         payload_ref[chip, seq_count + held :, :] = down_ref[columns, :]
+
+    row = lax.broadcasted_iota(jnp.int32, (seq_count, seq_count), 0)
+    place = lax.broadcasted_iota(jnp.int32, (seq_count, seq_count), 1)
+
+    def column(values):
+        return jnp.sum(jnp.where(row == place, values, 0.0), axis=1, keepdims=True)
+
+    slot_total = first_ref.shape[1]
+    devices = 2 * chips
+    grid = lax.broadcasted_iota(jnp.int32, (seq_count, devices), 1).astype(jnp.float32)
+    slots = lax.broadcasted_iota(jnp.int32, (seq_count, slot_total), 1).astype(jnp.float32)
+    named = [column(ids_ref[k : k + 1, :].astype(jnp.float32)) for k in range(2)]
+    hot = [(expert == grid).astype(jnp.float32) for expert in named]
+    before = jnp.dot(
+        (place < row).astype(jnp.float32), hot[0] + hot[1], preferred_element_type=jnp.float32
+    )
+    for k, select_ref in enumerate((first_ref, second_ref)):
+        rank = jnp.sum(before * hot[k], axis=1, keepdims=True)
+        target = named[k] * (slot_total // devices) + rank
+        select_ref[...] = (target == slots).astype(jnp.float32).astype(jnp.bfloat16)
+    odds = [column(pair_ref[k : k + 1, :]) for k in range(2)]
+    group = column(group_ref[...])
+    for k in range(2):
+        routes_ref[k] = group * odds[k] / (odds[0] + odds[1])
 
 
 def experts(
@@ -199,15 +225,20 @@
 
     held = output_weight.shape[1] // 2
     vmem = pl.BlockSpec(memory_space=pltpu.VMEM)
-    payload, normed, own_rows = pl.pallas_call(
+    capacity = 4 * seq_count // devices
+    slot_total = devices * capacity
+    payload, forget_logits, own_rows, *routing = pl.pallas_call(
         first_payload,
         out_shape=(
             jax.ShapeDtypeStruct((chips, seq_count + 2 * held, slab), jnp.bfloat16),
-            jax.ShapeDtypeStruct((seq_count, width), jnp.bfloat16),
-            jax.ShapeDtypeStruct((query_weight.shape[0], 5 * slab), jnp.bfloat16),
+            jax.ShapeDtypeStruct((seq_count, 1), jnp.float32),
+            pltpu.VMEM((query_weight.shape[0], 5 * slab), jnp.bfloat16),
+            jax.ShapeDtypeStruct((seq_count, slot_total), jnp.bfloat16),
+            jax.ShapeDtypeStruct((seq_count, slot_total), jnp.bfloat16),
+            jax.ShapeDtypeStruct((2, seq_count, 1), jnp.float32),
         ),
-        in_specs=(vmem,) * 9,
-        out_specs=(vmem,) * 3,
+        in_specs=(vmem,) * 14,
+        out_specs=(vmem,) * 6,
         name="first_payload",
     )(
         tokens,
@@ -219,7 +250,13 @@
         value_weight,
         dense_gate_proj,
         dense_up_proj,
-    )
+        forget_weight.T,
+        forget_bias[None],
+        expert_ids.T,
+        pair_prob.T,
+        group_prob[None],
+    )
+    select_first, select_second, routes = routing
     received = exchanged(payload, Z)
 
     swap = [(0, 1), (1, 0)]
@@ -243,7 +280,7 @@
     shares = shares.reshape(pairs, seq_count, projection_width)
     projected = jnp.sum(shares.astype(jnp.float32), axis=0).astype(jnp.bfloat16)
     projected = projected.reshape(seq_count, 3, 1, head_size)
-    log_forget = jax.nn.log_sigmoid(product(normed, forget_weight) + forget_bias)
+    log_forget = jax.nn.log_sigmoid(forget_logits)
     attended = attend(
         projected[:, 0],
         projected[:, 1],
@@ -254,17 +291,6 @@
         lengths,
         log_forget,
     ).reshape(seq_count, head_size)
-    picks = expert_ids.reshape(-1)
-    capacity = 4 * seq_count // devices
-    slot_total = devices * capacity
-    pick_onehot = (picks[:, None] == jnp.arange(devices, dtype=jnp.int32)[None, :]).astype(jnp.int32)
-    earlier = jnp.cumsum(pick_onehot, axis=0) - pick_onehot
-    slot_rank = jnp.sum(earlier * pick_onehot, axis=1)
-    destination = (picks * capacity + slot_rank).reshape(seq_count, 2)
-    slot_grid = jnp.arange(slot_total, dtype=jnp.int32)
-    select_first = (destination[:, 0:1] == slot_grid[None, :]).astype(jnp.bfloat16)
-    select_second = (destination[:, 1:2] == slot_grid[None, :]).astype(jnp.bfloat16)
-    routes = group_prob[:, None] * pair_prob / jnp.sum(pair_prob, axis=1, keepdims=True)
     head_terms = product_transposed(attended, output_columns).astype(jnp.bfloat16)
     lane = lax.axis_index("x")
     share = width // lax.axis_size("x")
@@ -272,7 +298,7 @@
         (
             head_terms,
             (select_first, select_second),
-            (routes[:, 0], routes[:, 1]),
+            (routes[0], routes[1]),
             lane,
             lane * share,
             dense_mix.astype(jnp.float32),
@@ -307,7 +333,7 @@
     hbm = pl.BlockSpec(memory_space=pl.ANY)
     payload = pl.pallas_call(
         experts,
-        out_shape=jax.ShapeDtypeStruct((slot_total, payload_width), jnp.bfloat16),
+        out_shape=pltpu.VMEM((slot_total, payload_width), jnp.bfloat16),
         in_specs=(vmem, vmem, hbm, hbm, hbm),
         out_specs=vmem,
         scratch_shapes=(
@@ -334,8 +360,8 @@
     dense_hidden = jax.nn.silu(dense_parts[:, :head_size]) * dense_parts[:, head_size:]
     dense_terms = product_transposed(dense_hidden.astype(jnp.bfloat16), down_columns)
     side_total = (
-        routes[0][:, None] * product(select_first, returned)
-        + routes[1][:, None] * product(select_second, returned)
+        routes[0] * product(select_first, returned)
+        + routes[1] * product(select_second, returned)
         + mix[:, None] * dense_terms
     )
     result = residual.astype(jnp.float32) + summed_over_heads(side_total.astype(jnp.bfloat16))

time: 173 us -> 169 us (0.977)
  other arithmetic: 8.81 us -> 6.17 us
  local copies, waits for them, and re-layouts: 3.93 us -> 2.13 us
    all_to_all x2, starting transfers between devices: 16.8 us -> 23.4 us  [exchanged(): return lax.all_to_all(pieces, axes, split_axis=0, concat_axis=0, tiled=True)]
    ppermute x1, starting transfers between devices: 8.73 us -> 2.86 us  [layer(): their_rows = lax.ppermute(own_rows, 'c', swap)]
  transfers between devices with their start and end apart: 6 -> 6, of which waited for: 2 -> 2; matrix products, arithmetic and copies ran while one was open for 7% -> 4% of each run, Pallas kernels for 0% -> 0%
where the time goes in v4:
time: 169 us; the launch traced here: 167 us
  blocking collectives  96 us (57%)
  starting transfers between devices  40.1 us (24%)
  waiting for transfers between devices  13.8 us (8%)
  other arithmetic  6.17 us (4%)
  Pallas kernels  4.76 us (3%)
  matrix products  2.92 us (2%)
  local copies, waits for them, and re-layouts  2.13 us (1%)
    all_to_all x7, blocking collectives, exchanged(): return lax.all_to_all(pieces, axes, split_axis=0, concat_axis=0, tiled=True)  96 us
    all_to_all x2, starting transfers between devices, exchanged(): return lax.all_to_all(pieces, axes, split_axis=0, concat_axis=0, tiled=True)  23.4 us
    all_to_all x2, waiting for transfers between devices, exchanged(): return lax.all_to_all(pieces, axes, split_axis=0, concat_axis=0, tiled=True)  13.8 us
    ppermute x1, starting transfers between devices, layer(): other_halves = lax.ppermute(halves, 'zl', neighbours)  7.22 us
    ppermute x1, starting transfers between devices, layer(): lax.ppermute(chip_rows, 'zl', neighbours)  3.54 us
  transfers between devices with their start and end apart: 6, of which 2 were waited for; matrix products, arithmetic and copies ran while one was open for 4% of the time, Pallas kernels for 0%

profile of v4, /device:TPU:1, one launch (start us, length us, event | category | flops | bytes accessed | tf_op | source)
XLA Modules:
  0.0 167.1 jit_solution(377233599422443250)
XLA Ops:
  0.8 1.9 %first_payload.1 = (bf16[16,80,128]{2,1,0:T(8,128)(2,1)}, f32[16,1]{1,0:T(8,128)}, bf16[64,640]{1,0:T(8,128)(2,1)S(1)}, bf16[16,64]{1,0:T(8,128)(2,1)}, bf16[16,64]{1,0:T(8,128)(2,1)}, /*index=5*/f32[2,16,1]{2,1,0:T(8,128)}) custom-call(bf16[16,2048]{1,0:T(8,128)(2,1)} %tokens_ref.1, f32[1,2048]{1,0:T(1,128)} %bitcast.83, bf16[64,128]{1,0:T(8,128)(2,1)} %bitcast.80, ...), custom_call_target="tpu_custom_call" | custom-call | tf_op jit(solution)/shard_map/first_payload/pallas_call | solution.py:230
  2.7 15.9 %all-to-all-start = ((bf16[16,80,128]{2,1,0:T(8,128)(2,1)}), bf16[16,80,128]{2,1,0:T(8,128)(2,1)S(1)}, u32[]{:S(2)}, u32[]{:S(2)}) async-start(bf16[16,80,128]{2,1,0:T(8,128)(2,1)} %get-tuple-element.21), calls=%async_computation | async-start | bytes 655360 | tf_op jit(solution)/shard_map/all_to_all | solution.py:19
  18.6 2.9 %collective-permute-start = (bf16[64,640]{1,0:T(8,128)(2,1)S(1)}, bf16[64,640]{1,0:T(8,128)(2,1)S(1)}, u32[]{:S(2)}, u32[]{:S(2)}) collective-permute-start(bf16[64,640]{1,0:T(8,128)(2,1)S(1)} %get-tuple-element.22), channel_id=1, source_target_pairs={{0,16},{16,0},{1,17},{17,1},{2,18},{18,2},{3,19},{19,3},{4,20},{20... | collective-permute-start | bytes 245768 | tf_op jit(solution)/shard_map/ppermute | solution.py:264
  21.5 0.7 broadcast_add_fusion
  22.1 1.0 fusion.17
  23.3 3.5 %collective-permute-start.1 = (bf16[128,640]{1,0:T(8,128)(2,1)S(1)}, bf16[128,640]{1,0:T(8,128)(2,1)S(1)}, u32[]{:S(2)}, u32[]{:S(2)}) collective-permute-start(bf16[128,640]{1,0:T(8,128)(2,1)S(1)} %maximum_select_fusion.3), channel_id=1, source_target_pairs={{0,32},{32,0},{64,96},{96,64},{1,33},{33,1},{65,97},{97,65},{2,34}... | collective-permute-start | bytes 491528 | tf_op jit(solution)/shard_map/ppermute | solution.py:266
  26.8 0.8 fusion.22
  27.7 6.3 %all-to-all-done = bf16[16,80,128]{2,1,0:T(8,128)(2,1)S(1)} async-done(((bf16[16,80,128]{2,1,0:T(8,128)(2,1)}), bf16[16,80,128]{2,1,0:T(8,128)(2,1)S(1)}, u32[]{:S(2)}, u32[]{:S(2)}) %all-to-all-start) | async-done | bytes 327712 | tf_op jit(solution)/shard_map/all_to_all | solution.py:19
  34.0 7.2 %collective-permute-start.2 = (bf16[16,2,1,32,128]{4,3,2,0,1:T(8,128)(2,1)S(1)}, bf16[16,2,1,32,128]{4,3,2,0,1:T(8,128)(2,1)S(1)}, u32[]{:S(2)}, u32[]{:S(2)}) collective-permute-start(bf16[16,2,1,32,128]{4,3,2,0,1:T(8,128)(2,1)S(1)} %copy.45), channel_id=1, source_target_pairs={{0,32},{32,0},{64,96},{96,64},{1,33},{33,1},{65,97},{97,65},{2,34}... | collective-permute-start | bytes 786440 | tf_op jit(solution)/shard_map/ppermute | solution.py:272
  41.4 0.8 fusion.7
  42.3 7.5 %all-to-all-start.1 = ((bf16[16,8,384]{2,1,0:T(8,128)(2,1)}), bf16[16,8,384]{2,1,0:T(8,128)(2,1)S(1)}, u32[]{:S(2)}, u32[]{:S(2)}) async-start(bf16[16,8,384]{2,1,0:T(8,128)(2,1)} %fusion.7), calls=%async_computation.1 | async-start | bytes 196608 | tf_op jit(solution)/shard_map/all_to_all | solution.py:19
  49.8 0.9 maximum_select_fusion.1
  50.8 3.1 %collective-permute-start.3 = (bf16[16,2,2,32,128]{4,3,2,0,1:T(8,128)(2,1)}, bf16[16,2,2,32,128]{4,3,2,0,1:T(8,128)(2,1)S(1)}, u32[]{:S(2)}, u32[]{:S(2)}) collective-permute-start(bf16[16,2,2,32,128]{4,3,2,0,1:T(8,128)(2,1)} %maximum_select_fusion.1), channel_id=1, source_target_pairs={{0,16},{16,0},{1,17},{17,1},{2,18},{18,2},{3,19},{19,3},{4,20},{20... | collective-permute-start | bytes 1572872 | tf_op jit(solution)/shard_map/ppermute | solution.py:274
  54.2 7.5 %all-to-all-done.1 = bf16[16,8,384]{2,1,0:T(8,128)(2,1)S(1)} async-done(((bf16[16,8,384]{2,1,0:T(8,128)(2,1)}), bf16[16,8,384]{2,1,0:T(8,128)(2,1)S(1)}, u32[]{:S(2)}, u32[]{:S(2)}) %all-to-all-start.1) | async-done | bytes 98336 | tf_op jit(solution)/shard_map/all_to_all | solution.py:19
  61.9 0.6 fusion.5
  62.6 0.3 fusion.37
  62.9 0.3 fusion.35
  63.3 0.4 fusion.3
  64.0 0.3 convolution_convert_fusion
  64.3 9.3 %all_to_all.45 = bf16[4,16,2048]{2,1,0:T(8,128)(2,1)S(1)} all-to-all(bf16[4,16,2048]{2,1,0:T(8,128)(2,1)S(1)} %broadcast_in_dim.55), channel_id=1, replica_groups=mesh['zh'=4,'zl'=4,'c'=2,'y'=4,'x'=4] {'x'}, dimensions={0} | all-to-all | bytes 524288 | tf_op jit(solution)/shard_map/all_to_all | solution.py:19
  73.7 9.5 %all_to_all.46 = bf16[4,16,2048]{2,1,0:T(8,128)(2,1)S(1)} all-to-all(bf16[4,16,2048]{2,1,0:T(8,128)(2,1)S(1)} %broadcast_in_dim.56), channel_id=1, replica_groups=mesh['zh'=4,'zl'=4,'c'=2,'y'=4,'x'=4] {'y'}, dimensions={0} | all-to-all | bytes 524288 | tf_op jit(solution)/shard_map/all_to_all | solution.py:19
  83.4 0.2 multiply_reduce_fusion
  83.8 0.2 convolution_convert_fusion.2
  84.1 22.7 %all_to_all.47 = bf16[32,2,640]{2,1,0:T(2,128)(2,1)S(1)} all-to-all(bf16[32,2,640]{2,1,0:T(2,128)(2,1)S(1)} %pad_maximum_fusion.2), channel_id=1, replica_groups=mesh['zh'=4,'zl'=4,'c'=2,'y'=4,'x'=4] {'zh','zl','c'}, dimensions={0} | all-to-all | bytes 163840 | tf_op jit(solution)/shard_map/all_to_all | solution.py:19
  107.0 8.3 %all_to_all.48 = bf16[4,32,2,640]{3,2,1,0:T(2,128)(2,1)S(1)} all-to-all(bf16[4,32,2,640]{3,2,1,0:T(2,128)(2,1)S(1)} %broadcast_in_dim.57), channel_id=1, replica_groups=mesh['zh'=4,'zl'=4,'c'=2,'y'=4,'x'=4] {'x'}, dimensions={0} | all-to-all | bytes 655360 | tf_op jit(solution)/shard_map/all_to_all | solution.py:19
  115.2 0.8 reshape.288.rows_ref
  116.1 2.8 %experts.1 = bf16[64,2560]{1,0:T(8,128)(2,1)S(1)} custom-call(bf16[4,64,640]{2,1,0:T(8,128)(2,1)} %reshape.288.rows_ref, bf16[256,640]{1,0:T(8,128)(2,1)} %copy-done.1, bf16[2048,128]{1,0:T(8,128)(2,1)} %bitcast.72, bf16[2048,128]{1,0:T(8,128)(2,1)} %bitcast.73, bf16[128,2048]{1,0:T(8,128)(2,1)} %bitcast.74), custom_call_target="tpu_custom_call" | custom-call | tf_op jit(solution)/shard_map/experts/pallas_call | solution.py:334
  119.1 30.4 %all_to_all.49 = bf16[32,2,2560]{2,1,0:T(2,128)(2,1)S(1)} all-to-all(bf16[32,2,2560]{2,1,0:T(2,128)(2,1)S(1)} %reshape.289), channel_id=1, replica_groups=mesh['zh'=4,'zl'=4,'c'=2,'y'=4,'x'=4] {'zh','zl','c'}, dimensions={0} | all-to-all | bytes 655360 | tf_op jit(solution)/shard_map/all_to_all | solution.py:19
  150.2 0.2 fusion.2
  150.5 7.9 %all_to_all.50 = bf16[4,16,2048]{2,1,0:T(8,128)(2,1)S(1)} all-to-all(bf16[4,16,2048]{2,1,0:T(8,128)(2,1)S(1)} %broadcast_in_dim.58), channel_id=1, replica_groups=mesh['zh'=4,'zl'=4,'c'=2,'y'=4,'x'=4] {'x'}, dimensions={0} | all-to-all | bytes 524288 | tf_op jit(solution)/shard_map/all_to_all | solution.py:19
  158.5 7.9 %all_to_all.51 = bf16[4,16,2048]{2,1,0:T(8,128)(2,1)S(1)} all-to-all(bf16[4,16,2048]{2,1,0:T(8,128)(2,1)S(1)} %broadcast_in_dim.59), channel_id=1, replica_groups=mesh['zh'=4,'zl'=4,'c'=2,'y'=4,'x'=4] {'y'}, dimensions={0} | all-to-all | bytes 524288 | tf_op jit(solution)/shard_map/all_to_all | solution.py:19
  166.5 0.6 fusion.12
  (71 shorter events, 2.9 us)
Async XLA Ops:
  0.0 61.9 %copy-start = (bf16[16,1,384,128]{3,2,1,0:T(8,128)(2,1)S(1)}, bf16[16,1,384,128]{3,2,1,0:T(8,128)(2,1)}, u32[]{:S(2)}) copy-start(bf16[16,1,384,128]{3,2,1,0:T(8,128)(2,1)} %param.30) | copy-start | bytes 4718596
  0.0 41.3 %copy-start.8 = (bf16[2048]{0:T(1024)(128)(2,1)S(1)}, bf16[2048]{0:T(1024)(128)(2,1)}, u32[]{:S(2)}) copy-start(bf16[2048]{0:T(1024)(128)(2,1)} %param.39) | copy-start | bytes 12292
  2.7 38.5 %copy-start.6 = (f32[2,16,1]{2,1,0:T(8,128)S(1)}, f32[2,16,1]{2,1,0:T(8,128)}, u32[]{:S(2)}) copy-start(f32[2,16,1]{2,1,0:T(8,128)} %get-tuple-element.26) | copy-start | bytes 388
  2.7 31.2 %all-to-all-start = ((bf16[16,80,128]{2,1,0:T(8,128)(2,1)}), bf16[16,80,128]{2,1,0:T(8,128)(2,1)S(1)}, u32[]{:S(2)}, u32[]{:S(2)}) async-start(bf16[16,80,128]{2,1,0:T(8,128)(2,1)} %get-tuple-element.21), calls=%async_computation | async-start | bytes 655360 | tf_op jit(solution)/shard_map/all_to_all | solution.py:19
  18.6 4.6 %collective-permute-start = (bf16[64,640]{1,0:T(8,128)(2,1)S(1)}, bf16[64,640]{1,0:T(8,128)(2,1)S(1)}, u32[]{:S(2)}, u32[]{:S(2)}) collective-permute-start(bf16[64,640]{1,0:T(8,128)(2,1)S(1)} %get-tuple-element.22), channel_id=1, source_target_pairs={{0,16},{16,0},{1,17},{17,1},{2,18},{18,2},{3,19},{19,3},{4,20},{20... | collective-permute-start | bytes 245768 | tf_op jit(solution)/shard_map/ppermute | solution.py:264
  23.3 18.1 %collective-permute-start.1 = (bf16[128,640]{1,0:T(8,128)(2,1)S(1)}, bf16[128,640]{1,0:T(8,128)(2,1)S(1)}, u32[]{:S(2)}, u32[]{:S(2)}) collective-permute-start(bf16[128,640]{1,0:T(8,128)(2,1)S(1)} %maximum_select_fusion.3), channel_id=1, source_target_pairs={{0,32},{32,0},{64,96},{96,64},{1,33},{33,1},{65,97},{97,65},{2,34}... | collective-permute-start | bytes 491528 | tf_op jit(solution)/shard_map/ppermute | solution.py:266
  34.0 15.8 %collective-permute-start.2 = (bf16[16,2,1,32,128]{4,3,2,0,1:T(8,128)(2,1)S(1)}, bf16[16,2,1,32,128]{4,3,2,0,1:T(8,128)(2,1)S(1)}, u32[]{:S(2)}, u32[]{:S(2)}) collective-permute-start(bf16[16,2,1,32,128]{4,3,2,0,1:T(8,128)(2,1)S(1)} %copy.45), channel_id=1, source_target_pairs={{0,32},{32,0},{64,96},{96,64},{1,33},{33,1},{65,97},{97,65},{2,34}... | collective-permute-start | bytes 786440 | tf_op jit(solution)/shard_map/ppermute | solution.py:272
  41.4 12.6 %copy-start.1 = (bf16[256,640]{1,0:T(8,128)(2,1)}, bf16[256,640]{1,0:T(8,128)(2,1)S(1)}, u32[]{:S(2)}) copy-start(bf16[256,640]{1,0:T(8,128)(2,1)S(1)} %maximum_select_fusion.2.dense_ref) | copy-start | bytes 983044
  42.3 19.4 %all-to-all-start.1 = ((bf16[16,8,384]{2,1,0:T(8,128)(2,1)}), bf16[16,8,384]{2,1,0:T(8,128)(2,1)S(1)}, u32[]{:S(2)}, u32[]{:S(2)}) async-start(bf16[16,8,384]{2,1,0:T(8,128)(2,1)} %fusion.7), calls=%async_computation.1 | async-start | bytes 196608 | tf_op jit(solution)/shard_map/all_to_all | solution.py:19
  50.8 13.0 %collective-permute-start.3 = (bf16[16,2,2,32,128]{4,3,2,0,1:T(8,128)(2,1)}, bf16[16,2,2,32,128]{4,3,2,0,1:T(8,128)(2,1)S(1)}, u32[]{:S(2)}, u32[]{:S(2)}) collective-permute-start(bf16[16,2,2,32,128]{4,3,2,0,1:T(8,128)(2,1)} %maximum_select_fusion.1), channel_id=1, source_target_pairs={{0,16},{16,0},{1,17},{17,1},{2,18},{18,2},{3,19},{19,3},{4,20},{20... | collective-permute-start | bytes 1572872 | tf_op jit(solution)/shard_map/ppermute | solution.py:274
  54.1 8.6 %copy-start.3 = (f32[16,1,384]{2,1,0:T(1,128)S(1)}, f32[16,1,384]{2,1,0:T(1,128)}, u32[]{:S(2)}) copy-start(f32[16,1,384]{2,1,0:T(1,128)} %param.32) | copy-start | bytes 73732
  54.1 8.5 %copy-start.9 = (s32[16]{0:T(128)S(1)}, s32[16]{0:T(128)}, u32[]{:S(2)}) copy-start(s32[16]{0:T(128)} %param.33) | copy-start | bytes 196
  61.7 1.6 copy-start.10
  64.0 19.3 %copy-start.2 = (bf16[16,2048]{1,0:T(8,128)(2,1)S(1)}, bf16[16,2048]{1,0:T(8,128)(2,1)}, u32[]{:S(2)}) copy-start(bf16[16,2048]{1,0:T(8,128)(2,1)} %tokens_ref.1) | copy-start | bytes 196612
  64.0 19.5 %copy-start.7 = (f32[2048]{0:T(1024)S(1)}, f32[2048]{0:T(1024)}, u32[]{:S(2)}) copy-start(f32[2048]{0:T(1024)} %param.35) | copy-start | bytes 24580
  64.2 19.5 %copy-start.4 = (bf16[16,64]{1,0:T(8,128)(2,1)S(1)}, bf16[16,64]{1,0:T(8,128)(2,1)}, u32[]{:S(2)}) copy-start(bf16[16,64]{1,0:T(8,128)(2,1)} %get-tuple-element.30) | copy-start | bytes 6148
  64.2 19.5 %copy-start.5 = (bf16[16,64]{1,0:T(8,128)(2,1)S(1)}, bf16[16,64]{1,0:T(8,128)(2,1)}, u32[]{:S(2)}) copy-start(bf16[16,64]{1,0:T(8,128)(2,1)} %get-tuple-element.29) | copy-start | bytes 6148

commit v5 on v4

--- a/solution.py
+++ b/solution.py
@@ -21,6 +21,10 @@
 
 def from_all(array, axis):
     return exchanged(jnp.broadcast_to(array, (lax.axis_size(axis), *array.shape)), axis)
+
+
+def summed_at_once(array):
+    return jnp.sum(from_all(array, TP).astype(jnp.float32), axis=0)
 
 
 def summed_over_heads(array):
@@ -347,7 +351,9 @@
         ),
         name="experts",
     )(
-        arrived.reshape(lanes, slot_total, share + slab),
+        pltpu.with_memory_space_constraint(
+            arrived.reshape(lanes, slot_total, share + slab), pltpu.VMEM
+        ),
         pair_rows,
         expert_gate[0],
         expert_up[0],
@@ -364,7 +370,7 @@
         + routes[1] * product(select_second, returned)
         + mix[:, None] * dense_terms
     )
-    result = residual.astype(jnp.float32) + summed_over_heads(side_total.astype(jnp.bfloat16))
+    result = residual.astype(jnp.float32) + summed_at_once(side_total.astype(jnp.bfloat16))
     return result.astype(jnp.bfloat16)
 
 

time: 169 us -> 170 us (level)
  blocking collectives: 96 us -> 98.9 us
    all_to_all x7 -> x6, blocking collectives: 96 us -> 98.9 us  [exchanged(): return lax.all_to_all(pieces, axes, split_axis=0, concat_axis=0, tiled=True)]
where the time goes in v5:
time: 170 us; the launch traced here: 169 us
  blocking collectives  98.9 us (58%)
  starting transfers between devices  40.1 us (24%)
  waiting for transfers between devices  13.8 us (8%)
  other arithmetic  6.24 us (4%)
  Pallas kernels  4.66 us (3%)
  matrix products  2.92 us (2%)
    all_to_all x6, blocking collectives, exchanged(): return lax.all_to_all(pieces, axes, split_axis=0, concat_axis=0, tiled=True)  98.9 us
    all_to_all x2, starting transfers between devices, exchanged(): return lax.all_to_all(pieces, axes, split_axis=0, concat_axis=0, tiled=True)  23.4 us
    all_to_all x2, waiting for transfers between devices, exchanged(): return lax.all_to_all(pieces, axes, split_axis=0, concat_axis=0, tiled=True)  13.8 us
    ppermute x1, starting transfers between devices, layer(): other_halves = lax.ppermute(halves, 'zl', neighbours)  7.22 us
    ppermute x1, starting transfers between devices, layer(): lax.ppermute(chip_rows, 'zl', neighbours)  3.54 us
  transfers between devices with their start and end apart: 6, of which 2 were waited for; matrix products, arithmetic and copies ran while one was open for 4% of the time, Pallas kernels for 0%

profile of v5, /device:TPU:1, one launch (start us, length us, event | category | flops | bytes accessed | tf_op | source)
XLA Modules:
  0.0 169.4 jit_solution(3345025082873810583)
XLA Ops:
  0.8 1.9 %first_payload.1 = (bf16[16,80,128]{2,1,0:T(8,128)(2,1)}, f32[16,1]{1,0:T(8,128)}, bf16[64,640]{1,0:T(8,128)(2,1)S(1)}, bf16[16,64]{1,0:T(8,128)(2,1)}, bf16[16,64]{1,0:T(8,128)(2,1)}, /*index=5*/f32[2,16,1]{2,1,0:T(8,128)}) custom-call(bf16[16,2048]{1,0:T(8,128)(2,1)} %tokens_ref.1, f32[1,2048]{1,0:T(1,128)} %bitcast.83, bf16[64,128]{1,0:T(8,128)(2,1)} %bitcast.80, ...), custom_call_target="tpu_custom_call" | custom-call | tf_op jit(solution)/shard_map/first_payload/pallas_call | solution.py:234
  2.7 15.9 %all-to-all-start = ((bf16[16,80,128]{2,1,0:T(8,128)(2,1)}), bf16[16,80,128]{2,1,0:T(8,128)(2,1)S(1)}, u32[]{:S(2)}, u32[]{:S(2)}) async-start(bf16[16,80,128]{2,1,0:T(8,128)(2,1)} %get-tuple-element.21), calls=%async_computation | async-start | bytes 655360 | tf_op jit(solution)/shard_map/all_to_all | solution.py:19
  18.6 2.9 %collective-permute-start = (bf16[64,640]{1,0:T(8,128)(2,1)S(1)}, bf16[64,640]{1,0:T(8,128)(2,1)S(1)}, u32[]{:S(2)}, u32[]{:S(2)}) collective-permute-start(bf16[64,640]{1,0:T(8,128)(2,1)S(1)} %get-tuple-element.22), channel_id=1, source_target_pairs={{0,16},{16,0},{1,17},{17,1},{2,18},{18,2},{3,19},{19,3},{4,20},{20... | collective-permute-start | bytes 245768 | tf_op jit(solution)/shard_map/ppermute | solution.py:268
  21.5 0.7 broadcast_add_fusion
  22.1 1.0 fusion.17
  23.3 3.5 %collective-permute-start.1 = (bf16[128,640]{1,0:T(8,128)(2,1)S(1)}, bf16[128,640]{1,0:T(8,128)(2,1)S(1)}, u32[]{:S(2)}, u32[]{:S(2)}) collective-permute-start(bf16[128,640]{1,0:T(8,128)(2,1)S(1)} %maximum_select_fusion.3), channel_id=1, source_target_pairs={{0,32},{32,0},{64,96},{96,64},{1,33},{33,1},{65,97},{97,65},{2,34}... | collective-permute-start | bytes 491528 | tf_op jit(solution)/shard_map/ppermute | solution.py:270
  26.8 0.8 fusion.22
  27.7 6.3 %all-to-all-done = bf16[16,80,128]{2,1,0:T(8,128)(2,1)S(1)} async-done(((bf16[16,80,128]{2,1,0:T(8,128)(2,1)}), bf16[16,80,128]{2,1,0:T(8,128)(2,1)S(1)}, u32[]{:S(2)}, u32[]{:S(2)}) %all-to-all-start) | async-done | bytes 327712 | tf_op jit(solution)/shard_map/all_to_all | solution.py:19
  34.0 7.2 %collective-permute-start.2 = (bf16[16,2,1,32,128]{4,3,2,0,1:T(8,128)(2,1)S(1)}, bf16[16,2,1,32,128]{4,3,2,0,1:T(8,128)(2,1)S(1)}, u32[]{:S(2)}, u32[]{:S(2)}) collective-permute-start(bf16[16,2,1,32,128]{4,3,2,0,1:T(8,128)(2,1)S(1)} %copy.45), channel_id=1, source_target_pairs={{0,32},{32,0},{64,96},{96,64},{1,33},{33,1},{65,97},{97,65},{2,34}... | collective-permute-start | bytes 786440 | tf_op jit(solution)/shard_map/ppermute | solution.py:276
  41.4 0.8 fusion.7
  42.3 7.5 %all-to-all-start.1 = ((bf16[16,8,384]{2,1,0:T(8,128)(2,1)}), bf16[16,8,384]{2,1,0:T(8,128)(2,1)S(1)}, u32[]{:S(2)}, u32[]{:S(2)}) async-start(bf16[16,8,384]{2,1,0:T(8,128)(2,1)} %fusion.7), calls=%async_computation.1 | async-start | bytes 196608 | tf_op jit(solution)/shard_map/all_to_all | solution.py:19
  49.8 0.9 maximum_select_fusion.1
  50.8 3.1 %collective-permute-start.3 = (bf16[16,2,2,32,128]{4,3,2,0,1:T(8,128)(2,1)}, bf16[16,2,2,32,128]{4,3,2,0,1:T(8,128)(2,1)S(1)}, u32[]{:S(2)}, u32[]{:S(2)}) collective-permute-start(bf16[16,2,2,32,128]{4,3,2,0,1:T(8,128)(2,1)} %maximum_select_fusion.1), channel_id=1, source_target_pairs={{0,16},{16,0},{1,17},{17,1},{2,18},{18,2},{3,19},{19,3},{4,20},{20... | collective-permute-start | bytes 1572872 | tf_op jit(solution)/shard_map/ppermute | solution.py:278
  54.2 7.5 %all-to-all-done.1 = bf16[16,8,384]{2,1,0:T(8,128)(2,1)S(1)} async-done(((bf16[16,8,384]{2,1,0:T(8,128)(2,1)}), bf16[16,8,384]{2,1,0:T(8,128)(2,1)S(1)}, u32[]{:S(2)}, u32[]{:S(2)}) %all-to-all-start.1) | async-done | bytes 98336 | tf_op jit(solution)/shard_map/all_to_all | solution.py:19
  61.7 0.2 fusion.26
  61.9 0.6 fusion.5
  62.6 0.3 fusion.37
  62.9 0.3 fusion.35
  63.3 0.4 fusion.3
  64.0 0.3 convolution_convert_fusion
  64.3 9.3 %all_to_all.40 = bf16[4,16,2048]{2,1,0:T(8,128)(2,1)S(1)} all-to-all(bf16[4,16,2048]{2,1,0:T(8,128)(2,1)S(1)} %broadcast_in_dim.52), channel_id=1, replica_groups=mesh['zh'=4,'zl'=4,'c'=2,'y'=4,'x'=4] {'x'}, dimensions={0} | all-to-all | bytes 524288 | tf_op jit(solution)/shard_map/all_to_all | solution.py:19
  73.7 9.5 %all_to_all.41 = bf16[4,16,2048]{2,1,0:T(8,128)(2,1)S(1)} all-to-all(bf16[4,16,2048]{2,1,0:T(8,128)(2,1)S(1)} %broadcast_in_dim.53), channel_id=1, replica_groups=mesh['zh'=4,'zl'=4,'c'=2,'y'=4,'x'=4] {'y'}, dimensions={0} | all-to-all | bytes 524288 | tf_op jit(solution)/shard_map/all_to_all | solution.py:19
  83.4 0.2 multiply_reduce_fusion
  83.8 0.2 convolution_convert_fusion.2
  84.1 22.7 %all_to_all.42 = bf16[32,2,640]{2,1,0:T(2,128)(2,1)S(1)} all-to-all(bf16[32,2,640]{2,1,0:T(2,128)(2,1)S(1)} %pad_maximum_fusion.2), channel_id=1, replica_groups=mesh['zh'=4,'zl'=4,'c'=2,'y'=4,'x'=4] {'zh','zl','c'}, dimensions={0} | all-to-all | bytes 163840 | tf_op jit(solution)/shard_map/all_to_all | solution.py:19
  107.0 8.3 %all_to_all.43 = bf16[4,32,2,640]{3,2,1,0:T(2,128)(2,1)S(1)} all-to-all(bf16[4,32,2,640]{3,2,1,0:T(2,128)(2,1)S(1)} %broadcast_in_dim.54), channel_id=1, replica_groups=mesh['zh'=4,'zl'=4,'c'=2,'y'=4,'x'=4] {'x'}, dimensions={0} | all-to-all | bytes 655360 | tf_op jit(solution)/shard_map/all_to_all | solution.py:19
  115.4 2.7 %experts.1 = bf16[64,2560]{1,0:T(8,128)(2,1)S(1)} custom-call(bf16[4,64,640]{2,1,0:T(8,128)(2,1)S(1)} %reshape.288.rows_ref, bf16[256,640]{1,0:T(8,128)(2,1)} %copy-done.1, bf16[2048,128]{1,0:T(8,128)(2,1)} %bitcast.72, bf16[2048,128]{1,0:T(8,128)(2,1)} %bitcast.73, bf16[128,2048]{1,0:T(8,128)(2,1)} %bitcast.74), custom_call_target="tpu_custom_call" | custom-call | tf_op jit(solution)/shard_map/experts/pallas_call | solution.py:338
  118.3 30.4 %all_to_all.44 = bf16[32,2,2560]{2,1,0:T(2,128)(2,1)S(1)} all-to-all(bf16[32,2,2560]{2,1,0:T(2,128)(2,1)S(1)} %reshape.289), channel_id=1, replica_groups=mesh['zh'=4,'zl'=4,'c'=2,'y'=4,'x'=4] {'zh','zl','c'}, dimensions={0} | all-to-all | bytes 655360 | tf_op jit(solution)/shard_map/all_to_all | solution.py:19
  148.6 0.2 slice.63
  149.4 0.2 fusion.2
  149.8 18.8 %all_to_all.45 = bf16[16,16,2048]{2,1,0:T(8,128)(2,1)S(1)} all-to-all(bf16[16,16,2048]{2,1,0:T(8,128)(2,1)S(1)} %broadcast_in_dim.55), channel_id=1, replica_groups=mesh['zh'=4,'zl'=4,'c'=2,'y'=4,'x'=4] {'y','x'}, dimensions={0} | all-to-all | bytes 2097152 | tf_op jit(solution)/shard_map/all_to_all | solution.py:19
  168.7 0.6 fusion.12
  (68 shorter events, 2.7 us)
Async XLA Ops:
  0.0 61.9 %copy-start = (bf16[16,1,384,128]{3,2,1,0:T(8,128)(2,1)S(1)}, bf16[16,1,384,128]{3,2,1,0:T(8,128)(2,1)}, u32[]{:S(2)}) copy-start(bf16[16,1,384,128]{3,2,1,0:T(8,128)(2,1)} %param.30) | copy-start | bytes 4718596
  0.0 41.3 %copy-start.8 = (bf16[2048]{0:T(1024)(128)(2,1)S(1)}, bf16[2048]{0:T(1024)(128)(2,1)}, u32[]{:S(2)}) copy-start(bf16[2048]{0:T(1024)(128)(2,1)} %param.39) | copy-start | bytes 12292
  2.7 38.5 %copy-start.6 = (f32[2,16,1]{2,1,0:T(8,128)S(1)}, f32[2,16,1]{2,1,0:T(8,128)}, u32[]{:S(2)}) copy-start(f32[2,16,1]{2,1,0:T(8,128)} %get-tuple-element.26) | copy-start | bytes 388
  2.7 31.2 %all-to-all-start = ((bf16[16,80,128]{2,1,0:T(8,128)(2,1)}), bf16[16,80,128]{2,1,0:T(8,128)(2,1)S(1)}, u32[]{:S(2)}, u32[]{:S(2)}) async-start(bf16[16,80,128]{2,1,0:T(8,128)(2,1)} %get-tuple-element.21), calls=%async_computation | async-start | bytes 655360 | tf_op jit(solution)/shard_map/all_to_all | solution.py:19
  18.6 4.6 %collective-permute-start = (bf16[64,640]{1,0:T(8,128)(2,1)S(1)}, bf16[64,640]{1,0:T(8,128)(2,1)S(1)}, u32[]{:S(2)}, u32[]{:S(2)}) collective-permute-start(bf16[64,640]{1,0:T(8,128)(2,1)S(1)} %get-tuple-element.22), channel_id=1, source_target_pairs={{0,16},{16,0},{1,17},{17,1},{2,18},{18,2},{3,19},{19,3},{4,20},{20... | collective-permute-start | bytes 245768 | tf_op jit(solution)/shard_map/ppermute | solution.py:268
  23.3 18.1 %collective-permute-start.1 = (bf16[128,640]{1,0:T(8,128)(2,1)S(1)}, bf16[128,640]{1,0:T(8,128)(2,1)S(1)}, u32[]{:S(2)}, u32[]{:S(2)}) collective-permute-start(bf16[128,640]{1,0:T(8,128)(2,1)S(1)} %maximum_select_fusion.3), channel_id=1, source_target_pairs={{0,32},{32,0},{64,96},{96,64},{1,33},{33,1},{65,97},{97,65},{2,34}... | collective-permute-start | bytes 491528 | tf_op jit(solution)/shard_map/ppermute | solution.py:270
  34.0 15.8 %collective-permute-start.2 = (bf16[16,2,1,32,128]{4,3,2,0,1:T(8,128)(2,1)S(1)}, bf16[16,2,1,32,128]{4,3,2,0,1:T(8,128)(2,1)S(1)}, u32[]{:S(2)}, u32[]{:S(2)}) collective-permute-start(bf16[16,2,1,32,128]{4,3,2,0,1:T(8,128)(2,1)S(1)} %copy.45), channel_id=1, source_target_pairs={{0,32},{32,0},{64,96},{96,64},{1,33},{33,1},{65,97},{97,65},{2,34}... | collective-permute-start | bytes 786440 | tf_op jit(solution)/shard_map/ppermute | solution.py:276
  41.4 12.6 %copy-start.1 = (bf16[256,640]{1,0:T(8,128)(2,1)}, bf16[256,640]{1,0:T(8,128)(2,1)S(1)}, u32[]{:S(2)}) copy-start(bf16[256,640]{1,0:T(8,128)(2,1)S(1)} %maximum_select_fusion.2.dense_ref) | copy-start | bytes 983044
  42.3 19.4 %all-to-all-start.1 = ((bf16[16,8,384]{2,1,0:T(8,128)(2,1)}), bf16[16,8,384]{2,1,0:T(8,128)(2,1)S(1)}, u32[]{:S(2)}, u32[]{:S(2)}) async-start(bf16[16,8,384]{2,1,0:T(8,128)(2,1)} %fusion.7), calls=%async_computation.1 | async-start | bytes 196608 | tf_op jit(solution)/shard_map/all_to_all | solution.py:19
  50.8 13.0 %collective-permute-start.3 = (bf16[16,2,2,32,128]{4,3,2,0,1:T(8,128)(2,1)}, bf16[16,2,2,32,128]{4,3,2,0,1:T(8,128)(2,1)S(1)}, u32[]{:S(2)}, u32[]{:S(2)}) collective-permute-start(bf16[16,2,2,32,128]{4,3,2,0,1:T(8,128)(2,1)} %maximum_select_fusion.1), channel_id=1, source_target_pairs={{0,16},{16,0},{1,17},{17,1},{2,18},{18,2},{3,19},{19,3},{4,20},{20... | collective-permute-start | bytes 1572872 | tf_op jit(solution)/shard_map/ppermute | solution.py:278
  54.1 8.6 %copy-start.3 = (f32[16,1,384]{2,1,0:T(1,128)S(1)}, f32[16,1,384]{2,1,0:T(1,128)}, u32[]{:S(2)}) copy-start(f32[16,1,384]{2,1,0:T(1,128)} %param.32) | copy-start | bytes 73732
  54.1 8.5 %copy-start.9 = (s32[16]{0:T(128)S(1)}, s32[16]{0:T(128)}, u32[]{:S(2)}) copy-start(s32[16]{0:T(128)} %param.33) | copy-start | bytes 196
  61.7 1.6 copy-start.10
  64.0 19.3 %copy-start.2 = (bf16[16,2048]{1,0:T(8,128)(2,1)S(1)}, bf16[16,2048]{1,0:T(8,128)(2,1)}, u32[]{:S(2)}) copy-start(bf16[16,2048]{1,0:T(8,128)(2,1)} %tokens_ref.1) | copy-start | bytes 196612
  64.0 19.5 %copy-start.7 = (f32[2048]{0:T(1024)S(1)}, f32[2048]{0:T(1024)}, u32[]{:S(2)}) copy-start(f32[2048]{0:T(1024)} %param.35) | copy-start | bytes 24580
  64.2 19.5 %copy-start.4 = (bf16[16,64]{1,0:T(8,128)(2,1)S(1)}, bf16[16,64]{1,0:T(8,128)(2,1)}, u32[]{:S(2)}) copy-start(bf16[16,64]{1,0:T(8,128)(2,1)} %get-tuple-element.30) | copy-start | bytes 6148
  64.2 19.5 %copy-start.5 = (bf16[16,64]{1,0:T(8,128)(2,1)S(1)}, bf16[16,64]{1,0:T(8,128)(2,1)}, u32[]{:S(2)}) copy-start(bf16[16,64]{1,0:T(8,128)(2,1)} %get-tuple-element.29) | copy-start | bytes 6148

commit v6 on v5

--- a/solution.py
+++ b/solution.py
@@ -21,10 +21,6 @@
 
 def from_all(array, axis):
     return exchanged(jnp.broadcast_to(array, (lax.axis_size(axis), *array.shape)), axis)
-
-
-def summed_at_once(array):
-    return jnp.sum(from_all(array, TP).astype(jnp.float32), axis=0)
 
 
 def summed_over_heads(array):
@@ -274,8 +270,14 @@
 
     halves = received[:, seq_count:].reshape(chips, 2, 1, held, slab)
     other_halves = lax.ppermute(halves, "zl", neighbours)
-    both = in_order(halves, other_halves, side, 2)
-    columns = in_order(both[:, None], lax.ppermute(both, "c", swap)[:, None], core, 1)
+    their_halves = lax.ppermute(halves, "c", swap)
+    their_others = lax.ppermute(other_halves, "c", swap)
+    columns = in_order(
+        in_order(halves, other_halves, side, 2)[:, None],
+        in_order(their_halves, their_others, side, 2)[:, None],
+        core,
+        1,
+    )
     output_columns = columns[:, :, 0].reshape(width, head_size)
     down_columns = columns[:, :, 1].reshape(width, head_size)
 
@@ -370,7 +372,7 @@
         + routes[1] * product(select_second, returned)
         + mix[:, None] * dense_terms
     )
-    result = residual.astype(jnp.float32) + summed_at_once(side_total.astype(jnp.bfloat16))
+    result = residual.astype(jnp.float32) + summed_over_heads(side_total.astype(jnp.bfloat16))
     return result.astype(jnp.bfloat16)
 
 

time: 170 us -> 172 us (1.012)
  blocking collectives: 98.9 us -> 95.9 us
  starting transfers between devices: 40.1 us -> 42.1 us
  waiting for transfers between devices: 13.8 us -> 15.8 us
    ppermute x1 -> x2, starting transfers between devices: 3.1 us -> 8.46 us  [the longest x1 6.26 us: layer(): their_halves = lax.ppermute(halves, 'c', swap)]
    all_to_all x2, starting transfers between devices: 23.4 us -> 20 us  [exchanged(): return lax.all_to_all(pieces, axes, split_axis=0, concat_axis=0, tiled=True)]
    all_to_all x6 -> x7, blocking collectives: 98.9 us -> 95.9 us  [exchanged(): return lax.all_to_all(pieces, axes, split_axis=0, concat_axis=0, tiled=True)]
    all_to_all x2, waiting for transfers between devices: 13.8 us -> 15.7 us  [exchanged(): return lax.all_to_all(pieces, axes, split_axis=0, concat_axis=0, tiled=True)]
  transfers between devices with their start and end apart: 6 -> 7, of which waited for: 2 -> 2; matrix products, arithmetic and copies ran while one was open for 4% -> 3% of each run, Pallas kernels for 0% -> 0%
where the time goes in v6:
time: 172 us; the launch traced here: 170 us
  blocking collectives  95.9 us (56%)
  starting transfers between devices  42.1 us (24%)
  waiting for transfers between devices  15.8 us (9%)
  other arithmetic  6.3 us (4%)
  Pallas kernels  4.68 us (3%)
  matrix products  2.93 us (2%)
    all_to_all x7, blocking collectives, exchanged(): return lax.all_to_all(pieces, axes, split_axis=0, concat_axis=0, tiled=True)  95.9 us
    all_to_all x2, starting transfers between devices, exchanged(): return lax.all_to_all(pieces, axes, split_axis=0, concat_axis=0, tiled=True)  20 us
    all_to_all x2, waiting for transfers between devices, exchanged(): return lax.all_to_all(pieces, axes, split_axis=0, concat_axis=0, tiled=True)  15.7 us
    ppermute x1, starting transfers between devices, layer(): other_halves = lax.ppermute(halves, 'zl', neighbours)  7.22 us
    ppermute x1, starting transfers between devices, layer(): their_halves = lax.ppermute(halves, 'c', swap)  6.26 us
    ppermute x1, starting transfers between devices, layer(): lax.ppermute(chip_rows, 'zl', neighbours)  3.54 us
  transfers between devices with their start and end apart: 7, of which 2 were waited for; matrix products, arithmetic and copies ran while one was open for 3% of the time, Pallas kernels for 0%

profile of v6, /device:TPU:1, one launch (start us, length us, event | category | flops | bytes accessed | tf_op | source)
XLA Modules:
  0.0 170.4 jit_solution(11475612519983716140)
XLA Ops:
  0.8 1.9 %first_payload.1 = (bf16[16,80,128]{2,1,0:T(8,128)(2,1)}, f32[16,1]{1,0:T(8,128)}, bf16[64,640]{1,0:T(8,128)(2,1)S(1)}, bf16[16,64]{1,0:T(8,128)(2,1)}, bf16[16,64]{1,0:T(8,128)(2,1)}, /*index=5*/f32[2,16,1]{2,1,0:T(8,128)}) custom-call(bf16[16,2048]{1,0:T(8,128)(2,1)} %tokens_ref.1, f32[1,2048]{1,0:T(1,128)} %bitcast.83, bf16[64,128]{1,0:T(8,128)(2,1)} %bitcast.80, ...), custom_call_target="tpu_custom_call" | custom-call | tf_op jit(solution)/shard_map/first_payload/pallas_call | solution.py:230
  2.7 15.9 %all-to-all-start = ((bf16[16,80,128]{2,1,0:T(8,128)(2,1)}), bf16[16,80,128]{2,1,0:T(8,128)(2,1)S(1)}, u32[]{:S(2)}, u32[]{:S(2)}) async-start(bf16[16,80,128]{2,1,0:T(8,128)(2,1)} %get-tuple-element.21), calls=%async_computation | async-start | bytes 655360 | tf_op jit(solution)/shard_map/all_to_all | solution.py:19
  18.6 2.9 %collective-permute-start = (bf16[64,640]{1,0:T(8,128)(2,1)S(1)}, bf16[64,640]{1,0:T(8,128)(2,1)S(1)}, u32[]{:S(2)}, u32[]{:S(2)}) collective-permute-start(bf16[64,640]{1,0:T(8,128)(2,1)S(1)} %get-tuple-element.22), channel_id=1, source_target_pairs={{0,16},{16,0},{1,17},{17,1},{2,18},{18,2},{3,19},{19,3},{4,20},{20... | collective-permute-start | bytes 245768 | tf_op jit(solution)/shard_map/ppermute | solution.py:264
  21.5 0.7 broadcast_add_fusion
  22.1 1.0 fusion.17
  23.3 3.5 %collective-permute-start.1 = (bf16[128,640]{1,0:T(8,128)(2,1)S(1)}, bf16[128,640]{1,0:T(8,128)(2,1)S(1)}, u32[]{:S(2)}, u32[]{:S(2)}) collective-permute-start(bf16[128,640]{1,0:T(8,128)(2,1)S(1)} %maximum_select_fusion.3), channel_id=1, source_target_pairs={{0,32},{32,0},{64,96},{96,64},{1,33},{33,1},{65,97},{97,65},{2,34}... | collective-permute-start | bytes 491528 | tf_op jit(solution)/shard_map/ppermute | solution.py:266
  26.8 0.8 fusion.22
  27.7 6.3 %all-to-all-done = bf16[16,80,128]{2,1,0:T(8,128)(2,1)S(1)} async-done(((bf16[16,80,128]{2,1,0:T(8,128)(2,1)}), bf16[16,80,128]{2,1,0:T(8,128)(2,1)S(1)}, u32[]{:S(2)}, u32[]{:S(2)}) %all-to-all-start) | async-done | bytes 327712 | tf_op jit(solution)/shard_map/all_to_all | solution.py:19
  34.0 7.2 %collective-permute-start.2 = (bf16[16,2,1,32,128]{4,3,0,1,2:T(8,128)(2,1)S(1)}, bf16[16,2,1,32,128]{4,3,0,1,2:T(8,128)(2,1)S(1)}, u32[]{:S(2)}, u32[]{:S(2)}) collective-permute-start(bf16[16,2,1,32,128]{4,3,0,1,2:T(8,128)(2,1)S(1)} %copy.43), channel_id=1, source_target_pairs={{0,32},{32,0},{64,96},{96,64},{1,33},{33,1},{65,97},{97,65},{2,34}... | collective-permute-start | bytes 786440 | tf_op jit(solution)/shard_map/ppermute | solution.py:272
  41.4 6.3 %collective-permute-start.3 = (bf16[16,2,1,32,128]{4,3,0,1,2:T(8,128)(2,1)S(1)}, bf16[16,2,1,32,128]{4,3,0,1,2:T(8,128)(2,1)S(1)}, u32[]{:S(2)}, u32[]{:S(2)}) collective-permute-start(bf16[16,2,1,32,128]{4,3,0,1,2:T(8,128)(2,1)S(1)} %copy.43), channel_id=1, source_target_pairs={{0,16},{16,0},{1,17},{17,1},{2,18},{18,2},{3,19},{19,3},{4,20},{20... | collective-permute-start | bytes 786440 | tf_op jit(solution)/shard_map/ppermute | solution.py:273
  47.7 0.8 fusion.7
  48.5 4.1 %all-to-all-start.1 = ((bf16[16,8,384]{2,1,0:T(8,128)(2,1)}), bf16[16,8,384]{2,1,0:T(8,128)(2,1)S(1)}, u32[]{:S(2)}, u32[]{:S(2)}) async-start(bf16[16,8,384]{2,1,0:T(8,128)(2,1)} %fusion.7), calls=%async_computation.1 | async-start | bytes 196608 | tf_op jit(solution)/shard_map/all_to_all | solution.py:19
  52.9 2.2 %collective-permute-start.4 = (bf16[16,2,1,32,128]{4,3,0,1,2:T(8,128)(2,1)S(1)}, bf16[16,2,1,32,128]{4,3,0,1,2:T(8,128)(2,1)}, u32[]{:S(2)}, u32[]{:S(2)}) collective-permute-start(bf16[16,2,1,32,128]{4,3,0,1,2:T(8,128)(2,1)S(1)} %collective-permute-done.2), channel_id=1, source_target_pairs={{0,16},{16,0},{1,17},{17,1},{2,18},{18,2},{3,19},{19,3},{4,20},{20... | collective-permute-start | bytes 786440 | tf_op jit(solution)/shard_map/ppermute | solution.py:274
  55.2 9.5 %all-to-all-done.1 = bf16[16,8,384]{2,1,0:T(8,128)(2,1)S(1)} async-done(((bf16[16,8,384]{2,1,0:T(8,128)(2,1)}), bf16[16,8,384]{2,1,0:T(8,128)(2,1)S(1)}, u32[]{:S(2)}, u32[]{:S(2)}) %all-to-all-start.1) | async-done | bytes 98336 | tf_op jit(solution)/shard_map/all_to_all | solution.py:19
  64.9 0.6 fusion.5
  65.6 0.3 fusion.37
  66.0 0.3 fusion.35
  66.3 0.4 fusion.3
  66.8 1.1 maximum_select_fusion.1
  68.1 0.3 convolution_convert_fusion
  68.4 9.3 %all_to_all.45 = bf16[4,16,2048]{2,1,0:T(8,128)(2,1)S(1)} all-to-all(bf16[4,16,2048]{2,1,0:T(8,128)(2,1)S(1)} %broadcast_in_dim.52), channel_id=1, replica_groups=mesh['zh'=4,'zl'=4,'c'=2,'y'=4,'x'=4] {'x'}, dimensions={0} | all-to-all | bytes 524288 | tf_op jit(solution)/shard_map/all_to_all | solution.py:19
  77.8 9.5 %all_to_all.46 = bf16[4,16,2048]{2,1,0:T(8,128)(2,1)S(1)} all-to-all(bf16[4,16,2048]{2,1,0:T(8,128)(2,1)S(1)} %broadcast_in_dim.53), channel_id=1, replica_groups=mesh['zh'=4,'zl'=4,'c'=2,'y'=4,'x'=4] {'y'}, dimensions={0} | all-to-all | bytes 524288 | tf_op jit(solution)/shard_map/all_to_all | solution.py:19
  87.5 0.2 multiply_reduce_fusion
  87.9 0.2 convolution_convert_fusion.2
  88.3 22.6 %all_to_all.47 = bf16[32,2,640]{2,1,0:T(2,128)(2,1)S(1)} all-to-all(bf16[32,2,640]{2,1,0:T(2,128)(2,1)S(1)} %pad_maximum_fusion.2), channel_id=1, replica_groups=mesh['zh'=4,'zl'=4,'c'=2,'y'=4,'x'=4] {'zh','zl','c'}, dimensions={0} | all-to-all | bytes 163840 | tf_op jit(solution)/shard_map/all_to_all | solution.py:19
  111.0 8.3 %all_to_all.48 = bf16[4,32,2,640]{3,2,1,0:T(2,128)(2,1)S(1)} all-to-all(bf16[4,32,2,640]{3,2,1,0:T(2,128)(2,1)S(1)} %broadcast_in_dim.54), channel_id=1, replica_groups=mesh['zh'=4,'zl'=4,'c'=2,'y'=4,'x'=4] {'x'}, dimensions={0} | all-to-all | bytes 655360 | tf_op jit(solution)/shard_map/all_to_all | solution.py:19
  119.4 2.7 %experts.1 = bf16[64,2560]{1,0:T(8,128)(2,1)S(1)} custom-call(bf16[4,64,640]{2,1,0:T(8,128)(2,1)S(1)} %reshape.343.rows_ref, bf16[256,640]{1,0:T(8,128)(2,1)} %copy-done.1, bf16[2048,128]{1,0:T(8,128)(2,1)} %bitcast.71, bf16[2048,128]{1,0:T(8,128)(2,1)} %bitcast.72, bf16[128,2048]{1,0:T(8,128)(2,1)} %bitcast.73), custom_call_target="tpu_custom_call" | custom-call | tf_op jit(solution)/shard_map/experts/pallas_call | solution.py:340
  122.3 30.4 %all_to_all.49 = bf16[32,2,2560]{2,1,0:T(2,128)(2,1)S(1)} all-to-all(bf16[32,2,2560]{2,1,0:T(2,128)(2,1)S(1)} %reshape.344), channel_id=1, replica_groups=mesh['zh'=4,'zl'=4,'c'=2,'y'=4,'x'=4] {'zh','zl','c'}, dimensions={0} | all-to-all | bytes 655360 | tf_op jit(solution)/shard_map/all_to_all | solution.py:19
  153.5 0.2 fusion.2
  153.8 7.9 %all_to_all.50 = bf16[4,16,2048]{2,1,0:T(8,128)(2,1)S(1)} all-to-all(bf16[4,16,2048]{2,1,0:T(8,128)(2,1)S(1)} %broadcast_in_dim.55), channel_id=1, replica_groups=mesh['zh'=4,'zl'=4,'c'=2,'y'=4,'x'=4] {'x'}, dimensions={0} | all-to-all | bytes 524288 | tf_op jit(solution)/shard_map/all_to_all | solution.py:19
  161.8 7.9 %all_to_all.51 = bf16[4,16,2048]{2,1,0:T(8,128)(2,1)S(1)} all-to-all(bf16[4,16,2048]{2,1,0:T(8,128)(2,1)S(1)} %broadcast_in_dim.56), channel_id=1, replica_groups=mesh['zh'=4,'zl'=4,'c'=2,'y'=4,'x'=4] {'y'}, dimensions={0} | all-to-all | bytes 524288 | tf_op jit(solution)/shard_map/all_to_all | solution.py:19
  169.7 0.6 fusion.12
  (73 shorter events, 3.0 us)
Async XLA Ops:
  0.0 64.9 %copy-start = (bf16[16,1,384,128]{3,2,1,0:T(8,128)(2,1)S(1)}, bf16[16,1,384,128]{3,2,1,0:T(8,128)(2,1)}, u32[]{:S(2)}) copy-start(bf16[16,1,384,128]{3,2,1,0:T(8,128)(2,1)} %param.30) | copy-start | bytes 4718596
  0.0 41.3 %copy-start.8 = (bf16[2048]{0:T(1024)(128)(2,1)S(1)}, bf16[2048]{0:T(1024)(128)(2,1)}, u32[]{:S(2)}) copy-start(bf16[2048]{0:T(1024)(128)(2,1)} %param.39) | copy-start | bytes 12292
  2.7 38.5 %copy-start.6 = (f32[2,16,1]{2,1,0:T(8,128)S(1)}, f32[2,16,1]{2,1,0:T(8,128)}, u32[]{:S(2)}) copy-start(f32[2,16,1]{2,1,0:T(8,128)} %get-tuple-element.26) | copy-start | bytes 388
  2.7 31.2 %all-to-all-start = ((bf16[16,80,128]{2,1,0:T(8,128)(2,1)}), bf16[16,80,128]{2,1,0:T(8,128)(2,1)S(1)}, u32[]{:S(2)}, u32[]{:S(2)}) async-start(bf16[16,80,128]{2,1,0:T(8,128)(2,1)} %get-tuple-element.21), calls=%async_computation | async-start | bytes 655360 | tf_op jit(solution)/shard_map/all_to_all | solution.py:19
  18.6 4.6 %collective-permute-start = (bf16[64,640]{1,0:T(8,128)(2,1)S(1)}, bf16[64,640]{1,0:T(8,128)(2,1)S(1)}, u32[]{:S(2)}, u32[]{:S(2)}) collective-permute-start(bf16[64,640]{1,0:T(8,128)(2,1)S(1)} %get-tuple-element.22), channel_id=1, source_target_pairs={{0,16},{16,0},{1,17},{17,1},{2,18},{18,2},{3,19},{19,3},{4,20},{20... | collective-permute-start | bytes 245768 | tf_op jit(solution)/shard_map/ppermute | solution.py:264
  23.3 18.1 %collective-permute-start.1 = (bf16[128,640]{1,0:T(8,128)(2,1)S(1)}, bf16[128,640]{1,0:T(8,128)(2,1)S(1)}, u32[]{:S(2)}, u32[]{:S(2)}) collective-permute-start(bf16[128,640]{1,0:T(8,128)(2,1)S(1)} %maximum_select_fusion.3), channel_id=1, source_target_pairs={{0,32},{32,0},{64,96},{96,64},{1,33},{33,1},{65,97},{97,65},{2,34}... | collective-permute-start | bytes 491528 | tf_op jit(solution)/shard_map/ppermute | solution.py:266
  34.0 18.7 %collective-permute-start.2 = (bf16[16,2,1,32,128]{4,3,0,1,2:T(8,128)(2,1)S(1)}, bf16[16,2,1,32,128]{4,3,0,1,2:T(8,128)(2,1)S(1)}, u32[]{:S(2)}, u32[]{:S(2)}) collective-permute-start(bf16[16,2,1,32,128]{4,3,0,1,2:T(8,128)(2,1)S(1)} %copy.43), channel_id=1, source_target_pairs={{0,32},{32,0},{64,96},{96,64},{1,33},{33,1},{65,97},{97,65},{2,34}... | collective-permute-start | bytes 786440 | tf_op jit(solution)/shard_map/ppermute | solution.py:272
  41.4 13.7 %copy-start.1 = (bf16[256,640]{1,0:T(8,128)(2,1)}, bf16[256,640]{1,0:T(8,128)(2,1)S(1)}, u32[]{:S(2)}) copy-start(bf16[256,640]{1,0:T(8,128)(2,1)S(1)} %maximum_select_fusion.2.dense_ref) | copy-start | bytes 983044
  41.4 25.3 %collective-permute-start.3 = (bf16[16,2,1,32,128]{4,3,0,1,2:T(8,128)(2,1)S(1)}, bf16[16,2,1,32,128]{4,3,0,1,2:T(8,128)(2,1)S(1)}, u32[]{:S(2)}, u32[]{:S(2)}) collective-permute-start(bf16[16,2,1,32,128]{4,3,0,1,2:T(8,128)(2,1)S(1)} %copy.43), channel_id=1, source_target_pairs={{0,16},{16,0},{1,17},{17,1},{2,18},{18,2},{3,19},{19,3},{4,20},{20... | collective-permute-start | bytes 786440 | tf_op jit(solution)/shard_map/ppermute | solution.py:273
  48.5 16.1 %all-to-all-start.1 = ((bf16[16,8,384]{2,1,0:T(8,128)(2,1)}), bf16[16,8,384]{2,1,0:T(8,128)(2,1)S(1)}, u32[]{:S(2)}, u32[]{:S(2)}) async-start(bf16[16,8,384]{2,1,0:T(8,128)(2,1)} %fusion.7), calls=%async_computation.1 | async-start | bytes 196608 | tf_op jit(solution)/shard_map/all_to_all | solution.py:19
  52.9 13.9 %collective-permute-start.4 = (bf16[16,2,1,32,128]{4,3,0,1,2:T(8,128)(2,1)S(1)}, bf16[16,2,1,32,128]{4,3,0,1,2:T(8,128)(2,1)}, u32[]{:S(2)}, u32[]{:S(2)}) collective-permute-start(bf16[16,2,1,32,128]{4,3,0,1,2:T(8,128)(2,1)S(1)} %collective-permute-done.2), channel_id=1, source_target_pairs={{0,16},{16,0},{1,17},{17,1},{2,18},{18,2},{3,19},{19,3},{4,20},{20... | collective-permute-start | bytes 786440 | tf_op jit(solution)/shard_map/ppermute | solution.py:274
  55.1 10.6 %copy-start.3 = (f32[16,1,384]{2,1,0:T(1,128)S(1)}, f32[16,1,384]{2,1,0:T(1,128)}, u32[]{:S(2)}) copy-start(f32[16,1,384]{2,1,0:T(1,128)} %param.32) | copy-start | bytes 73732
  55.1 10.6 %copy-start.9 = (s32[16]{0:T(128)S(1)}, s32[16]{0:T(128)}, u32[]{:S(2)}) copy-start(s32[16]{0:T(128)} %param.33) | copy-start | bytes 196
  64.7 1.6 copy-start.10
  68.1 19.3 %copy-start.2 = (bf16[16,2048]{1,0:T(8,128)(2,1)S(1)}, bf16[16,2048]{1,0:T(8,128)(2,1)}, u32[]{:S(2)}) copy-start(bf16[16,2048]{1,0:T(8,128)(2,1)} %tokens_ref.1) | copy-start | bytes 196612
  68.1 19.5 %copy-start.7 = (f32[2048]{0:T(1024)S(1)}, f32[2048]{0:T(1024)}, u32[]{:S(2)}) copy-start(f32[2048]{0:T(1024)} %param.35) | copy-start | bytes 24580
  68.4 19.5 %copy-start.4 = (bf16[16,64]{1,0:T(8,128)(2,1)S(1)}, bf16[16,64]{1,0:T(8,128)(2,1)}, u32[]{:S(2)}) copy-start(bf16[16,64]{1,0:T(8,128)(2,1)} %get-tuple-element.30) | copy-start | bytes 6148
  68.4 19.5 %copy-start.5 = (bf16[16,64]{1,0:T(8,128)(2,1)S(1)}, bf16[16,64]{1,0:T(8,128)(2,1)}, u32[]{:S(2)}) copy-start(bf16[16,64]{1,0:T(8,128)(2,1)} %get-tuple-element.29) | copy-start | bytes 6148

commit v7 on v6

--- a/solution.py
+++ b/solution.py
@@ -261,9 +261,10 @@
 
     swap = [(0, 1), (1, 0)]
     neighbours = [(k, k ^ 1) for k in range(quarters)]
-    their_rows = lax.ppermute(own_rows, "c", swap)
-    chip_rows = in_order(own_rows, their_rows, core, 0)
-    pair_rows = in_order(chip_rows, lax.ppermute(chip_rows, "zl", neighbours), side, 0)
+    neighbour_rows = lax.ppermute(own_rows, "zl", neighbours)
+    pair_rows = in_order(own_rows[None, None], neighbour_rows[None, None], side, 0)
+    pair_rows = in_order(pair_rows, lax.ppermute(pair_rows, "c", swap), core, 1)
+    pair_rows = pair_rows.reshape(4 * own_rows.shape[0], own_rows.shape[1])
     projection_width = 3 * head_size
     token_columns = received[:, :seq_count].reshape(chips, 2, half, slab)
     token_columns = token_columns.transpose(0, 2, 1, 3).reshape(chips * half, 2 * slab)

time: 172 us -> 177 us (1.029)
  waiting for transfers between devices: 15.8 us -> 20.9 us
    ppermute x2, waiting for transfers between devices: 0.01 us -> 11.7 us  [the longest x1 11.7 us: layer(): neighbour_rows = lax.ppermute(own_rows, 'zl', neighbours)]
    all_to_all x2, waiting for transfers between devices: 15.7 us -> 9.23 us  [exchanged(): return lax.all_to_all(pieces, axes, split_axis=0, concat_axis=0, tiled=True)]
    ppermute x1, starting transfers between devices: 7.22 us -> 1.92 us  [layer(): other_halves = lax.ppermute(halves, 'zl', neighbours)]
    all_to_all x2, starting transfers between devices: 20 us -> 24.5 us  [exchanged(): return lax.all_to_all(pieces, axes, split_axis=0, concat_axis=0, tiled=True)]
where the time goes in v7:
time: 177 us; the launch traced here: 175 us
  blocking collectives  95.9 us (54%)
  starting transfers between devices  41.4 us (23%)
  waiting for transfers between devices  20.9 us (12%)
  other arithmetic  6.27 us (4%)
  Pallas kernels  4.68 us (3%)
  matrix products  2.93 us (2%)
    all_to_all x7, blocking collectives, exchanged(): return lax.all_to_all(pieces, axes, split_axis=0, concat_axis=0, tiled=True)  95.9 us
    all_to_all x2, starting transfers between devices, exchanged(): return lax.all_to_all(pieces, axes, split_axis=0, concat_axis=0, tiled=True)  24.5 us
    ppermute x1, waiting for transfers between devices, layer(): neighbour_rows = lax.ppermute(own_rows, 'zl', neighbours)  11.7 us
    all_to_all x2, waiting for transfers between devices, exchanged(): return lax.all_to_all(pieces, axes, split_axis=0, concat_axis=0, tiled=True)  9.23 us
    ppermute x1, starting transfers between devices, layer(): their_halves = lax.ppermute(halves, 'c', swap)  5.4 us
    ppermute x1, starting transfers between devices, layer(): pair_rows = in_order(pair_rows, lax.ppermute(pair_rows, 'c', swap), core, 1)  3.84 us
  transfers between devices with their start and end apart: 7, of which 2 were waited for; matrix products, arithmetic and copies ran while one was open for 3% of the time, Pallas kernels for 0%

profile of v7, /device:TPU:1, one launch (start us, length us, event | category | flops | bytes accessed | tf_op | source)
XLA Modules:
  0.0 174.8 jit_solution(5091859230989530922)
XLA Ops:
  0.8 1.9 %first_payload.1 = (bf16[16,80,128]{2,1,0:T(8,128)(2,1)}, f32[16,1]{1,0:T(8,128)}, bf16[64,640]{1,0:T(8,128)(2,1)S(1)}, bf16[16,64]{1,0:T(8,128)(2,1)}, bf16[16,64]{1,0:T(8,128)(2,1)}, /*index=5*/f32[2,16,1]{2,1,0:T(8,128)}) custom-call(bf16[16,2048]{1,0:T(8,128)(2,1)} %tokens_ref.1, f32[1,2048]{1,0:T(1,128)} %bitcast.90, bf16[64,128]{1,0:T(8,128)(2,1)} %bitcast.87, ...), custom_call_target="tpu_custom_call" | custom-call | tf_op jit(solution)/shard_map/first_payload/pallas_call | solution.py:230
  2.7 15.9 %all-to-all-start = ((bf16[16,80,128]{2,1,0:T(8,128)(2,1)}), bf16[16,80,128]{2,1,0:T(8,128)(2,1)S(1)}, u32[]{:S(2)}, u32[]{:S(2)}) async-start(bf16[16,80,128]{2,1,0:T(8,128)(2,1)} %get-tuple-element.21), calls=%async_computation | async-start | bytes 655360 | tf_op jit(solution)/shard_map/all_to_all | solution.py:19
  18.6 3.3 %collective-permute-start = (bf16[64,640]{1,0:T(8,128)(2,1)S(1)}, bf16[64,640]{1,0:T(8,128)(2,1)S(1)}, u32[]{:S(2)}, u32[]{:S(2)}) collective-permute-start(bf16[64,640]{1,0:T(8,128)(2,1)S(1)} %get-tuple-element.22), channel_id=1, source_target_pairs={{0,32},{32,0},{64,96},{96,64},{1,33},{33,1},{65,97},{97,65},{2,34}... | collective-permute-start | bytes 245768 | tf_op jit(solution)/shard_map/ppermute | solution.py:264
  21.9 0.7 broadcast_add_fusion
  22.5 1.0 fusion.17
  23.6 11.7 %collective-permute-done = bf16[64,640]{1,0:T(8,128)(2,1)S(1)} collective-permute-done((bf16[64,640]{1,0:T(8,128)(2,1)S(1)}, bf16[64,640]{1,0:T(8,128)(2,1)S(1)}, u32[]{:S(2)}, u32[]{:S(2)}) %collective-permute-start) | collective-permute-done | bytes 81952 | tf_op jit(solution)/shard_map/ppermute | solution.py:264
  35.4 3.8 %collective-permute-start.1 = (bf16[2,1,64,640]{3,2,1,0:T(8,128)(2,1)S(1)}, bf16[2,1,64,640]{3,2,1,0:T(8,128)(2,1)S(1)}, u32[]{:S(2)}, u32[]{:S(2)}) collective-permute-start(bf16[2,1,64,640]{3,2,1,0:T(8,128)(2,1)S(1)} %maximum_select_fusion.3), channel_id=1, source_target_pairs={{0,16},{16,0},{1,17},{17,1},{2,18},{18,2},{3,19},{19,3},{4,20},{20... | collective-permute-start | bytes 491528 | tf_op jit(solution)/shard_map/ppermute | solution.py:266
  39.2 0.8 fusion.22
  40.1 1.9 %collective-permute-start.2 = (bf16[16,2,1,32,128]{4,3,0,1,2:T(8,128)(2,1)S(1)}, bf16[16,2,1,32,128]{4,3,0,1,2:T(8,128)(2,1)S(1)}, u32[]{:S(2)}, u32[]{:S(2)}) collective-permute-start(bf16[16,2,1,32,128]{4,3,0,1,2:T(8,128)(2,1)S(1)} %copy.43), channel_id=1, source_target_pairs={{0,32},{32,0},{64,96},{96,64},{1,33},{33,1},{65,97},{97,65},{2,34}... | collective-permute-start | bytes 786440 | tf_op jit(solution)/shard_map/ppermute | solution.py:273
  42.3 5.4 %collective-permute-start.3 = (bf16[16,2,1,32,128]{4,3,0,1,2:T(8,128)(2,1)S(1)}, bf16[16,2,1,32,128]{4,3,0,1,2:T(8,128)(2,1)S(1)}, u32[]{:S(2)}, u32[]{:S(2)}) collective-permute-start(bf16[16,2,1,32,128]{4,3,0,1,2:T(8,128)(2,1)S(1)} %copy.43), channel_id=1, source_target_pairs={{0,16},{16,0},{1,17},{17,1},{2,18},{18,2},{3,19},{19,3},{4,20},{20... | collective-permute-start | bytes 786440 | tf_op jit(solution)/shard_map/ppermute | solution.py:274
  47.7 0.8 fusion.7
  48.5 8.7 %all-to-all-start.1 = ((bf16[16,8,384]{2,1,0:T(8,128)(2,1)}), bf16[16,8,384]{2,1,0:T(8,128)(2,1)S(1)}, u32[]{:S(2)}, u32[]{:S(2)}) async-start(bf16[16,8,384]{2,1,0:T(8,128)(2,1)} %fusion.7), calls=%async_computation.1 | async-start | bytes 196608 | tf_op jit(solution)/shard_map/all_to_all | solution.py:19
  57.4 2.4 %collective-permute-start.4 = (bf16[16,2,1,32,128]{4,3,0,1,2:T(8,128)(2,1)S(1)}, bf16[16,2,1,32,128]{4,3,0,1,2:T(8,128)(2,1)}, u32[]{:S(2)}, u32[]{:S(2)}) collective-permute-start(bf16[16,2,1,32,128]{4,3,0,1,2:T(8,128)(2,1)S(1)} %collective-permute-done.2), channel_id=1, source_target_pairs={{0,16},{16,0},{1,17},{17,1},{2,18},{18,2},{3,19},{19,3},{4,20},{20... | collective-permute-start | bytes 786440 | tf_op jit(solution)/shard_map/ppermute | solution.py:275
  59.9 9.2 %all-to-all-done.1 = bf16[16,8,384]{2,1,0:T(8,128)(2,1)S(1)} async-done(((bf16[16,8,384]{2,1,0:T(8,128)(2,1)}), bf16[16,8,384]{2,1,0:T(8,128)(2,1)S(1)}, u32[]{:S(2)}, u32[]{:S(2)}) %all-to-all-start.1) | async-done | bytes 98336 | tf_op jit(solution)/shard_map/all_to_all | solution.py:19
  69.4 0.6 fusion.5
  70.1 0.3 fusion.37
  70.4 0.3 fusion.35
  70.8 0.4 fusion.3
  71.2 1.1 maximum_select_fusion.1
  72.5 0.3 convolution_convert_fusion
  72.9 9.3 %all_to_all.45 = bf16[4,16,2048]{2,1,0:T(8,128)(2,1)S(1)} all-to-all(bf16[4,16,2048]{2,1,0:T(8,128)(2,1)S(1)} %broadcast_in_dim.54), channel_id=1, replica_groups=mesh['zh'=4,'zl'=4,'c'=2,'y'=4,'x'=4] {'x'}, dimensions={0} | all-to-all | bytes 524288 | tf_op jit(solution)/shard_map/all_to_all | solution.py:19
  82.3 9.5 %all_to_all.46 = bf16[4,16,2048]{2,1,0:T(8,128)(2,1)S(1)} all-to-all(bf16[4,16,2048]{2,1,0:T(8,128)(2,1)S(1)} %broadcast_in_dim.55), channel_id=1, replica_groups=mesh['zh'=4,'zl'=4,'c'=2,'y'=4,'x'=4] {'y'}, dimensions={0} | all-to-all | bytes 524288 | tf_op jit(solution)/shard_map/all_to_all | solution.py:19
  92.0 0.2 multiply_reduce_fusion
  92.4 0.2 convolution_convert_fusion.2
  92.7 22.6 %all_to_all.47 = bf16[32,2,640]{2,1,0:T(2,128)(2,1)S(1)} all-to-all(bf16[32,2,640]{2,1,0:T(2,128)(2,1)S(1)} %pad_maximum_fusion.2), channel_id=1, replica_groups=mesh['zh'=4,'zl'=4,'c'=2,'y'=4,'x'=4] {'zh','zl','c'}, dimensions={0} | all-to-all | bytes 163840 | tf_op jit(solution)/shard_map/all_to_all | solution.py:19
  115.5 8.3 %all_to_all.48 = bf16[4,32,2,640]{3,2,1,0:T(2,128)(2,1)S(1)} all-to-all(bf16[4,32,2,640]{3,2,1,0:T(2,128)(2,1)S(1)} %broadcast_in_dim.56), channel_id=1, replica_groups=mesh['zh'=4,'zl'=4,'c'=2,'y'=4,'x'=4] {'x'}, dimensions={0} | all-to-all | bytes 655360 | tf_op jit(solution)/shard_map/all_to_all | solution.py:19
  123.9 2.7 %experts.1 = bf16[64,2560]{1,0:T(8,128)(2,1)S(1)} custom-call(bf16[4,64,640]{2,1,0:T(8,128)(2,1)S(1)} %reshape.416.rows_ref, bf16[256,640]{1,0:T(8,128)(2,1)} %bitcast.74, bf16[2048,128]{1,0:T(8,128)(2,1)} %bitcast.77, bf16[2048,128]{1,0:T(8,128)(2,1)} %bitcast.78, bf16[128,2048]{1,0:T(8,128)(2,1)} %bitcast.79), custom_call_target="tpu_custom_call" | custom-call | tf_op jit(solution)/shard_map/experts/pallas_call | solution.py:341
  126.7 30.4 %all_to_all.49 = bf16[32,2,2560]{2,1,0:T(2,128)(2,1)S(1)} all-to-all(bf16[32,2,2560]{2,1,0:T(2,128)(2,1)S(1)} %reshape.417), channel_id=1, replica_groups=mesh['zh'=4,'zl'=4,'c'=2,'y'=4,'x'=4] {'zh','zl','c'}, dimensions={0} | all-to-all | bytes 655360 | tf_op jit(solution)/shard_map/all_to_all | solution.py:19
  157.9 0.2 fusion.2
  158.2 7.9 %all_to_all.50 = bf16[4,16,2048]{2,1,0:T(8,128)(2,1)S(1)} all-to-all(bf16[4,16,2048]{2,1,0:T(8,128)(2,1)S(1)} %broadcast_in_dim.57), channel_id=1, replica_groups=mesh['zh'=4,'zl'=4,'c'=2,'y'=4,'x'=4] {'x'}, dimensions={0} | all-to-all | bytes 524288 | tf_op jit(solution)/shard_map/all_to_all | solution.py:19
  166.2 7.9 %all_to_all.51 = bf16[4,16,2048]{2,1,0:T(8,128)(2,1)S(1)} all-to-all(bf16[4,16,2048]{2,1,0:T(8,128)(2,1)S(1)} %broadcast_in_dim.58), channel_id=1, replica_groups=mesh['zh'=4,'zl'=4,'c'=2,'y'=4,'x'=4] {'y'}, dimensions={0} | all-to-all | bytes 524288 | tf_op jit(solution)/shard_map/all_to_all | solution.py:19
  174.2 0.6 fusion.12
  (73 shorter events, 2.9 us)
Async XLA Ops:
  0.0 69.4 %copy-start = (bf16[16,1,384,128]{3,2,1,0:T(8,128)(2,1)S(1)}, bf16[16,1,384,128]{3,2,1,0:T(8,128)(2,1)}, u32[]{:S(2)}) copy-start(bf16[16,1,384,128]{3,2,1,0:T(8,128)(2,1)} %param.30) | copy-start | bytes 4718596
  0.0 42.2 %copy-start.8 = (bf16[2048]{0:T(1024)(128)(2,1)S(1)}, bf16[2048]{0:T(1024)(128)(2,1)}, u32[]{:S(2)}) copy-start(bf16[2048]{0:T(1024)(128)(2,1)} %param.39) | copy-start | bytes 12292
  2.7 39.3 %copy-start.6 = (f32[2,16,1]{2,1,0:T(8,128)S(1)}, f32[2,16,1]{2,1,0:T(8,128)}, u32[]{:S(2)}) copy-start(f32[2,16,1]{2,1,0:T(8,128)} %get-tuple-element.26) | copy-start | bytes 388
  2.7 37.3 %all-to-all-start = ((bf16[16,80,128]{2,1,0:T(8,128)(2,1)}), bf16[16,80,128]{2,1,0:T(8,128)(2,1)S(1)}, u32[]{:S(2)}, u32[]{:S(2)}) async-start(bf16[16,80,128]{2,1,0:T(8,128)(2,1)} %get-tuple-element.21), calls=%async_computation | async-start | bytes 655360 | tf_op jit(solution)/shard_map/all_to_all | solution.py:19
  18.6 16.8 %collective-permute-start = (bf16[64,640]{1,0:T(8,128)(2,1)S(1)}, bf16[64,640]{1,0:T(8,128)(2,1)S(1)}, u32[]{:S(2)}, u32[]{:S(2)}) collective-permute-start(bf16[64,640]{1,0:T(8,128)(2,1)S(1)} %get-tuple-element.22), channel_id=1, source_target_pairs={{0,32},{32,0},{64,96},{96,64},{1,33},{33,1},{65,97},{97,65},{2,34}... | collective-permute-start | bytes 245768 | tf_op jit(solution)/shard_map/ppermute | solution.py:264
  35.4 6.8 %collective-permute-start.1 = (bf16[2,1,64,640]{3,2,1,0:T(8,128)(2,1)S(1)}, bf16[2,1,64,640]{3,2,1,0:T(8,128)(2,1)S(1)}, u32[]{:S(2)}, u32[]{:S(2)}) collective-permute-start(bf16[2,1,64,640]{3,2,1,0:T(8,128)(2,1)S(1)} %maximum_select_fusion.3), channel_id=1, source_target_pairs={{0,16},{16,0},{1,17},{17,1},{2,18},{18,2},{3,19},{19,3},{4,20},{20... | collective-permute-start | bytes 491528 | tf_op jit(solution)/shard_map/ppermute | solution.py:266
  40.1 17.1 %collective-permute-start.2 = (bf16[16,2,1,32,128]{4,3,0,1,2:T(8,128)(2,1)S(1)}, bf16[16,2,1,32,128]{4,3,0,1,2:T(8,128)(2,1)S(1)}, u32[]{:S(2)}, u32[]{:S(2)}) collective-permute-start(bf16[16,2,1,32,128]{4,3,0,1,2:T(8,128)(2,1)S(1)} %copy.43), channel_id=1, source_target_pairs={{0,32},{32,0},{64,96},{96,64},{1,33},{33,1},{65,97},{97,65},{2,34}... | collective-permute-start | bytes 786440 | tf_op jit(solution)/shard_map/ppermute | solution.py:273
  42.3 17.6 %copy-start.1 = (bf16[2,2,64,640]{3,2,1,0:T(8,128)(2,1)}, bf16[2,2,64,640]{3,2,1,0:T(8,128)(2,1)S(1)}, u32[]{:S(2)}) copy-start(bf16[2,2,64,640]{3,2,1,0:T(8,128)(2,1)S(1)} %maximum_select_fusion.2) | copy-start | bytes 983044
  42.3 28.9 %collective-permute-start.3 = (bf16[16,2,1,32,128]{4,3,0,1,2:T(8,128)(2,1)S(1)}, bf16[16,2,1,32,128]{4,3,0,1,2:T(8,128)(2,1)S(1)}, u32[]{:S(2)}, u32[]{:S(2)}) collective-permute-start(bf16[16,2,1,32,128]{4,3,0,1,2:T(8,128)(2,1)S(1)} %copy.43), channel_id=1, source_target_pairs={{0,16},{16,0},{1,17},{17,1},{2,18},{18,2},{3,19},{19,3},{4,20},{20... | collective-permute-start | bytes 786440 | tf_op jit(solution)/shard_map/ppermute | solution.py:274
  48.5 20.6 %all-to-all-start.1 = ((bf16[16,8,384]{2,1,0:T(8,128)(2,1)}), bf16[16,8,384]{2,1,0:T(8,128)(2,1)S(1)}, u32[]{:S(2)}, u32[]{:S(2)}) async-start(bf16[16,8,384]{2,1,0:T(8,128)(2,1)} %fusion.7), calls=%async_computation.1 | async-start | bytes 196608 | tf_op jit(solution)/shard_map/all_to_all | solution.py:19
  57.4 13.8 %collective-permute-start.4 = (bf16[16,2,1,32,128]{4,3,0,1,2:T(8,128)(2,1)S(1)}, bf16[16,2,1,32,128]{4,3,0,1,2:T(8,128)(2,1)}, u32[]{:S(2)}, u32[]{:S(2)}) collective-permute-start(bf16[16,2,1,32,128]{4,3,0,1,2:T(8,128)(2,1)S(1)} %collective-permute-done.2), channel_id=1, source_target_pairs={{0,16},{16,0},{1,17},{17,1},{2,18},{18,2},{3,19},{19,3},{4,20},{20... | collective-permute-start | bytes 786440 | tf_op jit(solution)/shard_map/ppermute | solution.py:275
  59.8 10.3 %copy-start.3 = (f32[16,1,384]{2,1,0:T(1,128)S(1)}, f32[16,1,384]{2,1,0:T(1,128)}, u32[]{:S(2)}) copy-start(f32[16,1,384]{2,1,0:T(1,128)} %param.32) | copy-start | bytes 73732
  59.8 10.3 %copy-start.9 = (s32[16]{0:T(128)S(1)}, s32[16]{0:T(128)}, u32[]{:S(2)}) copy-start(s32[16]{0:T(128)} %param.33) | copy-start | bytes 196
  69.1 1.6 copy-start.10
  72.5 19.3 %copy-start.2 = (bf16[16,2048]{1,0:T(8,128)(2,1)S(1)}, bf16[16,2048]{1,0:T(8,128)(2,1)}, u32[]{:S(2)}) copy-start(bf16[16,2048]{1,0:T(8,128)(2,1)} %tokens_ref.1) | copy-start | bytes 196612
  72.5 19.5 %copy-start.7 = (f32[2048]{0:T(1024)S(1)}, f32[2048]{0:T(1024)}, u32[]{:S(2)}) copy-start(f32[2048]{0:T(1024)} %param.35) | copy-start | bytes 24580
  72.8 19.5 %copy-start.4 = (bf16[16,64]{1,0:T(8,128)(2,1)S(1)}, bf16[16,64]{1,0:T(8,128)(2,1)}, u32[]{:S(2)}) copy-start(bf16[16,64]{1,0:T(8,128)(2,1)} %get-tuple-element.30) | copy-start | bytes 6148
  72.8 19.5 %copy-start.5 = (bf16[16,64]{1,0:T(8,128)(2,1)S(1)}, bf16[16,64]{1,0:T(8,128)(2,1)}, u32[]{:S(2)}) copy-start(bf16[16,64]{1,0:T(8,128)(2,1)} %get-tuple-element.29) | copy-start | bytes 6148
